TPU v7x, 32 devices: a whole 2x2x4 slice. The times are simulated.
32 devices in a mesh: ep: 4 (over y, x), tp: 8 (over z, core).
Axes of the slice: x: 2, y: 2, z: 4, core: 2. Of those that a mesh axis runs over, the one named last changes fastest.
Arguments:
- query_rows: bfloat16 [512, 2048], P('ep', 'tp'), may hold values from -32 to 32
- key_rows: bfloat16 [512, 2048], P('ep', 'tp'), may hold values from -8 to 8
- value_rows: bfloat16 [512, 2048], P('ep', 'tp'), may hold values from -8 to 8
- query_norm_gain: float32 [64], replicated, may hold values from 0.1 to 1.9
- key_gain: float32 [64], replicated, may hold values from 0.1 to 1.9
- break_offset: float32 [32], P('tp'), may hold values from -12 to 3
- mixer_out_weight: bfloat16 [2048, 2048], P('tp'), may hold values from -0.75 to 0.75
- routed_tokens: bfloat16 [4096, 2048], P(('ep', 'tp')), may hold values from -6 to 6
- expert_gain: float32 [2048], replicated, may hold values from 0.1 to 1.9
- routes: int32 [4096, 2], P(('ep', 'tp')), may hold values from 0 to 3, as said below
- route_scores: float32 [4096, 2], P(('ep', 'tp')), may hold values from -6 to 6
- gate_weight: bfloat16 [4, 2048, 3584], P('ep', None, 'tp'), may hold values from -0.125 to 0.125
- up_weight: bfloat16 [4, 2048, 3584], P('ep', None, 'tp'), may hold values from -0.125 to 0.125
- down_weight: bfloat16 [4, 3584, 2048], P('ep', 'tp'), may hold values from -0.09375 to 0.09375
Outputs:
- attention_output: bfloat16 [512, 2048], P(('ep', 'tp'))
- expert_output: bfloat16 [4096, 2048], P(('ep', 'tp'))
Inputs may be any that keep to these rules, and one draw needn't show every extreme that they name: `routes`: each row names 2 different experts. Among the rows of one device no expert is named more than 64 times, and one expert is named exactly 64 times by the rows of every device.
All inputs are finite; a program needn't handle non-finite values.
Results may differ from a plain program's by a relative error of at most 0.018.
Values may be sent and summed in bfloat16 or wider, within the bound.
No kernel may reach another device: no remote copies, remote signals or barrier semaphores. Data moves between devices by JAX's collectives and lax.ppermute only.
A program may use at most 128 MiB of HBM per device.

v0:
```python
import jax
import jax.numpy as jnp
from jax import lax
from jax.sharding import PartitionSpec as P

HEAD_DIM = 64
TOP_K = 2


EPS = 1e-06


def shifted(array, axis, by):
    peers = lax.axis_size(axis)
    pairs = [(i, i + by) for i in range(peers) if 0 <= i + by < peers]
    return lax.ppermute(array, axis, pairs)


def norm_heads(flat, gain):
    count = flat.shape[0]
    split = flat.astype(jnp.float32).reshape(count, -1, HEAD_DIM)
    scaled = split * lax.rsqrt(jnp.mean(split * split, axis=2, keepdims=True) + EPS)
    return (scaled * gain).astype(jnp.bfloat16)


def absorb(carry_state, query_norm, key_flat, value_flat, offsets, allowed):
    running_sum, carried = carry_state
    key_count = key_flat.shape[0]
    key_norm = key_flat.reshape(key_count, -1, HEAD_DIM)
    value_heads = value_flat.reshape(key_count, -1, HEAD_DIM)
    scores = jnp.einsum("qhd,khd->hqk", query_norm, key_norm, preferred_element_type=jnp.float32)
    scores = scores * HEAD_DIM ** (-0.5) + offsets[:, None, None]
    log_rise = jax.nn.log_sigmoid(scores)
    log_fail = jnp.where(allowed[None], log_rise - scores, 0.0)
    log_after = carried[:, :, None] + lax.cumsum(log_fail, axis=2, reverse=True) - log_fail
    weights = jnp.where(allowed[None], jnp.exp(log_rise + log_after), 0.0).astype(jnp.bfloat16)
    running_sum = running_sum + jnp.einsum(
        "hqk,khd->qhd", weights, value_heads, preferred_element_type=jnp.float32
    )
    return (running_sum, carried + jnp.sum(log_fail, axis=2))


def mixer_reduce(heads_mixed, mixer_out_weight):
    return lax.psum_scatter(
        jnp.dot(heads_mixed, mixer_out_weight, preferred_element_type=jnp.float32).astype(
            jnp.bfloat16
        ),
        "tp",
        scatter_dimension=0,
        tiled=True,
    ).astype(jnp.float32)


def body(
    query_rows,
    key_rows,
    value_rows,
    query_norm_gain,
    key_gain,
    break_offset,
    mixer_out_weight,
    routed_tokens,
    expert_gain,
    routes,
    route_scores,
    gate_weight,
    up_weight,
    down_weight,
):
    gate_local = gate_weight[0]
    up_local = up_weight[0]
    down_local = down_weight[0]
    row_count = query_rows.shape[0]
    query_norm = norm_heads(query_rows, query_norm_gain)
    head_count = query_norm.shape[1]
    key_flat = norm_heads(key_rows, key_gain).reshape(row_count, -1)
    my_index = lax.axis_index("ep")
    devices_ep = lax.axis_size("ep")
    token_position = jnp.arange(row_count)
    earlier = token_position[None, :] < token_position[:, None]
    carry_state = (
        jnp.zeros((row_count, head_count, HEAD_DIM), jnp.float32),
        jnp.zeros((head_count, row_count), jnp.float32),
    )
    carry_state = absorb(carry_state, query_norm, key_flat, value_rows, break_offset, earlier)

    def next_turn(turn_index, loop_carry):
        key_now, value_now, state_now = loop_carry
        key_now, value_now = shifted((key_now, value_now), "ep", 1)
        allowed = jnp.broadcast_to(my_index >= turn_index, (row_count, row_count))
        return (
            key_now,
            value_now,
            absorb(state_now, query_norm, key_now, value_now, break_offset, allowed),
        )

    carry_state = lax.fori_loop(1, devices_ep, next_turn, (key_flat, value_rows, carry_state))[2]
    heads_mixed = carry_state[0].astype(jnp.bfloat16).reshape(row_count, -1)
    token_count = routed_tokens.shape[0]
    model_width = routed_tokens.shape[1]
    as_float = routed_tokens.astype(jnp.float32)
    normed = (
        as_float
        * lax.rsqrt(jnp.mean(as_float * as_float, axis=1, keepdims=True) + EPS)
        * expert_gain
    ).astype(jnp.bfloat16)
    expert_count = lax.axis_size("ep")
    capacity = max(2, token_count * TOP_K // expert_count)
    flat_routes = routes.reshape(-1)
    member = (flat_routes[:, None] == jnp.arange(expert_count, dtype=jnp.int32)[None, :]).astype(
        jnp.int32
    )
    ahead = jnp.sum((jnp.cumsum(member, axis=0) - member) * member, axis=1)
    slot_index = flat_routes * capacity + ahead
    select = (
        slot_index[:, None] == jnp.arange(expert_count * capacity, dtype=jnp.int32)[None, :]
    ).astype(jnp.bfloat16)
    copies = jnp.repeat(normed, TOP_K, axis=0)
    outgoing = jnp.einsum("cs,cd->sd", select, copies, preferred_element_type=jnp.float32).astype(
        jnp.bfloat16
    )
    arrived = lax.all_to_all(outgoing, "ep", split_axis=0, concat_axis=0, tiled=True)
    piece = lax.all_gather(arrived, "tp", axis=0, tiled=True)
    gate_piece = jnp.dot(piece, gate_local, preferred_element_type=jnp.float32)
    up_piece = jnp.dot(piece, up_local, preferred_element_type=jnp.float32)
    hidden = (jax.nn.silu(gate_piece) * up_piece).astype(jnp.bfloat16)
    mixer_sum = mixer_reduce(heads_mixed, mixer_out_weight)
    expert_sum = lax.psum_scatter(
        jnp.dot(hidden, down_local, preferred_element_type=jnp.float32).astype(jnp.bfloat16),
        "tp",
        scatter_dimension=0,
        tiled=True,
    )
    returned = lax.all_to_all(expert_sum, "ep", split_axis=0, concat_axis=0, tiled=True)
    results = jnp.einsum("cs,sd->cd", select, returned, preferred_element_type=jnp.float32)
    results = results.reshape(token_count, TOP_K, model_width)
    differences = route_scores[:, None, :] - route_scores[:, :, None]
    route_weight = 1.0 / jnp.sum(jnp.exp(differences), axis=2)
    expert_output = jnp.sum(route_weight[..., None] * results, axis=1).astype(jnp.bfloat16)
    return (mixer_sum.astype(jnp.bfloat16), expert_output)


def solution(mesh):
    in_specs = (
        P("ep", "tp"),
        P("ep", "tp"),
        P("ep", "tp"),
        P(),
        P(),
        P("tp"),
        P("tp", None),
        P(("ep", "tp"), None),
        P(),
        P(("ep", "tp"), None),
        P(("ep", "tp"), None),
        P("ep", None, "tp"),
        P("ep", None, "tp"),
        P("ep", "tp", None),
    )
    out_specs = (P(("ep", "tp"), None), P(("ep", "tp"), None))
    return jax.shard_map(body, mesh=mesh, in_specs=in_specs, out_specs=out_specs, check_vma=False)
```

profile of v0, /device:TPU:0, one launch (start us, length us, event | category | flops | bytes accessed | tf_op | source)
XLA Modules:
  0.0 263.1 jit_solution(493648359935207742)
XLA Ops:
  7.2 0.9 copy.60
  8.4 1.2 reduce-window.6
  10.1 1.2 fusion.14
  11.3 1.2 fusion.16
  12.6 0.6 broadcast_in_dim.65
  13.2 1.2 reshape.147
  14.4 1.8 convolution_convert_fusion.1
  16.2 19.2 %all_to_all.24 = bf16[4,64,2048]{2,1,0:T(8,128)(2,1)} all-to-all(bf16[4,64,2048]{2,1,0:T(8,128)(2,1)S(1)} %bitcast.83), channel_id=1, replica_groups=mesh['ep'=4,'tp'=8] {'ep'}, dimensions={0} | all-to-all | bytes 2097152 | tf_op jit(solution)/shard_map/all_to_all | solution.py:122
  35.5 81.9 %all-gather.2.cloned.1.call-done = bf16[2048,2048]{1,0:T(8,128)(2,1)} async-done(((bf16[256,2048]{1,0:T(8,128)(2,1)}), bf16[2048,2048]{1,0:T(8,128)(2,1)}) %all-gather.2.cloned.1.call-update) | async-done | bytes 8388624 | tf_op jit(solution)/shard_map/all_gather | solution.py:123
  117.4 7.2 %fusion.10 = f32[2048,448]{0,1:T(8,128)S(1)} fusion(bf16[2048,2048]{1,0:T(8,128)(2,1)} %all-gather.2.cloned.1.call-done, bf16[1,2048,448]{1,2,0:T(8,128)(2,1)} %param.27), kind=kOutput, calls=%fused_computation.22 | convolution fusion | flops 3758096384 | bytes 13893632 | tf_op jit(solution)/shard_map/dot_general | solution.py:124
  124.6 4.3 %multiply_convert_fusion = bf16[2048,448]{0,1:T(8,128)(2,1)S(1)} fusion(f32[2048,448]{0,1:T(8,128)S(1)} %fusion.10, bf16[2048,2048]{1,0:T(8,128)(2,1)S(1)} %copy-done.8, bf16[1,2048,448]{1,2,0:T(8,128)(2,1)S(1)} %copy-done.9), kind=kOutput, calls=%fused_computation.16 | convolution fusion | flops 3763601408 | bytes 15728640 | tf_op jit(solution)/shard_map/dot_general | solution.py:125
  128.9 6.9 %convolution_convert_fusion = bf16[2048,2048]{1,0:T(8,128)(2,1)} fusion(bf16[2048,448]{0,1:T(8,128)(2,1)S(1)} %multiply_convert_fusion, bf16[1,448,2048]{2,1,0:T(8,128)(2,1)S(1)} %copy-done), kind=kOutput, calls=%fused_computation.15 | convolution fusion | flops 3762290688 | bytes 12058624 | tf_op jit(solution)/shard_map/dot_general | solution.py:129
  136.1 0.5 copy-done.1
  138.0 4.4 %reduce_window_sum.35 = f32[4,128,128]{1,2,0:T(8,128)S(1)} reduce-window(f32[4,128,128]{1,2,0:T(8,128)S(1)} %get-tuple-element.197, f32[]{:T(128)} %constant.53.clone.1), window={size=1x1x128 pad=0_0x0_0x0_127}, to_apply=%region_2.3 | reduce-window | flops 8323072 | bytes 524292 | tf_op jit(solution)/shard_map/absorb/reduce_window_sum | solution.py:35
  142.8 36.9 %while.19 = (s32[]{:T(128)}, bf16[128,256]{0,1:T(8,128)(2,1)S(1)}, bf16[128,256]{0,1:T(8,128)(2,1)S(1)}, f32[128,4,64]{0,2,1:T(8,128)S(1)}, f32[4,128]{1,0:T(4,1...) while((s32[]{:T(128)}, bf16[128,256]{0,1:T(8,128)(2,1)S(1)}, ...), condition=%wide.region_7.8_spmd, body=%wide.region_4.7_spmd.sunk | while | flops 27738116 | bytes 3139796 | solution.py:97
  142.8 3.4 %collective-permute-start = (bf16[128,256]{0,1:T(8,128)(2,1)S(1)}, bf16[128,256]{0,1:T(8,128)(2,1)S(1)}, u32[]{:S(2)}, u32[]{:S(2)}) collective-permute-start(bf16[128,256]{0,1:T(8,128)(2,1)S(1)} %get-tuple-element.268), channel_id=1, source_target_pairs={{0,8},{8,16},{16,24},{1,9},{9,17},{17,25},{2,10},{10,18},{18,26},{... | collective-permute-start | bytes 196616 | tf_op jit(solution)/shard_map/while/body/eval_jaxpr/ppermute | solution.py:16
  146.1 3.4 %collective-permute-start.1 = (bf16[128,256]{0,1:T(8,128)(2,1)S(1)}, bf16[128,256]{0,1:T(8,128)(2,1)S(1)}, u32[]{:S(2)}, u32[]{:S(2)}) collective-permute-start(bf16[128,256]{0,1:T(8,128)(2,1)S(1)} %get-tuple-element.269), channel_id=1, source_target_pairs={{0,8},{8,16},{16,24},{1,9},{9,17},{17,25},{2,10},{10,18},{18,26},{... | collective-permute-start | bytes 196616 | tf_op jit(solution)/shard_map/while/body/eval_jaxpr/ppermute | solution.py:16
  150.0 4.4 %reduce_window_sum.40 = f32[4,128,128]{1,2,0:T(8,128)S(1)} reduce-window(f32[4,128,128]{1,2,0:T(8,128)S(1)} %get-tuple-element.255, f32[]{:T(128)} %constant.53.clone.1..sunk), window={size=1x1x128 pad=0_0x0_0x0_127}, to_apply=%region_5.5 | reduce-window | flops 8323072 | bytes 524292 | tf_op jit(solution)/shard_map/while/body/eval_jaxpr/reduce_window_sum | solution.py:35
  154.5 0.4 fusion.57
  154.9 3.4 %collective-permute-start = (bf16[128,256]{0,1:T(8,128)(2,1)S(1)}, bf16[128,256]{0,1:T(8,128)(2,1)S(1)}, u32[]{:S(2)}, u32[]{:S(2)}) collective-permute-start(bf16[128,256]{0,1:T(8,128)(2,1)S(1)} %get-tuple-element.268), channel_id=1, source_target_pairs={{0,8},{8,16},{16,24},{1,9},{9,17},{17,25},{2,10},{10,18},{18,26},{... | collective-permute-start | bytes 196616 | tf_op jit(solution)/shard_map/while/body/eval_jaxpr/ppermute | solution.py:16
  158.3 3.6 %collective-permute-start.1 = (bf16[128,256]{0,1:T(8,128)(2,1)S(1)}, bf16[128,256]{0,1:T(8,128)(2,1)S(1)}, u32[]{:S(2)}, u32[]{:S(2)}) collective-permute-start(bf16[128,256]{0,1:T(8,128)(2,1)S(1)} %get-tuple-element.269), channel_id=1, source_target_pairs={{0,8},{8,16},{16,24},{1,9},{9,17},{17,25},{2,10},{10,18},{18,26},{... | collective-permute-start | bytes 196616 | tf_op jit(solution)/shard_map/while/body/eval_jaxpr/ppermute | solution.py:16
  162.4 4.4 %reduce_window_sum.40 = f32[4,128,128]{1,2,0:T(8,128)S(1)} reduce-window(f32[4,128,128]{1,2,0:T(8,128)S(1)} %get-tuple-element.255, f32[]{:T(128)} %constant.53.clone.1..sunk), window={size=1x1x128 pad=0_0x0_0x0_127}, to_apply=%region_5.5 | reduce-window | flops 8323072 | bytes 524292 | tf_op jit(solution)/shard_map/while/body/eval_jaxpr/reduce_window_sum | solution.py:35
  166.9 0.4 fusion.57
  167.3 2.5 collective-permute-start
  169.8 4.5 %collective-permute-start.1 = (bf16[128,256]{0,1:T(8,128)(2,1)S(1)}, bf16[128,256]{0,1:T(8,128)(2,1)S(1)}, u32[]{:S(2)}, u32[]{:S(2)}) collective-permute-start(bf16[128,256]{0,1:T(8,128)(2,1)S(1)} %get-tuple-element.269), channel_id=1, source_target_pairs={{0,8},{8,16},{16,24},{1,9},{9,17},{17,25},{2,10},{10,18},{18,26},{... | collective-permute-start | bytes 196616 | tf_op jit(solution)/shard_map/while/body/eval_jaxpr/ppermute | solution.py:16
  174.8 4.4 %reduce_window_sum.40 = f32[4,128,128]{1,2,0:T(8,128)S(1)} reduce-window(f32[4,128,128]{1,2,0:T(8,128)S(1)} %get-tuple-element.255, f32[]{:T(128)} %constant.53.clone.1..sunk), window={size=1x1x128 pad=0_0x0_0x0_127}, to_apply=%region_5.5 | reduce-window | flops 8323072 | bytes 524292 | tf_op jit(solution)/shard_map/while/body/eval_jaxpr/reduce_window_sum | solution.py:35
  179.8 2.4 convolution_convert_fusion.2
  182.1 41.8 %reduce-scatter.5.cloned.1.call-done = bf16[256,2048]{1,0:T(8,128)(2,1)} async-done(((bf16[2048,2048]{1,0:T(8,128)(2,1)}), bf16[256,2048]{1,0:T(8,128)(2,1)}) %reduce-scatter.5.cloned.1.call-update) | async-done | bytes 1048592 | tf_op jit(solution)/shard_map/reduce_scatter | solution.py:128
  223.9 3.7 %all-to-all-start.1 = ((bf16[4,64,2048]{2,1,0:T(8,128)(2,1)}), bf16[4,64,2048]{2,1,0:T(8,128)(2,1)S(1)}, u32[]{:S(2)}, u32[]{:S(2)}) async-start(bf16[4,64,2048]{2,1,0:T(8,128)(2,1)} %bitcast.86), calls=%async_computation.3 | async-start | bytes 2097152 | tf_op jit(solution)/shard_map/all_to_all | solution.py:134
  227.9 11.7 %all-to-all-done.1 = bf16[4,64,2048]{2,1,0:T(8,128)(2,1)S(1)} async-done(((bf16[4,64,2048]{2,1,0:T(8,128)(2,1)}), bf16[4,64,2048]{2,1,0:T(8,128)(2,1)S(1)}, u32[]{:S(2)}, u32[]{:S(2)}) %all-to-all-start.1) | async-done | bytes 1048608 | tf_op jit(solution)/shard_map/all_to_all | solution.py:134
  239.6 1.3 fusion.12
  241.0 15.6 %reduce-scatter.3.cloned.1.call-done = bf16[16,2048]{1,0:T(8,128)(2,1)} async-done(((bf16[128,2048]{1,0:T(8,128)(2,1)}), bf16[16,2048]{1,0:T(8,128)(2,1)}) %reduce-scatter.3.cloned.1.call-update) | async-done | bytes 65552 | tf_op jit(solution)/shard_map/reduce_scatter | solution.py:44
  (82 shorter events, 4.8 us)
Async XLA Ops:
  7.2 121.7 %copy-start = (bf16[1,448,2048]{2,1,0:T(8,128)(2,1)S(1)}, bf16[1,448,2048]{2,1,0:T(8,128)(2,1)}, u32[]{:S(2)}) copy-start(bf16[1,448,2048]{2,1,0:T(8,128)(2,1)} %param.29) | copy-start | bytes 5505028
  7.2 110.2 %all-gather.2.cloned.1.call-start = ((), (), s32[]{:S(2)}) async-start(), calls=%async_computation.5 | async-start | bytes 9437184 | tf_op jit(solution)/shard_map/all_gather | solution.py:123
  35.5 188.5 %reduce-scatter.5.cloned.1.call-start = ((), (), s32[]{:S(2)}) async-start(), calls=%async_computation.6 | async-start | bytes 9437184 | tf_op jit(solution)/shard_map/reduce_scatter | solution.py:128
  117.4 7.2 %copy-start.8 = (bf16[2048,2048]{1,0:T(8,128)(2,1)S(1)}, bf16[2048,2048]{1,0:T(8,128)(2,1)}, u32[]{:S(2)}) copy-start(bf16[2048,2048]{1,0:T(8,128)(2,1)} %all-gather.2.cloned.1.call-done) | copy-start | bytes 25165828
  117.4 7.2 %copy-start.9 = (bf16[1,2048,448]{1,2,0:T(8,128)(2,1)S(1)}, bf16[1,2048,448]{1,2,0:T(8,128)(2,1)}, u32[]{:S(2)}) copy-start(bf16[1,2048,448]{1,2,0:T(8,128)(2,1)} %param.28) | copy-start | bytes 5505028
  135.8 0.8 copy-start.1
  135.8 0.9 copy-start.2
  135.8 1.1 copy-start.3
  135.8 1.2 copy-start.7
  135.8 1.5 copy-start.6
  135.8 1.6 copy-start.10
  135.8 120.7 %reduce-scatter.3.cloned.1.call-start = ((), (), s32[]{:S(2)}) async-start(), calls=%async_computation.4 | async-start | bytes 589824 | tf_op jit(solution)/shard_map/reduce_scatter | solution.py:44
  142.8 6.8 %collective-permute-start = (bf16[128,256]{0,1:T(8,128)(2,1)S(1)}, bf16[128,256]{0,1:T(8,128)(2,1)S(1)}, u32[]{:S(2)}, u32[]{:S(2)}) collective-permute-start(bf16[128,256]{0,1:T(8,128)(2,1)S(1)} %get-tuple-element.268), channel_id=1, source_target_pairs={{0,8},{8,16},{16,24},{1,9},{9,17},{17,25},{2,10},{10,18},{18,26},{... | collective-permute-start | bytes 196616 | tf_op jit(solution)/shard_map/while/body/eval_jaxpr/ppermute | solution.py:16
  146.1 8.3 %collective-permute-start.1 = (bf16[128,256]{0,1:T(8,128)(2,1)S(1)}, bf16[128,256]{0,1:T(8,128)(2,1)S(1)}, u32[]{:S(2)}, u32[]{:S(2)}) collective-permute-start(bf16[128,256]{0,1:T(8,128)(2,1)S(1)} %get-tuple-element.269), channel_id=1, source_target_pairs={{0,8},{8,16},{16,24},{1,9},{9,17},{17,25},{2,10},{10,18},{18,26},{... | collective-permute-start | bytes 196616 | tf_op jit(solution)/shard_map/while/body/eval_jaxpr/ppermute | solution.py:16
  154.9 7.0 %collective-permute-start = (bf16[128,256]{0,1:T(8,128)(2,1)S(1)}, bf16[128,256]{0,1:T(8,128)(2,1)S(1)}, u32[]{:S(2)}, u32[]{:S(2)}) collective-permute-start(bf16[128,256]{0,1:T(8,128)(2,1)S(1)} %get-tuple-element.268), channel_id=1, source_target_pairs={{0,8},{8,16},{16,24},{1,9},{9,17},{17,25},{2,10},{10,18},{18,26},{... | collective-permute-start | bytes 196616 | tf_op jit(solution)/shard_map/while/body/eval_jaxpr/ppermute | solution.py:16
  158.3 8.6 %collective-permute-start.1 = (bf16[128,256]{0,1:T(8,128)(2,1)S(1)}, bf16[128,256]{0,1:T(8,128)(2,1)S(1)}, u32[]{:S(2)}, u32[]{:S(2)}) collective-permute-start(bf16[128,256]{0,1:T(8,128)(2,1)S(1)} %get-tuple-element.269), channel_id=1, source_target_pairs={{0,8},{8,16},{16,24},{1,9},{9,17},{17,25},{2,10},{10,18},{18,26},{... | collective-permute-start | bytes 196616 | tf_op jit(solution)/shard_map/while/body/eval_jaxpr/ppermute | solution.py:16
  167.3 7.0 %collective-permute-start = (bf16[128,256]{0,1:T(8,128)(2,1)S(1)}, bf16[128,256]{0,1:T(8,128)(2,1)S(1)}, u32[]{:S(2)}, u32[]{:S(2)}) collective-permute-start(bf16[128,256]{0,1:T(8,128)(2,1)S(1)} %get-tuple-element.268), channel_id=1, source_target_pairs={{0,8},{8,16},{16,24},{1,9},{9,17},{17,25},{2,10},{10,18},{18,26},{... | collective-permute-start | bytes 196616 | tf_op jit(solution)/shard_map/while/body/eval_jaxpr/ppermute | solution.py:16
  169.8 9.5 %collective-permute-start.1 = (bf16[128,256]{0,1:T(8,128)(2,1)S(1)}, bf16[128,256]{0,1:T(8,128)(2,1)S(1)}, u32[]{:S(2)}, u32[]{:S(2)}) collective-permute-start(bf16[128,256]{0,1:T(8,128)(2,1)S(1)} %get-tuple-element.269), channel_id=1, source_target_pairs={{0,8},{8,16},{16,24},{1,9},{9,17},{17,25},{2,10},{10,18},{18,26},{... | collective-permute-start | bytes 196616 | tf_op jit(solution)/shard_map/while/body/eval_jaxpr/ppermute | solution.py:16
  179.7 48.2 %copy-start.5 = (f32[128,2]{0,1:T(2,128)S(1)}, f32[128,2]{0,1:T(2,128)}, u32[]{:S(2)}) copy-start(f32[128,2]{0,1:T(2,128)} %param.26) | copy-start | bytes 3076
  179.7 48.2 %copy-start.4 = (s32[128,2]{0,1:T(2,128)S(1)}, s32[128,2]{0,1:T(2,128)}, u32[]{:S(2)}) copy-start(s32[128,2]{0,1:T(2,128)} %param.25) | copy-start | bytes 3076
  223.9 15.7 %all-to-all-start.1 = ((bf16[4,64,2048]{2,1,0:T(8,128)(2,1)}), bf16[4,64,2048]{2,1,0:T(8,128)(2,1)S(1)}, u32[]{:S(2)}, u32[]{:S(2)}) async-start(bf16[4,64,2048]{2,1,0:T(8,128)(2,1)} %bitcast.86), calls=%async_computation.3 | async-start | bytes 2097152 | tf_op jit(solution)/shard_map/all_to_all | solution.py:134
Sparse Core Ops, SparseCore 0:
  35.6 81.7 all-gather.1
  136.0 87.9 reduce-scatter.4
  226.8 29.7 reduce-scatter.2
where the time goes:
time: 264 us; the launch traced here: 263 us
  waiting for transfers between devices  151 us (57%)
  matrix products  26.4 us (10%)
  starting transfers between devices  24.8 us (9%)
  other arithmetic  22.8 us (9%)
  blocking collectives  19.2 us (7%)
  between operations  14 us (5%)
  local copies, waits for them, and re-layouts  4.56 us (2%)
    all_gather x1, waiting for transfers between devices, body(): piece = lax.all_gather(arrived, 'tp', axis=0, tiled=True)  81.9 us
    reduce_scatter x1, waiting for transfers between devices, body(): lax.psum_scatter(jnp.dot(hidden, down_local, preferred_element_type=jnp.f...  41.8 us
    ppermute x6, starting transfers between devices, shifted(): return lax.ppermute(array, axis, pairs)  20.8 us
    all_to_all x1, blocking collectives, body(): lax.all_to_all(outgoing, 'ep', split_axis=0, concat_axis=0, tiled=True)  19.2 us
    another operation x4, other arithmetic, absorb(): lax.cumsum(log_fail, axis=2, reverse=True)  17.7 us
    reduce_scatter x1, waiting for transfers between devices, mixer_reduce(): lax.psum_scatter(jnp.dot(heads_mixed, mixer_out_weight, preferred_element...  15.6 us
    all_to_all x1, waiting for transfers between devices, body(): lax.all_to_all(expert_sum, 'ep', split_axis=0, concat_axis=0, tiled=True)  11.7 us
    dot_general x1, matrix products, body(): gate_piece = jnp.dot(piece, gate_local, preferred_element_type=jnp.float32)  7.17 us
  transfers between devices with their start and end apart: 10, of which 4 were waited for; matrix products, arithmetic and copies ran while one was open for 10% of the time, Pallas kernels for 0%

commit v1 on v0

v1 whole, which is shorter than its diff:
```python
import jax
import jax.numpy as jnp
from jax import lax
from jax.experimental import pallas as pl
from jax.experimental.pallas import tpu as pltpu
from jax.sharding import PartitionSpec as P


HEAD_DIM = 64
TOP_K = 2
CORES = 2
LANES = 128
MOST_PERMUTES = 8


EPS = 1e-06


def partner(index, step, count):
    if count & (count - 1) == 0:
        return index ^ step
    return (index + step) % count


def relative(target, index, count):
    if count & (count - 1) == 0:
        return target ^ index
    return (target - index + count) % count


def over_ep(pieces, back=False):
    count = lax.axis_size("ep")
    if len(pieces) == 1:
        return [lax.all_to_all(pieces[0], "ep", split_axis=0, concat_axis=0, tiled=True)]
    moved = [pieces[0]]
    for step in range(1, count):
        pairs = [(i, partner(i, step, count)) for i in range(count)]
        if back:
            pairs = [(b, a) for a, b in pairs]
        moved.append(lax.ppermute(pieces[step], "ep", pairs))
    return moved


def over_z(array, pairs):
    pairs = [(a * CORES + c, b * CORES + c) for a, b in pairs for c in range(CORES)]
    return lax.ppermute(array, "tp", pairs)


RELAYED = 4


def gather_z(packed, levels):
    if levels != RELAYED:
        return [
            [over_z(packed, [(i, partner(i, step, levels)) for i in range(levels)])]
            for step in range(1, levels)
        ]
    beside = over_z(packed, [(0, 1), (1, 0), (2, 3), (3, 2)])
    across = over_z(packed, [(1, 2), (2, 1)])
    beyond = over_z(beside, [(1, 2), (2, 1)])
    second = over_z(across, [(1, 0), (2, 3)])
    third = over_z(beyond, [(1, 0), (2, 3)])
    return [[beside], [second, across], [third, beyond]]


def target_level(index, outer, level, levels):
    if levels != RELAYED:
        if levels & (levels - 1) == 0:
            return index ^ level
        return (index - level + levels) % levels
    return index ^ (3 - outer) if level == 2 else index ^ (2 + outer)


def over_core(array, step):
    count = lax.axis_size("tp")
    pairs = [(i, i // CORES * CORES + (i + step) % CORES) for i in range(count)]
    return lax.ppermute(array, "tp", pairs)


def dot(a, b, dims=((1,), (0,)), precision=None):
    return lax.dot_general(
        a, b, (dims, ((), ())), precision=precision, preferred_element_type=jnp.float32
    )


def whole(array):
    return pl.BlockSpec(array.shape, lambda *_: (0,) * array.ndim)


VECTOR = pl.BlockSpec(memory_space=pltpu.VMEM)
REMAIN = pl.BlockSpec(memory_space=pltpu.HBM)
PARAMS = pltpu.CompilerParams(vmem_limit_bytes=16 * 1024 * 1024)


SCALAR = pl.BlockSpec(memory_space=pltpu.SMEM)


def head_norm(rows, gain):
    split = rows.astype(jnp.float32)
    mean = jnp.sum(split * split, axis=1, keepdims=True) * (1.0 / HEAD_DIM)
    return (split * lax.rsqrt(mean + EPS) * gain).astype(jnp.bfloat16)


def attention_kernel(slots, *refs):
    me_ref, offset_ref, query_ref, query_gain_ref, key_gain_ref, mixer_ref = refs[:6]
    key_ref, value_ref, *block_refs, keep_ref, give_ref, terms_ref = refs[6:]
    row_count, width = query_ref.shape
    head_count = width // HEAD_DIM
    me = me_ref[0]
    if slots is None:
        blocks = [(block_refs[0][:, :width], block_refs[0][:, width:])]
        places = [0]
    else:
        fold = block_refs[0].shape[1] // (2 * width)
        part = row_count // fold
        blocks = [(key_ref[...], value_ref[...])]
        for ref in block_refs:
            rows = ref[slots : slots + part]
            rows = jnp.concatenate(
                [rows[:, 2 * width * f : 2 * width * (f + 1)] for f in range(fold)], axis=0
            )
            blocks.append((rows[:, :width], rows[:, width:]))
        places = [partner(me, step, len(blocks)) * row_count for step in range(len(blocks))]
    query_place = me * row_count + lax.broadcasted_iota(jnp.int32, (row_count, 1), 0)
    block_rows = blocks[0][0].shape[0]
    row = lax.broadcasted_iota(jnp.int32, (block_rows, block_rows), 0)
    column = lax.broadcasted_iota(jnp.int32, (block_rows, block_rows), 1)
    later = jnp.where(row > column, 1.0, 0.0).astype(jnp.bfloat16)
    key_iota = lax.broadcasted_iota(jnp.int32, (1, block_rows), 1)
    mixed = []
    for head in range(head_count):
        cut = slice(head * HEAD_DIM, (head + 1) * HEAD_DIM)
        query = head_norm(query_ref[:, cut], query_gain_ref[...])
        rises, fails, totals, allows = [], [], [], []
        for index, (keys, _) in enumerate(blocks):
            key = head_norm(keys[:, cut], key_gain_ref[...])
            scores = dot(query, key, ((1,), (1,))) * HEAD_DIM ** (-0.5) + offset_ref[head]
            before = places[index] + key_iota < query_place
            rise = jnp.minimum(scores, 0.0) - jnp.log1p(jnp.exp(-jnp.abs(scores)))
            fail = jnp.where(before, rise - scores, 0.0)
            rises.append(rise)
            fails.append(fail)
            allows.append(before)
            totals.append(jnp.sum(fail, axis=1, keepdims=True))
        mix = jnp.zeros((row_count, HEAD_DIM), jnp.float32)
        for index, (_, values) in enumerate(blocks):
            after = jnp.zeros((row_count, 1), jnp.float32)
            for other in range(len(blocks)):
                if other != index:
                    behind = places[other] > places[index]
                    after = after + jnp.where(behind, totals[other], 0.0)
            rest = fails[index]
            for _ in range(3):
                part = rest.astype(jnp.bfloat16)
                after = after + dot(part, later)
                rest = rest - part.astype(jnp.float32)
            weights = jnp.where(allows[index], jnp.exp(rises[index] + after), 0.0)
            mix = mix + dot(weights.astype(jnp.bfloat16), values[:, cut])
        mixed.append(mix.astype(jnp.bfloat16))
    terms = dot(jnp.concatenate(mixed, axis=1), mixer_ref[...]).astype(jnp.bfloat16)
    levels, owned = keep_ref.shape[:2]
    for index in range(levels * CORES):
        terms_ref[index] = terms[index * owned : (index + 1) * owned]
    core = me_ref[2]
    for level in range(levels):
        keep_ref[level] = terms_ref[level * CORES + core]
        give_ref[level] = terms_ref[level * CORES + 1 - core]


def attention(
    me, blocks, slots, query_rows, key_rows, value_rows, query_norm_gain, key_gain, offset, mixer
):
    row_count = query_rows.shape[0]
    owners = lax.axis_size("tp")
    shape = (owners // CORES, row_count // owners, mixer.shape[1])
    args = (query_rows, query_norm_gain[None], key_gain[None], mixer, key_rows, value_rows)
    return pl.pallas_call(
        lambda *refs: attention_kernel(slots, *refs),
        out_shape=[jax.ShapeDtypeStruct(shape, jnp.bfloat16)] * 2,
        grid=(1,),
        in_specs=[SCALAR, SCALAR] + [whole(a) for a in (*args, *blocks)],
        out_specs=[VECTOR] * 2,
        scratch_shapes=[pltpu.VMEM((owners, *shape[1:]), jnp.bfloat16)],
        compiler_params=PARAMS,
        cost_estimate=pl.CostEstimate(
            flops=6_000_000_000, bytes_accessed=3_000_000, transcendentals=1_000_000
        ),
        name="attention",
    )(me, offset, *args, *blocks)


def hits(rows, slot_count, capacity):
    slots = lax.broadcasted_iota(jnp.int32, (slot_count, 1), 0).astype(jnp.float32)
    return [
        rows[TOP_K + k : TOP_K + k + 1] * capacity + rows[k : k + 1] == slots for k in range(TOP_K)
    ]


def spread(rows, tokens, out_refs, slot_count, capacity):
    piece_rows = slot_count // len(out_refs)
    picked = 0.0
    for hit in hits(rows, slot_count, capacity):
        picked = picked + jnp.where(hit, 1.0, 0.0)
    picked = picked.astype(jnp.bfloat16)
    for index, ref in enumerate(out_refs):
        part = picked[index * piece_rows : (index + 1) * piece_rows]
        ref[:piece_rows] = dot(part, tokens).astype(jnp.bfloat16)


def prepare_kernel(expert_count, capacity, me_ref, *refs):
    inputs, outputs, scratch = refs[:6], refs[6:-6], refs[-6:]
    packed_ref, *out_refs = outputs
    both_ref = scratch[4]
    tokens_ref, gain_ref, routes_ref, scores_ref = scratch[:4]
    half = both_ref.shape[1] // 2
    targets = (*scratch[:4], both_ref.at[:, :half], both_ref.at[:, half:])
    copies = [
        pltpu.make_async_copy(source, target, scratch[5].at[index])
        for index, (source, target) in enumerate(zip(inputs, targets))
    ]
    for copy in copies:
        copy.start()
    for copy in copies:
        copy.wait()
    token_count, width = tokens_ref.shape
    as_float = tokens_ref[...].astype(jnp.float32)
    mean = jnp.sum(as_float * as_float, axis=1, keepdims=True) * (1.0 / width)
    normed = (as_float * lax.rsqrt(mean + EPS) * gain_ref[...]).astype(jnp.bfloat16)
    packed_ref[:, :width] = normed
    routes = routes_ref[...]
    scores = scores_ref[...]
    experts = lax.broadcasted_iota(jnp.int32, (expert_count, 1), 0)
    row = lax.broadcasted_iota(jnp.int32, (token_count, token_count), 0)
    column = lax.broadcasted_iota(jnp.int32, (token_count, token_count), 1)
    earlier = jnp.where(row < column, 1.0, 0.0).astype(jnp.bfloat16)
    taken = jnp.zeros((expert_count, 1), jnp.float32)
    aheads, nears, weights = [], [], []
    for k in range(TOP_K):
        chosen = routes[k : k + 1]
        member = jnp.where(chosen == experts, 1.0, 0.0)
        ahead = dot(member.astype(jnp.bfloat16), earlier) + taken
        aheads.append(jnp.sum(member * ahead, axis=0, keepdims=True))
        taken = taken + jnp.sum(member, axis=1, keepdims=True)
        if len(out_refs) == 1:
            near = chosen
        else:
            near = relative(chosen, me_ref[0], expert_count)
        nears.append(near.astype(jnp.float32))
        total = 0.0
        for j in range(TOP_K):
            total = total + jnp.exp(scores[j : j + 1] - scores[k : k + 1])
        weights.append(1.0 / total)
    rows = aheads + nears + weights
    rows = jnp.concatenate(
        rows + [jnp.zeros((LANES - len(rows), token_count), jnp.float32)], axis=0
    )
    packed_ref[:, width:] = rows.T.astype(jnp.bfloat16)
    slot_count = expert_count * capacity
    spread(rows, normed, out_refs, slot_count, capacity)
    for ref in out_refs[1:]:
        fold = width // both_ref.shape[1]
        part = both_ref.shape[0] // fold
        for f in range(fold):
            columns = slice(f * both_ref.shape[1], (f + 1) * both_ref.shape[1])
            ref[capacity:, columns] = both_ref[f * part : (f + 1) * part]


def piece_shapes(count, slot_count, width):
    return [
        jax.ShapeDtypeStruct((slot_count // count, width), jnp.bfloat16) for _ in range(count)
    ]


def prepare(me, tokens, gain, routes, scores, keys, values, expert_count, piece_count, capacity):
    token_count, width = tokens.shape
    both = (keys.shape[0], keys.shape[1] + values.shape[1])
    shapes = [jax.ShapeDtypeStruct((token_count, width + LANES), jnp.bfloat16)]
    shapes += piece_shapes(piece_count, expert_count * capacity, width)
    extra = both[0] * both[1] // width
    shapes[2:] = [jax.ShapeDtypeStruct((capacity + extra, width), jnp.bfloat16)] * (piece_count - 1)
    args = (tokens, gain[None], routes.T, scores.T, keys, values)
    args = tuple(pltpu.with_memory_space_constraint(a, pltpu.HBM) for a in args)
    packed, *pieces = pl.pallas_call(
        lambda *refs: prepare_kernel(expert_count, capacity, *refs),
        out_shape=shapes,
        in_specs=[SCALAR] + [REMAIN] * len(args),
        out_specs=[VECTOR] * len(shapes),
        scratch_shapes=[pltpu.VMEM(a.shape, a.dtype) for a in args[:4]]
        + [pltpu.VMEM(both, keys.dtype), pltpu.SemaphoreType.DMA((len(args),))],
        compiler_params=PARAMS,
        cost_estimate=pl.CostEstimate(
            flops=2_000_000_000, bytes_accessed=3_000_000, transcendentals=0
        ),
        name="prepare",
    )(me, *args)
    return packed, pieces


def select(me, candidates, piece_count, slot_count, capacity):
    token_count, width = candidates[0].shape
    width -= LANES

    def kernel(me_ref, *refs):
        packed = refs[0][...]
        if len(candidates) > 1:
            packed = jnp.where(me_ref[1] == 1, packed, refs[1][...])
        columns_ref, *out_refs = refs[len(candidates) :]
        columns_ref[...] = packed[:, width:]
        rows = packed[:, width:].astype(jnp.float32).T
        spread(rows, packed[:, :width], out_refs, slot_count, capacity)

    shapes = [jax.ShapeDtypeStruct((token_count, LANES), jnp.bfloat16)]
    shapes += piece_shapes(piece_count, slot_count, width)
    columns, *pieces = pl.pallas_call(
        kernel,
        out_shape=shapes,
        in_specs=[SCALAR] + [VECTOR] * len(candidates),
        out_specs=[VECTOR] * len(shapes),
        compiler_params=PARAMS,
        cost_estimate=pl.CostEstimate(
            flops=1_500_000_000, bytes_accessed=2_000_000, transcendentals=0
        ),
        name="select",
    )(me, *candidates)
    return columns, pieces


def expert_layer(pieces, piece_rows, weights, joined=False, addend=None):
    width = pieces[0].shape[1]
    count = len(pieces)
    row_count = count * piece_rows
    units = weights[0][0].shape[0]
    groups = len(weights)
    addends = [] if addend is None else [addend]
    far = [w for group in weights[1:] for w in group]

    def kernel(*refs):
        refs = list(refs)
        rows_refs = [refs.pop(0) for _ in pieces]
        addend_refs = [refs.pop(0) for _ in addends]
        own_refs = [refs.pop(0) for _ in range(3)]
        far_refs = [refs.pop(0) for _ in far]
        semaphores = refs.pop()
        near_refs = refs[len(refs) - len(far) :]
        out_refs = refs[: len(refs) - len(far)]
        copies = [
            pltpu.make_async_copy(source, target, semaphores.at[index])
            for index, (source, target) in enumerate(zip(far_refs, near_refs))
        ]
        for copy in copies:
            copy.start()
        rows = jnp.concatenate([ref[:piece_rows] for ref in rows_refs], axis=0)
        total = jnp.zeros((row_count, width), jnp.float32)
        for ref in addend_refs:
            total = ref[...].astype(jnp.float32)
        for g in range(groups):
            if g == 0:
                gate_ref, up_ref, down_ref = own_refs
            else:
                gate_ref, up_ref, down_ref = near_refs[3 * g - 3 : 3 * g]
                for copy in copies[3 * g - 3 : 3 * g]:
                    copy.wait()
            gate = dot(rows, gate_ref[...], ((1,), (1,)))
            up = dot(rows, up_ref[...], ((1,), (1,)))
            hidden = (gate / (1.0 + jnp.exp(-gate)) * up).astype(jnp.bfloat16)
            total = total + dot(hidden, down_ref[...])
        total = total.astype(jnp.bfloat16)
        part = row_count // len(out_refs)
        for index, ref in enumerate(out_refs):
            ref[...] = total[index * part : (index + 1) * part]

    shapes = piece_shapes(1 if joined else count, row_count, width)
    return list(
        pl.pallas_call(
            kernel,
            out_shape=shapes,
            in_specs=[VECTOR] * (count + len(addends) + 3) + [REMAIN] * len(far),
            out_specs=[VECTOR] * len(shapes),
            scratch_shapes=[pltpu.VMEM(w.shape, w.dtype) for w in far]
            + [pltpu.SemaphoreType.DMA((len(far),))],
            compiler_params=PARAMS,
            cost_estimate=pl.CostEstimate(
                flops=6 * row_count * units * groups * width,
                bytes_accessed=6 * units * groups * width,
                transcendentals=row_count * units * groups,
            ),
            name="expert_layer",
        )(*pieces, *addends, *weights[0], *far)
    )


def mixing(columns, piece_refs, capacity):
    slot_count = sum(ref.shape[0] for ref in piece_refs)
    columns = columns.astype(jnp.float32)
    slots = lax.broadcasted_iota(jnp.int32, (1, slot_count), 1).astype(jnp.float32)
    mix = 0.0
    for k in range(TOP_K):
        near = columns[:, TOP_K + k : TOP_K + k + 1]
        hit = near * capacity + columns[:, k : k + 1] == slots
        mix = mix + jnp.where(hit, columns[:, 2 * TOP_K + k : 2 * TOP_K + k + 1], 0.0)
    rows = jnp.concatenate([ref[...] for ref in piece_refs], axis=0)
    return dot(mix.astype(jnp.bfloat16), rows)


def combine(me, columns, pieces, capacity, level, levels, keep, took):
    token_count, width = columns.shape[0], pieces[0].shape[1]
    owned = keep.shape[1]

    def kernel(me_ref, columns_ref, keep_ref, took_ref, *refs):
        mixed = mixing(columns_ref[...], refs[:-1], capacity).astype(jnp.bfloat16)
        refs[-1][:token_count] = mixed
        targets = [target_level(me_ref[3], me_ref[1], level, levels)]
        if levels == RELAYED:
            targets.append(me_ref[3] ^ 1)
        for index, target in enumerate(targets):
            both = keep_ref[target].astype(jnp.float32) + took_ref[target].astype(jnp.float32)
            start = token_count + index * owned
            refs[-1][start : start + owned] = both.astype(jnp.bfloat16)

    rows = token_count + (2 if levels == RELAYED else 1) * owned
    return pl.pallas_call(
        kernel,
        out_shape=jax.ShapeDtypeStruct((rows, width), jnp.bfloat16),
        in_specs=[SCALAR] + [VECTOR] * (3 + len(pieces)),
        out_specs=VECTOR,
        compiler_params=PARAMS,
        cost_estimate=pl.CostEstimate(
            flops=1_500_000_000, bytes_accessed=2_000_000, transcendentals=0
        ),
        name="combine",
    )(me, columns, keep, took, *pieces)


def merge(share, beside, across, token_count, owned):
    end = token_count + owned

    def kernel(share_ref, beside_ref, across_ref, out_ref):
        total = share_ref[:end].astype(jnp.float32) + beside_ref[:end].astype(jnp.float32)
        out_ref[:token_count] = total[:token_count].astype(jnp.bfloat16)
        last = total[token_count:] + across_ref[end:].astype(jnp.float32)
        out_ref[token_count:] = last.astype(jnp.bfloat16)

    return pl.pallas_call(
        kernel,
        out_shape=jax.ShapeDtypeStruct((end, share.shape[1]), jnp.bfloat16),
        in_specs=[VECTOR] * 3,
        out_specs=VECTOR,
        compiler_params=PARAMS,
        cost_estimate=pl.CostEstimate(
            flops=500_000_000, bytes_accessed=2_000_000, transcendentals=0
        ),
        name="merge",
    )(share, beside, across)


def finish(me, packed, pieces, capacity, expert_shares, mixer_shares, keep, took):
    token_count, width = packed.shape
    width -= LANES
    owned = keep.shape[1]
    shares = list({id(a): a for a in (*expert_shares, *(a for a, _ in mixer_shares))}.values())
    places = {id(a): index for index, a in enumerate(shares)}

    def kernel(me_ref, columns_ref, keep_ref, took_ref, *refs):
        piece_refs = refs[: len(pieces)]
        share_refs = refs[len(pieces) : -2]
        expert_ref, mixer_ref = refs[-2:]
        total = mixing(columns_ref[...], piece_refs, capacity)
        for share in expert_shares:
            total = total + share_refs[places[id(share)]][:token_count].astype(jnp.float32)
        expert_ref[...] = total.astype(jnp.bfloat16)
        level = me_ref[3]
        mixer = keep_ref[level].astype(jnp.float32) + took_ref[level].astype(jnp.float32)
        for share, slot in mixer_shares:
            start = token_count + slot * owned
            rows = share_refs[places[id(share)]][start : start + owned]
            mixer = mixer + rows.astype(jnp.float32)
        mixer_ref[...] = mixer.astype(jnp.bfloat16)

    shapes = (
        jax.ShapeDtypeStruct((token_count, width), jnp.bfloat16),
        jax.ShapeDtypeStruct(keep.shape[1:], jnp.bfloat16),
    )
    return pl.pallas_call(
        kernel,
        grid=(1,),
        out_shape=shapes,
        in_specs=[SCALAR, pl.BlockSpec((token_count, LANES), lambda i: (0, width // LANES))]
        + [whole(a) for a in (keep, took, *pieces, *shares)],
        out_specs=[whole(a) for a in shapes],
        compiler_params=PARAMS,
        cost_estimate=pl.CostEstimate(
            flops=1_500_000_000, bytes_accessed=2_000_000, transcendentals=0
        ),
        name="finish",
    )(me, packed, keep, took, *pieces, *shares)


def body(
    query_rows,
    key_rows,
    value_rows,
    query_norm_gain,
    key_gain,
    break_offset,
    mixer_out_weight,
    routed_tokens,
    expert_gain,
    routes,
    route_scores,
    gate_weight,
    up_weight,
    down_weight,
):
    expert_count = lax.axis_size("ep")
    piece_count = expert_count if expert_count <= MOST_PERMUTES else 1
    levels = lax.axis_size("tp") // CORES
    token_count = routed_tokens.shape[0]
    capacity = max(2, token_count * TOP_K // expert_count)
    slot_count = expert_count * capacity

    level_index = lax.axis_index("tp") // CORES
    outer = (level_index == 0) | (level_index == levels - 1)
    core_index = lax.axis_index("tp") % CORES
    me = jnp.stack([lax.axis_index("ep"), outer, core_index, level_index]).astype(jnp.int32)
    packed, pieces = prepare(
        me,
        routed_tokens,
        expert_gain,
        routes,
        route_scores,
        key_rows,
        value_rows,
        expert_count,
        piece_count,
        capacity,
    )
    blocks = gather_z(packed, levels)
    own = (gate_weight[0].T, up_weight[0].T, down_weight[0])
    weights = [tuple(over_core(w, step) for w in own) for step in range(1, CORES)]
    own = tuple(pltpu.with_memory_space_constraint(w, pltpu.VMEM) for w in own)
    weights = [own] + weights
    arrived = [over_ep(pieces)]
    if piece_count == 1:
        both = jnp.concatenate([key_rows, value_rows], axis=1)
        others, slots = [lax.all_gather(both, "ep", axis=0, tiled=True)], None
    else:
        others, slots = arrived[0][1:], capacity
    keep, give = attention(
        me,
        others,
        slots,
        query_rows,
        key_rows,
        value_rows,
        query_norm_gain,
        key_gain,
        break_offset,
        mixer_out_weight,
    )
    took = over_core(give, 1)

    columns = [None]
    for level in range(1, levels):
        column, picked = select(
            me, blocks[level - 1], piece_count, slot_count, capacity
        )
        columns.append(column)
        arrived.append(over_ep(picked))

    piece_rows = slot_count // piece_count

    def layer(level, **options):
        return expert_layer(arrived[level], piece_rows, weights, **options)

    def share_of(level):
        returned = over_ep(layer(level), back=True)
        return combine(me, columns[level], returned, capacity, level, levels, keep, took)

    if levels == RELAYED:
        beside = over_z(layer(1, joined=True)[0], [(0, 1), (1, 0), (2, 3), (3, 2)])
        share = share_of(2)
        inner = over_z(share, [(1, 2), (2, 1)])
        distant = over_z(share, [(0, 2), (3, 1)])
        share = share_of(3)
        nearer = over_z(share, [(0, 1), (3, 2)])
        share = merge(share, nearer, inner, token_count, keep.shape[1])
        last = over_z(share, [(1, 3), (2, 0)])
        results = layer(0, addend=beside)
        expert_shares = [inner, distant, last]
        mixer_shares = [(inner, 0), (distant, 0), (nearer, 1), (last, 0)]
    else:
        expert_shares = []
        for level in range(1, levels):
            pairs = [(partner(i, level, levels), i) for i in range(levels)]
            expert_shares.append(over_z(share_of(level), pairs))
        results = layer(0)
        mixer_shares = [(share, 0) for share in expert_shares]
    returned = over_ep(results, back=True)
    expert_output, mixer_output = finish(
        me, packed, returned, capacity, expert_shares, mixer_shares, keep, took
    )
    return (mixer_output, expert_output)


def solution(mesh):
    in_specs = (
        P("ep", "tp"),
        P("ep", "tp"),
        P("ep", "tp"),
        P(),
        P(),
        P("tp"),
        P("tp", None),
        P(("ep", "tp"), None),
        P(),
        P(("ep", "tp"), None),
        P(("ep", "tp"), None),
        P("ep", None, "tp"),
        P("ep", None, "tp"),
        P("ep", "tp", None),
    )
    out_specs = (P(("ep", "tp"), None), P(("ep", "tp"), None))
    return jax.shard_map(
        body,
        mesh=mesh,
        in_specs=in_specs,
        out_specs=out_specs,
        check_vma=False,
    )
```

time: 264 us -> 180 us (0.68)
  waiting for transfers between devices: 151 us -> 102 us
  Pallas kernels: 0 us -> 31.6 us
  matrix products: 26.4 us -> 0 us
  other arithmetic: 22.8 us -> 0.08 us
  starting transfers between devices: 24.8 us -> 45.9 us
  blocking collectives: 19.2 us -> 0 us
  between operations: 14 us -> 0.97 us
  local copies, waits for them, and re-layouts: 4.56 us -> 0.04 us
    ppermute x6 -> x35, waiting for transfers between devices: 0.02 us -> 102 us  [the longest x10 57.9 us: over_z(): return lax.ppermute(array, 'tp', pairs)]
    all_gather x1 -> x0, waiting for transfers between devices: 81.9 us -> none  [body(): piece = lax.all_gather(arrived, 'tp', axis=0, tiled=True)]
    reduce_scatter x2 -> x0, waiting for transfers between devices: 57.4 us -> none  [the longest x1 41.8 us: body(): lax.psum_scatter(jnp.dot(hidden, down_local, preferred_element_type=jnp.f...]
    pallas_call x0 -> x13, Pallas kernels: none -> 31.6 us  [the longest x4 17.1 us: expert_layer(): pl.pallas_call(kernel, out_shape=shapes, in_specs=[VECTOR] * (count + len...]
    dot_general x14 -> x0, matrix products: 26.4 us -> none  [the longest x1 7.17 us: body(): gate_piece = jnp.dot(piece, gate_local, preferred_element_type=jnp.float32)]
    ppermute x6 -> x35, starting transfers between devices: 20.8 us -> 45.9 us  [the longest x21 27.9 us: over_ep(): moved.append(lax.ppermute(pieces[step], 'ep', pairs))]
    all_to_all x1 -> x0, blocking collectives: 19.2 us -> none  [body(): lax.all_to_all(outgoing, 'ep', split_axis=0, concat_axis=0, tiled=True)]
    another operation x6 -> x1, other arithmetic: 19 us -> 0.08 us  [body(): jnp.stack([lax.axis_index('ep'), outer, core_index, level_index])]
  transfers between devices with their start and end apart: 10 -> 35, of which waited for: 4 -> 17; matrix products, arithmetic and copies ran while one was open for 10% -> 0% of each run, Pallas kernels for 0% -> 15%
where the time goes in v1:
time: 180 us
  waiting for transfers between devices  102 us (57%)
  starting transfers between devices  45.9 us (26%)
  Pallas kernels  31.6 us (18%)
    ppermute x10, waiting for transfers between devices, over_z(): return lax.ppermute(array, 'tp', pairs)  57.9 us
    ppermute x21, waiting for transfers between devices, over_ep(): moved.append(lax.ppermute(pieces[step], 'ep', pairs))  43.7 us
    ppermute x21, starting transfers between devices, over_ep(): moved.append(lax.ppermute(pieces[step], 'ep', pairs))  27.9 us
    ppermute x10, starting transfers between devices, over_z(): return lax.ppermute(array, 'tp', pairs)  17.9 us
    pallas_call x4, Pallas kernels, expert_layer(): pl.pallas_call(kernel, out_shape=shapes, in_specs=[VECTOR] * (count + len...  17.1 us
    pallas_call x1, Pallas kernels, attention(): pl.pallas_call(lambda *refs: attention_kernel(slots, *refs), out_shape=[j...  4.69 us
  transfers between devices with their start and end apart: 35, of which 17 were waited for; matrix products, arithmetic and copies ran while one was open for 0% of the time, Pallas kernels for 15%

profile of v1, /device:TPU:0, one launch (start us, length us, event | category | flops | bytes accessed | tf_op | source)
XLA Modules:
  0.0 180.2 jit_solution(17908650414339193288)
XLA Ops:
  0.7 2.6 %prepare.1 = (bf16[128,2176]{1,0:T(8,128)(2,1)S(1)}, bf16[64,2048]{1,0:T(8,128)(2,1)S(1)}, bf16[96,2048]{1,0:T(8,128)(2,1)S(1)}, bf16[96,2048]{1,0:T(8,128)(2,1)S(1)}, bf16[96,2048]{1,0:T(8,128)(2,1)S(1)}) custom-call(s32[4]{0:T(128)S(1)} %pad_add_fusion.refs_0_.me_ref, bf16[128,2048]{1,0:T(8,128)(2,1)} %refs_1_.2, f32[1,2048]{1,0:T(1,128)} %bitcast.33, ...), custom_call_target="tpu_custom_call" | custom-call | flops 2000000000 | bytes 3000000 | tf_op jit(solution)/shard_map/prepare/pallas_call | solution.py:283
  4.0 3.0 %collective-permute-start = (bf16[96,2048]{1,0:T(8,128)(2,1)S(1)}, bf16[96,2048]{1,0:T(8,128)(2,1)S(1)}, u32[]{:S(2)}, u32[]{:S(2)}) collective-permute-start(bf16[96,2048]{1,0:T(8,128)(2,1)S(1)} %get-tuple-element.38), channel_id=1, source_target_pairs={{0,8},{8,0},{16,24},{24,16},{1,9},{9,1},{17,25},{25,17},{2,10},{10... | collective-permute-start | bytes 1179656 | tf_op jit(solution)/shard_map/ppermute | solution.py:40
  8.6 4.4 %collective-permute-start.4 = (bf16[128,2176]{1,0:T(8,128)(2,1)S(1)}, bf16[128,2176]{1,0:T(8,128)(2,1)S(1)}, u32[]{:S(2)}, u32[]{:S(2)}) collective-permute-start(bf16[128,2176]{1,0:T(8,128)(2,1)S(1)} %get-tuple-element.37.columns_ref), channel_id=1, source_target_pairs={{0,2},{1,3},{2,0},{3,1},{4,6},{5,7},{6,4},{7,5},{8,10},{9,11},{10,... | collective-permute-start | bytes 1671176 | tf_op jit(solution)/shard_map/ppermute | solution.py:46
  13.0 3.2 %collective-permute-done.refs_8_.refs_1_ = bf16[96,2048]{1,0:T(8,128)(2,1)S(1)} collective-permute-done((bf16[96,2048]{1,0:T(8,128)(2,1)S(1)}, bf16[96,2048]{1,0:T(8,128)(2,1)S(1)}, u32[]{:S(2)}, u32[]{:S(2)}) %collective-permute-start) | collective-permute-done | bytes 393248 | tf_op jit(solution)/shard_map/ppermute | solution.py:40
  19.0 6.1 %collective-permute-done.4.refs_0_ = bf16[128,2176]{1,0:T(8,128)(2,1)S(1)} collective-permute-done((bf16[128,2176]{1,0:T(8,128)(2,1)S(1)}, bf16[128,2176]{1,0:T(8,128)(2,1)S(1)}, u32[]{:S(2)}, u32[]{:S(2)}) %collective-permute-start.4) | collective-permute-done | bytes 557088 | tf_op jit(solution)/shard_map/ppermute | solution.py:46
  25.8 10.9 %collective-permute-done.16.refs_0_ = bf16[128,2176]{1,0:T(8,128)(2,1)S(1)} collective-permute-done((bf16[128,2176]{1,0:T(8,128)(2,1)S(1)}, bf16[128,2176]{1,0:T(8,128)(2,1)S(1)}, u32[]{:S(2)}, u32[]{:S(2)}) %collective-permute-start.16) | collective-permute-done | bytes 557088 | tf_op jit(solution)/shard_map/ppermute | solution.py:46
  39.3 8.8 %collective-permute-done.2.refs_10_.refs_3_ = bf16[96,2048]{1,0:T(8,128)(2,1)S(1)} collective-permute-done((bf16[96,2048]{1,0:T(8,128)(2,1)S(1)}, bf16[96,2048]{1,0:T(8,128)(2,1)S(1)}, u32[]{:S(2)}, u32[]{:S(2)}) %collective-permute-start.2) | collective-permute-done | bytes 393248 | tf_op jit(solution)/shard_map/ppermute | solution.py:40
  49.5 4.7 %attention.1 = (bf16[4,16,2048]{2,1,0:T(8,128)(2,1)S(1)}, bf16[4,16,2048]{2,1,0:T(8,128)(2,1)S(1)}) custom-call(s32[4]{0:T(128)S(1)} %pad_add_fusion.refs_0_.me_ref, f32[4]{0:T(128)S(1)} %copy-done.7, bf16[128,256]{1,0:T(8,128)(2,1)S(1)} %copy-done.6, f32[1,64]{1,0:T(1,128)S(1)} %bitcast.31, f32[1,64]{1,0:T(1,128)S(1)} %bitcast.32, ...), custom_call_target="tpu_custom_call" | custom-call | flops 6000000000 | bytes 3000000 | tf_op jit(solution)/shard_map/attention/pallas_call | solution.py:177
  55.3 7.8 %collective-permute-done.26.refs_0_ = bf16[128,2176]{1,0:T(8,128)(2,1)S(1)} collective-permute-done((bf16[128,2176]{1,0:T(8,128)(2,1)S(1)}, bf16[128,2176]{1,0:T(8,128)(2,1)S(1)}, u32[]{:S(2)}, u32[]{:S(2)}) %collective-permute-start.26) | collective-permute-done | bytes 557088 | tf_op jit(solution)/shard_map/ppermute | solution.py:46
  66.9 3.4 %collective-permute-done.19.refs_3_ = bf16[64,2048]{1,0:T(8,128)(2,1)S(1)} collective-permute-done((bf16[64,2048]{1,0:T(8,128)(2,1)S(1)}, bf16[64,2048]{1,0:T(8,128)(2,1)S(1)}, u32[]{:S(2)}, u32[]{:S(2)}) %collective-permute-start.19) | collective-permute-done | bytes 262176 | tf_op jit(solution)/shard_map/ppermute | solution.py:40
  70.3 2.4 %collective-permute-start.5 = (bf16[64,2048]{1,0:T(8,128)(2,1)S(1)}, bf16[64,2048]{1,0:T(8,128)(2,1)S(1)}, u32[]{:S(2)}, u32[]{:S(2)}) collective-permute-start(bf16[64,2048]{1,0:T(8,128)(2,1)S(1)} %get-tuple-element.45), channel_id=1, source_target_pairs={{0,8},{8,0},{16,24},{24,16},{1,9},{9,1},{17,25},{25,17},{2,10},{10... | collective-permute-start | bytes 786440 | tf_op jit(solution)/shard_map/ppermute | solution.py:40
  72.9 3.4 %collective-permute-start.29 = (bf16[64,2048]{1,0:T(8,128)(2,1)S(1)}, bf16[64,2048]{1,0:T(8,128)(2,1)S(1)}, u32[]{:S(2)}, u32[]{:S(2)}) collective-permute-start(bf16[64,2048]{1,0:T(8,128)(2,1)S(1)} %get-tuple-element.65), channel_id=1, source_target_pairs={{0,24},{8,16},{16,8},{24,0},{1,25},{9,17},{17,9},{25,1},{2,26},{10... | collective-permute-start | bytes 786440 | tf_op jit(solution)/shard_map/ppermute | solution.py:40
  76.3 4.2 %expert_layer.6 = (bf16[64,2048]{1,0:T(8,128)(2,1)S(1)}, bf16[64,2048]{1,0:T(8,128)(2,1)S(1)}, bf16[64,2048]{1,0:T(8,128)(2,1)S(1)}, bf16[64,2048]{1,0:T(8,128)(2,1)S(1)}) custom-call(bf16[64,2048]{1,0:T(8,128)(2,1)S(1)} %get-tuple-element.53.refs_0_, bf16[64,2048]{1,0:T(8,128)(2,1)S(1)} %collective-permute-done.17.refs_1_, ...), custom_call_target="tpu_custom_call" | custom-call | flops 2818572288 | bytes 11010048 | tf_op jit(solution)/shard_map/expert_layer/pallas_call | solution.py:374
  80.5 5.1 %collective-permute-done.27.refs_1_ = bf16[64,2048]{1,0:T(8,128)(2,1)S(1)} collective-permute-done((bf16[64,2048]{1,0:T(8,128)(2,1)S(1)}, bf16[64,2048]{1,0:T(8,128)(2,1)S(1)}, u32[]{:S(2)}, u32[]{:S(2)}) %collective-permute-start.27) | collective-permute-done | bytes 262176 | tf_op jit(solution)/shard_map/ppermute | solution.py:40
  85.7 3.1 %collective-permute-start.7 = (bf16[64,2048]{1,0:T(8,128)(2,1)S(1)}, bf16[64,2048]{1,0:T(8,128)(2,1)S(1)}, u32[]{:S(2)}, u32[]{:S(2)}) collective-permute-start(bf16[64,2048]{1,0:T(8,128)(2,1)S(1)} %get-tuple-element.47), channel_id=1, source_target_pairs={{0,24},{8,16},{16,8},{24,0},{1,25},{9,17},{17,9},{25,1},{2,26},{10... | collective-permute-start | bytes 786440 | tf_op jit(solution)/shard_map/ppermute | solution.py:40
  88.7 2.1 %collective-permute-done.29.refs_3_ = bf16[64,2048]{1,0:T(8,128)(2,1)S(1)} collective-permute-done((bf16[64,2048]{1,0:T(8,128)(2,1)S(1)}, bf16[64,2048]{1,0:T(8,128)(2,1)S(1)}, u32[]{:S(2)}, u32[]{:S(2)}) %collective-permute-start.29) | collective-permute-done | bytes 262176 | tf_op jit(solution)/shard_map/ppermute | solution.py:40
  90.8 1.6 collective-permute-start.20
  92.5 4.2 %expert_layer.7 = (bf16[64,2048]{1,0:T(8,128)(2,1)S(1)}, bf16[64,2048]{1,0:T(8,128)(2,1)S(1)}, bf16[64,2048]{1,0:T(8,128)(2,1)S(1)}, bf16[64,2048]{1,0:T(8,128)(2,1)S(1)}) custom-call(bf16[64,2048]{1,0:T(8,128)(2,1)S(1)} %get-tuple-element.62.refs_0_, bf16[64,2048]{1,0:T(8,128)(2,1)S(1)} %collective-permute-done.27.refs_1_, ...), custom_call_target="tpu_custom_call" | custom-call | flops 2818572288 | bytes 11010048 | tf_op jit(solution)/shard_map/expert_layer/pallas_call | solution.py:374
  96.7 2.0 %collective-permute-start.21 = (bf16[64,2048]{1,0:T(8,128)(2,1)S(1)}, bf16[64,2048]{1,0:T(8,128)(2,1)S(1)}, u32[]{:S(2)}, u32[]{:S(2)}) collective-permute-start(bf16[64,2048]{1,0:T(8,128)(2,1)S(1)} %get-tuple-element.59), channel_id=1, source_target_pairs={{16,0},{24,8},{0,16},{8,24},{17,1},{25,9},{1,17},{9,25},{18,2},{26... | collective-permute-start | bytes 786440 | tf_op jit(solution)/shard_map/ppermute | solution.py:40
  98.7 3.4 %collective-permute-done.6.refs_2_ = bf16[64,2048]{1,0:T(8,128)(2,1)S(1)} collective-permute-done((bf16[64,2048]{1,0:T(8,128)(2,1)S(1)}, bf16[64,2048]{1,0:T(8,128)(2,1)S(1)}, u32[]{:S(2)}, u32[]{:S(2)}) %collective-permute-start.6) | collective-permute-done | bytes 262176 | tf_op jit(solution)/shard_map/ppermute | solution.py:40
  102.9 2.7 %collective-permute-start.32 = (bf16[64,2048]{1,0:T(8,128)(2,1)S(1)}, bf16[64,2048]{1,0:T(8,128)(2,1)S(1)}, u32[]{:S(2)}, u32[]{:S(2)}) collective-permute-start(bf16[64,2048]{1,0:T(8,128)(2,1)S(1)} %get-tuple-element.69), channel_id=1, source_target_pairs={{24,0},{16,8},{8,16},{0,24},{25,1},{17,9},{9,17},{1,25},{26,2},{18... | collective-permute-start | bytes 786440 | tf_op jit(solution)/shard_map/ppermute | solution.py:40
  105.6 4.2 %expert_layer.4 = bf16[256,2048]{1,0:T(8,128)(2,1)S(1)} custom-call(bf16[64,2048]{1,0:T(8,128)(2,1)S(1)} %get-tuple-element.44.refs_0_, bf16[64,2048]{1,0:T(8,128)(2,1)S(1)} %collective-permute-done.5.refs_1_, bf16[64,2048]{1,0:T(8,128)(2,1)S(1)} %collective-permute-done.6.refs_2_, bf16[64,2048]{1,0:T(8,128)(2,1)S(1)} %collective-permute-done.7.refs_3_, ...), custom_call_target="tpu_custom_call" | custom-call | flops 2818572288 | bytes 11010048 | tf_op jit(solution)/shard_map/expert_layer/pallas_call | solution.py:374
  109.8 3.5 %collective-permute-done.21.refs_2_ = bf16[64,2048]{1,0:T(8,128)(2,1)S(1)} collective-permute-done((bf16[64,2048]{1,0:T(8,128)(2,1)S(1)}, bf16[64,2048]{1,0:T(8,128)(2,1)S(1)}, u32[]{:S(2)}, u32[]{:S(2)}) %collective-permute-start.21) | collective-permute-done | bytes 262176 | tf_op jit(solution)/shard_map/ppermute | solution.py:40
  115.1 4.6 %collective-permute-done.31.refs_2_ = bf16[64,2048]{1,0:T(8,128)(2,1)S(1)} collective-permute-done((bf16[64,2048]{1,0:T(8,128)(2,1)S(1)}, bf16[64,2048]{1,0:T(8,128)(2,1)S(1)}, u32[]{:S(2)}, u32[]{:S(2)}) %collective-permute-start.31) | collective-permute-done | bytes 262176 | tf_op jit(solution)/shard_map/ppermute | solution.py:40
  122.3 6.0 %collective-permute-start.24 = (bf16[160,2048]{1,0:T(8,128)(2,1)S(1)}, bf16[160,2048]{1,0:T(8,128)(2,1)S(1)}, u32[]{:S(2)}, u32[]{:S(2)}) collective-permute-start(bf16[160,2048]{1,0:T(8,128)(2,1)S(1)} %combine.2), channel_id=1, source_target_pairs={{0,4},{1,5},{6,2},{7,3},{8,12},{9,13},{14,10},{15,11},{16,20},{17,... | collective-permute-start | bytes 1966088 | tf_op jit(solution)/shard_map/ppermute | solution.py:46
  128.3 19.0 %collective-permute-done.33.beside_ref.refs_7_ = bf16[160,2048]{1,0:T(8,128)(2,1)S(1)} collective-permute-done((bf16[160,2048]{1,0:T(8,128)(2,1)S(1)}, bf16[160,2048]{1,0:T(8,128)(2,1)S(1)}, u32[]{:S(2)}, u32[]{:S(2)}) %collective-permute-start.33) | collective-permute-done | bytes 655392 | tf_op jit(solution)/shard_map/ppermute | solution.py:46
  148.7 4.5 %expert_layer.5 = (bf16[64,2048]{1,0:T(8,128)(2,1)S(1)}, bf16[64,2048]{1,0:T(8,128)(2,1)S(1)}, bf16[64,2048]{1,0:T(8,128)(2,1)S(1)}, bf16[64,2048]{1,0:T(8,128)(2,1)S(1)}) custom-call(bf16[64,2048]{1,0:T(8,128)(2,1)S(1)} %get-tuple-element.43.refs_0_, bf16[96,2048]{1,0:T(8,128)(2,1)S(1)} %collective-permute-done.refs_8_.refs_1_, ...), custom_call_target="tpu_custom_call" | custom-call | flops 2818572288 | bytes 11010048 | tf_op jit(solution)/shard_map/expert_layer/pallas_call | solution.py:374
  153.2 1.9 %collective-permute-start.12 = (bf16[64,2048]{1,0:T(8,128)(2,1)S(1)}, bf16[64,2048]{1,0:T(8,128)(2,1)S(1)}, u32[]{:S(2)}, u32[]{:S(2)}) collective-permute-start(bf16[64,2048]{1,0:T(8,128)(2,1)S(1)} %get-tuple-element.49), channel_id=1, source_target_pairs={{8,0},{0,8},{24,16},{16,24},{9,1},{1,9},{25,17},{17,25},{10,2},{2,... | collective-permute-start | bytes 786440 | tf_op jit(solution)/shard_map/ppermute | solution.py:40
  156.8 2.9 %collective-permute-done.12.refs_1_ = bf16[64,2048]{1,0:T(8,128)(2,1)S(1)} collective-permute-done((bf16[64,2048]{1,0:T(8,128)(2,1)S(1)}, bf16[64,2048]{1,0:T(8,128)(2,1)S(1)}, u32[]{:S(2)}, u32[]{:S(2)}) %collective-permute-start.12) | collective-permute-done | bytes 262176 | tf_op jit(solution)/shard_map/ppermute | solution.py:40
  159.7 4.6 %collective-permute-done.13.refs_2_ = bf16[64,2048]{1,0:T(8,128)(2,1)S(1)} collective-permute-done((bf16[64,2048]{1,0:T(8,128)(2,1)S(1)}, bf16[64,2048]{1,0:T(8,128)(2,1)S(1)}, u32[]{:S(2)}, u32[]{:S(2)}) %collective-permute-start.13) | collective-permute-done | bytes 262176 | tf_op jit(solution)/shard_map/ppermute | solution.py:40
  164.3 14.0 %collective-permute-done.34.refs_6_ = bf16[144,2048]{1,0:T(8,128)(2,1)S(1)} collective-permute-done((bf16[144,2048]{1,0:T(8,128)(2,1)S(1)}, bf16[144,2048]{1,0:T(8,128)(2,1)S(1)}, u32[]{:S(2)}, u32[]{:S(2)}) %collective-permute-start.34) | collective-permute-done | bytes 589856 | tf_op jit(solution)/shard_map/ppermute | solution.py:46
  178.3 1.9 %finish.1 = (bf16[128,2048]{1,0:T(8,128)(2,1)}, bf16[16,2048]{1,0:T(8,128)(2,1)}) custom-call(s32[4]{0:T(128)S(1)} %pad_add_fusion.refs_0_.me_ref, bf16[128,2176]{1,0:T(8,128)(2,1)S(1)} %get-tuple-element.37.columns_ref, bf16[4,16,2048]{2,1,0:T(8,128)(2,1)S(1)} %get-tuple-element.41.keep_ref, bf16[4,16,2048]{2,1,0:T(8,128)(2,1)S(1)} %collective-permute-done.3.took_ref, ...), custom_call_target="tpu_custom_call" | custom-call | flops 1500000000 | bytes 2000000 | tf_op jit(solution)/shard_map/finish/pallas_call | solution.py:483
  (72 shorter events, 23.0 us)
Async XLA Ops:
  3.3 14.3 %collective-permute-start.15 = (bf16[128,2176]{1,0:T(8,128)(2,1)S(1)}, bf16[128,2176]{1,0:T(8,128)(2,1)S(1)}, u32[]{:S(2)}, u32[]{:S(2)}) collective-permute-start(bf16[128,2176]{1,0:T(8,128)(2,1)S(1)} %get-tuple-element.37.columns_ref), channel_id=1, source_target_pairs={{2,4},{3,5},{4,2},{5,3},{10,12},{11,13},{12,10},{13,11},{18,20},{1... | collective-permute-start | bytes 1671176 | tf_op jit(solution)/shard_map/ppermute | solution.py:46
  4.0 12.2 %collective-permute-start = (bf16[96,2048]{1,0:T(8,128)(2,1)S(1)}, bf16[96,2048]{1,0:T(8,128)(2,1)S(1)}, u32[]{:S(2)}, u32[]{:S(2)}) collective-permute-start(bf16[96,2048]{1,0:T(8,128)(2,1)S(1)} %get-tuple-element.38), channel_id=1, source_target_pairs={{0,8},{8,0},{16,24},{24,16},{1,9},{9,1},{17,25},{25,17},{2,10},{10... | collective-permute-start | bytes 1179656 | tf_op jit(solution)/shard_map/ppermute | solution.py:40
  7.1 10.6 %collective-permute-start.1 = (bf16[96,2048]{1,0:T(8,128)(2,1)S(1)}, bf16[96,2048]{1,0:T(8,128)(2,1)S(1)}, u32[]{:S(2)}, u32[]{:S(2)}) collective-permute-start(bf16[96,2048]{1,0:T(8,128)(2,1)S(1)} %get-tuple-element.39), channel_id=1, source_target_pairs={{0,16},{8,24},{16,0},{24,8},{1,17},{9,25},{17,1},{25,9},{2,18},{10... | collective-permute-start | bytes 1179656 | tf_op jit(solution)/shard_map/ppermute | solution.py:40
  8.6 16.5 %collective-permute-start.4 = (bf16[128,2176]{1,0:T(8,128)(2,1)S(1)}, bf16[128,2176]{1,0:T(8,128)(2,1)S(1)}, u32[]{:S(2)}, u32[]{:S(2)}) collective-permute-start(bf16[128,2176]{1,0:T(8,128)(2,1)S(1)} %get-tuple-element.37.columns_ref), channel_id=1, source_target_pairs={{0,2},{1,3},{2,0},{3,1},{4,6},{5,7},{6,4},{7,5},{8,10},{9,11},{10,... | collective-permute-start | bytes 1671176 | tf_op jit(solution)/shard_map/ppermute | solution.py:46
  13.0 59.8 %collective-permute-start.8 = (bf16[448,2048]{1,0:T(8,128)(2,1)S(1)}, bf16[448,2048]{1,0:T(8,128)(2,1)S(1)}, u32[]{:S(2)}, u32[]{:S(2)}) collective-permute-start(bf16[448,2048]{1,0:T(8,128)(2,1)S(1)} %bitcast.16), channel_id=1, source_target_pairs={{0,1},{1,0},{2,3},{3,2},{4,5},{5,4},{6,7},{7,6},{8,9},{9,8},{10,11... | collective-permute-start | bytes 5505032 | tf_op jit(solution)/shard_map/ppermute | solution.py:77
  16.2 56.6 %collective-permute-start.9 = (bf16[448,2048]{1,0:T(8,128)(2,1)S(1)}, bf16[448,2048]{1,0:T(8,128)(2,1)S(1)}, u32[]{:S(2)}, u32[]{:S(2)}) collective-permute-start(bf16[448,2048]{1,0:T(8,128)(2,1)S(1)} %bitcast.21), channel_id=1, source_target_pairs={{0,1},{1,0},{2,3},{3,2},{4,5},{5,4},{6,7},{7,6},{8,9},{9,8},{10,11... | collective-permute-start | bytes 5505032 | tf_op jit(solution)/shard_map/ppermute | solution.py:77
  17.6 55.2 %collective-permute-start.10 = (bf16[448,2048]{1,0:T(8,128)(2,1)S(1)}, bf16[448,2048]{1,0:T(8,128)(2,1)S(1)}, u32[]{:S(2)}, u32[]{:S(2)}) collective-permute-start(bf16[448,2048]{1,0:T(8,128)(2,1)S(1)} %bitcast.26), channel_id=1, source_target_pairs={{0,1},{1,0},{2,3},{3,2},{4,5},{5,4},{6,7},{7,6},{8,9},{9,8},{10,11... | collective-permute-start | bytes 5505032 | tf_op jit(solution)/shard_map/ppermute | solution.py:77
  17.7 19.0 %collective-permute-start.16 = (bf16[128,2176]{1,0:T(8,128)(2,1)S(1)}, bf16[128,2176]{1,0:T(8,128)(2,1)S(1)}, u32[]{:S(2)}, u32[]{:S(2)}) collective-permute-start(bf16[128,2176]{1,0:T(8,128)(2,1)S(1)} %collective-permute-done.15.refs_1_), channel_id=1, source_target_pairs={{2,0},{3,1},{4,6},{5,7},{10,8},{11,9},{12,14},{13,15},{18,16},{19,... | collective-permute-start | bytes 1671176 | tf_op jit(solution)/shard_map/ppermute | solution.py:46
  25.1 23.0 %collective-permute-start.25 = (bf16[128,2176]{1,0:T(8,128)(2,1)S(1)}, bf16[128,2176]{1,0:T(8,128)(2,1)S(1)}, u32[]{:S(2)}, u32[]{:S(2)}) collective-permute-start(bf16[128,2176]{1,0:T(8,128)(2,1)S(1)} %collective-permute-done.4.refs_0_), channel_id=1, source_target_pairs={{2,4},{3,5},{4,2},{5,3},{10,12},{11,13},{12,10},{13,11},{18,20},{1... | collective-permute-start | bytes 1671176 | tf_op jit(solution)/shard_map/ppermute | solution.py:46
  36.7 11.4 %collective-permute-start.2 = (bf16[96,2048]{1,0:T(8,128)(2,1)S(1)}, bf16[96,2048]{1,0:T(8,128)(2,1)S(1)}, u32[]{:S(2)}, u32[]{:S(2)}) collective-permute-start(bf16[96,2048]{1,0:T(8,128)(2,1)S(1)} %get-tuple-element.40), channel_id=1, source_target_pairs={{0,24},{8,16},{16,8},{24,0},{1,25},{9,17},{17,9},{25,1},{2,26},{10... | collective-permute-start | bytes 1179656 | tf_op jit(solution)/shard_map/ppermute | solution.py:40
  48.1 15.0 %collective-permute-start.26 = (bf16[128,2176]{1,0:T(8,128)(2,1)S(1)}, bf16[128,2176]{1,0:T(8,128)(2,1)S(1)}, u32[]{:S(2)}, u32[]{:S(2)}) collective-permute-start(bf16[128,2176]{1,0:T(8,128)(2,1)S(1)} %collective-permute-done.25.refs_1_), channel_id=1, source_target_pairs={{2,0},{3,1},{4,6},{5,7},{10,8},{11,9},{12,14},{13,15},{18,16},{19,... | collective-permute-start | bytes 1671176 | tf_op jit(solution)/shard_map/ppermute | solution.py:46
  54.9 12.0 %collective-permute-start.18 = (bf16[64,2048]{1,0:T(8,128)(2,1)S(1)}, bf16[64,2048]{1,0:T(8,128)(2,1)S(1)}, u32[]{:S(2)}, u32[]{:S(2)}) collective-permute-start(bf16[64,2048]{1,0:T(8,128)(2,1)S(1)} %get-tuple-element.55), channel_id=1, source_target_pairs={{0,16},{8,24},{16,0},{24,8},{1,17},{9,25},{17,1},{25,9},{2,18},{10... | collective-permute-start | bytes 786440 | tf_op jit(solution)/shard_map/ppermute | solution.py:40
  66.9 29.8 %collective-permute-start.3 = (bf16[4,16,2048]{2,1,0:T(8,128)(2,1)S(1)}, bf16[4,16,2048]{2,1,0:T(8,128)(2,1)S(1)}, u32[]{:S(2)}, u32[]{:S(2)}) collective-permute-start(bf16[4,16,2048]{2,1,0:T(8,128)(2,1)S(1)} %get-tuple-element.42), channel_id=1, source_target_pairs={{0,1},{1,0},{2,3},{3,2},{4,5},{5,4},{6,7},{7,6},{8,9},{9,8},{10,11... | collective-permute-start | bytes 786440 | tf_op jit(solution)/shard_map/ppermute | solution.py:77
  70.3 28.4 %collective-permute-start.5 = (bf16[64,2048]{1,0:T(8,128)(2,1)S(1)}, bf16[64,2048]{1,0:T(8,128)(2,1)S(1)}, u32[]{:S(2)}, u32[]{:S(2)}) collective-permute-start(bf16[64,2048]{1,0:T(8,128)(2,1)S(1)} %get-tuple-element.45), channel_id=1, source_target_pairs={{0,8},{8,0},{16,24},{24,16},{1,9},{9,1},{17,25},{25,17},{2,10},{10... | collective-permute-start | bytes 786440 | tf_op jit(solution)/shard_map/ppermute | solution.py:40
  72.8 12.8 %collective-permute-start.27 = (bf16[64,2048]{1,0:T(8,128)(2,1)S(1)}, bf16[64,2048]{1,0:T(8,128)(2,1)S(1)}, u32[]{:S(2)}, u32[]{:S(2)}) collective-permute-start(bf16[64,2048]{1,0:T(8,128)(2,1)S(1)} %get-tuple-element.63), channel_id=1, source_target_pairs={{0,8},{8,0},{16,24},{24,16},{1,9},{9,1},{17,25},{25,17},{2,10},{10... | collective-permute-start | bytes 786440 | tf_op jit(solution)/shard_map/ppermute | solution.py:40
  72.8 12.9 %collective-permute-start.28 = (bf16[64,2048]{1,0:T(8,128)(2,1)S(1)}, bf16[64,2048]{1,0:T(8,128)(2,1)S(1)}, u32[]{:S(2)}, u32[]{:S(2)}) collective-permute-start(bf16[64,2048]{1,0:T(8,128)(2,1)S(1)} %get-tuple-element.64), channel_id=1, source_target_pairs={{0,16},{8,24},{16,0},{24,8},{1,17},{9,25},{17,1},{25,9},{2,18},{10... | collective-permute-start | bytes 786440 | tf_op jit(solution)/shard_map/ppermute | solution.py:40
  72.9 17.9 %collective-permute-start.29 = (bf16[64,2048]{1,0:T(8,128)(2,1)S(1)}, bf16[64,2048]{1,0:T(8,128)(2,1)S(1)}, u32[]{:S(2)}, u32[]{:S(2)}) collective-permute-start(bf16[64,2048]{1,0:T(8,128)(2,1)S(1)} %get-tuple-element.65), channel_id=1, source_target_pairs={{0,24},{8,16},{16,8},{24,0},{1,25},{9,17},{17,9},{25,1},{2,26},{10... | collective-permute-start | bytes 786440 | tf_op jit(solution)/shard_map/ppermute | solution.py:40
  85.5 16.5 %collective-permute-start.6 = (bf16[64,2048]{1,0:T(8,128)(2,1)S(1)}, bf16[64,2048]{1,0:T(8,128)(2,1)S(1)}, u32[]{:S(2)}, u32[]{:S(2)}) collective-permute-start(bf16[64,2048]{1,0:T(8,128)(2,1)S(1)} %get-tuple-element.46), channel_id=1, source_target_pairs={{0,16},{8,24},{16,0},{24,8},{1,17},{9,25},{17,1},{25,9},{2,18},{10... | collective-permute-start | bytes 786440 | tf_op jit(solution)/shard_map/ppermute | solution.py:40
  85.7 17.2 %collective-permute-start.7 = (bf16[64,2048]{1,0:T(8,128)(2,1)S(1)}, bf16[64,2048]{1,0:T(8,128)(2,1)S(1)}, u32[]{:S(2)}, u32[]{:S(2)}) collective-permute-start(bf16[64,2048]{1,0:T(8,128)(2,1)S(1)} %get-tuple-element.47), channel_id=1, source_target_pairs={{0,24},{8,16},{16,8},{24,0},{1,25},{9,17},{17,9},{25,1},{2,26},{10... | collective-permute-start | bytes 786440 | tf_op jit(solution)/shard_map/ppermute | solution.py:40
  90.8 12.1 %collective-permute-start.20 = (bf16[64,2048]{1,0:T(8,128)(2,1)S(1)}, bf16[64,2048]{1,0:T(8,128)(2,1)S(1)}, u32[]{:S(2)}, u32[]{:S(2)}) collective-permute-start(bf16[64,2048]{1,0:T(8,128)(2,1)S(1)} %get-tuple-element.58), channel_id=1, source_target_pairs={{8,0},{0,8},{24,16},{16,24},{9,1},{1,9},{25,17},{17,25},{10,2},{2,... | collective-permute-start | bytes 786440 | tf_op jit(solution)/shard_map/ppermute | solution.py:40
  96.7 16.7 %collective-permute-start.21 = (bf16[64,2048]{1,0:T(8,128)(2,1)S(1)}, bf16[64,2048]{1,0:T(8,128)(2,1)S(1)}, u32[]{:S(2)}, u32[]{:S(2)}) collective-permute-start(bf16[64,2048]{1,0:T(8,128)(2,1)S(1)} %get-tuple-element.59), channel_id=1, source_target_pairs={{16,0},{24,8},{0,16},{8,24},{17,1},{25,9},{1,17},{9,25},{18,2},{26... | collective-permute-start | bytes 786440 | tf_op jit(solution)/shard_map/ppermute | solution.py:40
  98.7 14.6 %collective-permute-start.22 = (bf16[64,2048]{1,0:T(8,128)(2,1)S(1)}, bf16[64,2048]{1,0:T(8,128)(2,1)S(1)}, u32[]{:S(2)}, u32[]{:S(2)}) collective-permute-start(bf16[64,2048]{1,0:T(8,128)(2,1)S(1)} %get-tuple-element.60), channel_id=1, source_target_pairs={{24,0},{16,8},{8,16},{0,24},{25,1},{17,9},{9,17},{1,25},{26,2},{18... | collective-permute-start | bytes 786440 | tf_op jit(solution)/shard_map/ppermute | solution.py:40
  102.1 13.0 %collective-permute-start.30 = (bf16[64,2048]{1,0:T(8,128)(2,1)S(1)}, bf16[64,2048]{1,0:T(8,128)(2,1)S(1)}, u32[]{:S(2)}, u32[]{:S(2)}) collective-permute-start(bf16[64,2048]{1,0:T(8,128)(2,1)S(1)} %get-tuple-element.67), channel_id=1, source_target_pairs={{8,0},{0,8},{24,16},{16,24},{9,1},{1,9},{25,17},{17,25},{10,2},{2,... | collective-permute-start | bytes 786440 | tf_op jit(solution)/shard_map/ppermute | solution.py:40
  102.9 16.8 %collective-permute-start.31 = (bf16[64,2048]{1,0:T(8,128)(2,1)S(1)}, bf16[64,2048]{1,0:T(8,128)(2,1)S(1)}, u32[]{:S(2)}, u32[]{:S(2)}) collective-permute-start(bf16[64,2048]{1,0:T(8,128)(2,1)S(1)} %get-tuple-element.68), channel_id=1, source_target_pairs={{16,0},{24,8},{0,16},{8,24},{17,1},{25,9},{1,17},{9,25},{18,2},{26... | collective-permute-start | bytes 786440 | tf_op jit(solution)/shard_map/ppermute | solution.py:40
  102.9 16.8 %collective-permute-start.32 = (bf16[64,2048]{1,0:T(8,128)(2,1)S(1)}, bf16[64,2048]{1,0:T(8,128)(2,1)S(1)}, u32[]{:S(2)}, u32[]{:S(2)}) collective-permute-start(bf16[64,2048]{1,0:T(8,128)(2,1)S(1)} %get-tuple-element.69), channel_id=1, source_target_pairs={{24,0},{16,8},{8,16},{0,24},{25,1},{17,9},{9,17},{1,25},{26,2},{18... | collective-permute-start | bytes 786440 | tf_op jit(solution)/shard_map/ppermute | solution.py:40
  113.3 35.4 %collective-permute-start.11 = (bf16[256,2048]{1,0:T(8,128)(2,1)S(1)}, bf16[256,2048]{1,0:T(8,128)(2,1)S(1)}, u32[]{:S(2)}, u32[]{:S(2)}) collective-permute-start(bf16[256,2048]{1,0:T(8,128)(2,1)S(1)} %expert_layer.4), channel_id=1, source_target_pairs={{0,2},{1,3},{2,0},{3,1},{4,6},{5,7},{6,4},{7,5},{8,10},{9,11},{10,... | collective-permute-start | bytes 3145736 | tf_op jit(solution)/shard_map/ppermute | solution.py:46
  114.3 13.9 %collective-permute-start.23 = (bf16[160,2048]{1,0:T(8,128)(2,1)S(1)}, bf16[160,2048]{1,0:T(8,128)(2,1)S(1)}, u32[]{:S(2)}, u32[]{:S(2)}) collective-permute-start(bf16[160,2048]{1,0:T(8,128)(2,1)S(1)} %combine.2), channel_id=1, source_target_pairs={{2,4},{3,5},{4,2},{5,3},{10,12},{11,13},{12,10},{13,11},{18,20},{1... | collective-permute-start | bytes 1966088 | tf_op jit(solution)/shard_map/ppermute | solution.py:46
  120.6 26.6 %collective-permute-start.33 = (bf16[160,2048]{1,0:T(8,128)(2,1)S(1)}, bf16[160,2048]{1,0:T(8,128)(2,1)S(1)}, u32[]{:S(2)}, u32[]{:S(2)}) collective-permute-start(bf16[160,2048]{1,0:T(8,128)(2,1)S(1)} %combine.3.share_ref), channel_id=1, source_target_pairs={{0,2},{1,3},{6,4},{7,5},{8,10},{9,11},{14,12},{15,13},{16,18},{17,... | collective-permute-start | bytes 1966088 | tf_op jit(solution)/shard_map/ppermute | solution.py:46
  122.3 34.5 %collective-permute-start.24 = (bf16[160,2048]{1,0:T(8,128)(2,1)S(1)}, bf16[160,2048]{1,0:T(8,128)(2,1)S(1)}, u32[]{:S(2)}, u32[]{:S(2)}) collective-permute-start(bf16[160,2048]{1,0:T(8,128)(2,1)S(1)} %combine.2), channel_id=1, source_target_pairs={{0,4},{1,5},{6,2},{7,3},{8,12},{9,13},{14,10},{15,11},{16,20},{17,... | collective-permute-start | bytes 1966088 | tf_op jit(solution)/shard_map/ppermute | solution.py:46
  147.4 30.9 %collective-permute-start.34 = (bf16[144,2048]{1,0:T(8,128)(2,1)S(1)}, bf16[144,2048]{1,0:T(8,128)(2,1)S(1)}, u32[]{:S(2)}, u32[]{:S(2)}) collective-permute-start(bf16[144,2048]{1,0:T(8,128)(2,1)S(1)} %merge.1), channel_id=1, source_target_pairs={{2,6},{3,7},{4,0},{5,1},{10,14},{11,15},{12,8},{13,9},{18,22},{19,... | collective-permute-start | bytes 1769480 | tf_op jit(solution)/shard_map/ppermute | solution.py:46
  155.1 9.2 %collective-permute-start.13 = (bf16[64,2048]{1,0:T(8,128)(2,1)S(1)}, bf16[64,2048]{1,0:T(8,128)(2,1)S(1)}, u32[]{:S(2)}, u32[]{:S(2)}) collective-permute-start(bf16[64,2048]{1,0:T(8,128)(2,1)S(1)} %get-tuple-element.50), channel_id=1, source_target_pairs={{16,0},{24,8},{0,16},{8,24},{17,1},{25,9},{1,17},{9,25},{18,2},{26... | collective-permute-start | bytes 786440 | tf_op jit(solution)/shard_map/ppermute | solution.py:40
  155.6 8.7 %collective-permute-start.14 = (bf16[64,2048]{1,0:T(8,128)(2,1)S(1)}, bf16[64,2048]{1,0:T(8,128)(2,1)S(1)}, u32[]{:S(2)}, u32[]{:S(2)}) collective-permute-start(bf16[64,2048]{1,0:T(8,128)(2,1)S(1)} %get-tuple-element.51), channel_id=1, source_target_pairs={{24,0},{16,8},{8,16},{0,24},{25,1},{17,9},{9,17},{1,25},{26,2},{18... | collective-permute-start | bytes 786440 | tf_op jit(solution)/shard_map/ppermute | solution.py:40
  (13 other events, 154.3 us)

commit v2 on v1

--- a/solution.py
+++ b/solution.py
@@ -47,6 +47,7 @@
 
 
 RELAYED = 4
+PARTS = 2
 
 
 def gather_z(packed, levels):
@@ -61,14 +62,6 @@
     second = over_z(across, [(1, 0), (2, 3)])
     third = over_z(beyond, [(1, 0), (2, 3)])
     return [[beside], [second, across], [third, beyond]]
-
-
-def target_level(index, outer, level, levels):
-    if levels != RELAYED:
-        if levels & (levels - 1) == 0:
-            return index ^ level
-        return (index - level + levels) % levels
-    return index ^ (3 - outer) if level == 2 else index ^ (2 + outer)
 
 
 def over_core(array, step):
@@ -325,59 +318,78 @@
     return columns, pieces
 
 
-def expert_layer(pieces, piece_rows, weights, joined=False, addend=None):
+def hold(arrays):
+    def kernel(*refs):
+        count = len(arrays)
+        copies = [
+            pltpu.make_async_copy(refs[i], refs[count + i], refs[-1].at[i]) for i in range(count)
+        ]
+        for copy in copies:
+            copy.start()
+        for copy in copies:
+            copy.wait()
+
+    return tuple(
+        pl.pallas_call(
+            kernel,
+            out_shape=[jax.ShapeDtypeStruct(a.shape, a.dtype) for a in arrays],
+            in_specs=[REMAIN] * len(arrays),
+            out_specs=[VECTOR] * len(arrays),
+            scratch_shapes=[pltpu.SemaphoreType.DMA((len(arrays),))],
+            compiler_params=PARAMS,
+            cost_estimate=pl.CostEstimate(
+                flops=500_000_000, bytes_accessed=6_000_000, transcendentals=0
+            ),
+            name="hold",
+        )(*arrays)
+    )
+
+
+def expert_layer(pieces, piece_rows, weights, joined=False, parts=1, terms=()):
     width = pieces[0].shape[1]
     count = len(pieces)
     row_count = count * piece_rows
     units = weights[0][0].shape[0]
     groups = len(weights)
-    addends = [] if addend is None else [addend]
-    far = [w for group in weights[1:] for w in group]
+    flat = [w for group in weights for w in group]
 
     def kernel(*refs):
         refs = list(refs)
         rows_refs = [refs.pop(0) for _ in pieces]
-        addend_refs = [refs.pop(0) for _ in addends]
-        own_refs = [refs.pop(0) for _ in range(3)]
-        far_refs = [refs.pop(0) for _ in far]
-        semaphores = refs.pop()
-        near_refs = refs[len(refs) - len(far) :]
-        out_refs = refs[: len(refs) - len(far)]
-        copies = [
-            pltpu.make_async_copy(source, target, semaphores.at[index])
-            for index, (source, target) in enumerate(zip(far_refs, near_refs))
-        ]
-        for copy in copies:
-            copy.start()
+        term_refs = [refs.pop(0) for _ in terms]
+        weight_refs = [refs.pop(0) for _ in flat]
+        out_refs = refs
         rows = jnp.concatenate([ref[:piece_rows] for ref in rows_refs], axis=0)
         total = jnp.zeros((row_count, width), jnp.float32)
-        for ref in addend_refs:
-            total = ref[...].astype(jnp.float32)
         for g in range(groups):
-            if g == 0:
-                gate_ref, up_ref, down_ref = own_refs
-            else:
-                gate_ref, up_ref, down_ref = near_refs[3 * g - 3 : 3 * g]
-                for copy in copies[3 * g - 3 : 3 * g]:
-                    copy.wait()
+            gate_ref, up_ref, down_ref = weight_refs[3 * g : 3 * g + 3]
             gate = dot(rows, gate_ref[...], ((1,), (1,)))
             up = dot(rows, up_ref[...], ((1,), (1,)))
             hidden = (gate / (1.0 + jnp.exp(-gate)) * up).astype(jnp.bfloat16)
             total = total + dot(hidden, down_ref[...])
         total = total.astype(jnp.bfloat16)
-        part = row_count // len(out_refs)
+        part = row_count // outputs
+        wide = width // parts
         for index, ref in enumerate(out_refs):
-            ref[...] = total[index * part : (index + 1) * part]
-
-    shapes = piece_shapes(1 if joined else count, row_count, width)
-    return list(
+            left = index // outputs * wide
+            top = index % outputs * part
+            ref[:part] = total[top : top + part, left : left + wide]
+        if terms:
+            me_ref, keep_ref, took_ref = term_refs
+            out_refs[0][row_count:] = owed(keep_ref, took_ref, me_ref[3] ^ 1)
+
+    outputs = 1 if joined else count
+    shapes = piece_shapes(outputs, row_count, width // parts) * parts
+    if terms:
+        shapes = piece_shapes(1, row_count + terms[1].shape[1], width)
+    results = list(
         pl.pallas_call(
             kernel,
             out_shape=shapes,
-            in_specs=[VECTOR] * (count + len(addends) + 3) + [REMAIN] * len(far),
+            in_specs=[VECTOR] * count
+            + [SCALAR, VECTOR, VECTOR][: len(terms)]
+            + [VECTOR] * len(flat),
             out_specs=[VECTOR] * len(shapes),
-            scratch_shapes=[pltpu.VMEM(w.shape, w.dtype) for w in far]
-            + [pltpu.SemaphoreType.DMA((len(far),))],
             compiler_params=PARAMS,
             cost_estimate=pl.CostEstimate(
                 flops=6 * row_count * units * groups * width,
@@ -385,8 +397,9 @@
                 transcendentals=row_count * units * groups,
             ),
             name="expert_layer",
-        )(*pieces, *addends, *weights[0], *far)
-    )
+        )(*pieces, *terms, *flat)
+    )
+    return [results[outputs * p : outputs * (p + 1)] for p in range(parts)]
 
 
 def mixing(columns, piece_refs, capacity):
@@ -402,97 +415,141 @@
     return dot(mix.astype(jnp.bfloat16), rows)
 
 
-def combine(me, columns, pieces, capacity, level, levels, keep, took):
-    token_count, width = columns.shape[0], pieces[0].shape[1]
-    owned = keep.shape[1]
-
-    def kernel(me_ref, columns_ref, keep_ref, took_ref, *refs):
-        mixed = mixing(columns_ref[...], refs[:-1], capacity).astype(jnp.bfloat16)
-        refs[-1][:token_count] = mixed
-        targets = [target_level(me_ref[3], me_ref[1], level, levels)]
-        if levels == RELAYED:
-            targets.append(me_ref[3] ^ 1)
-        for index, target in enumerate(targets):
-            both = keep_ref[target].astype(jnp.float32) + took_ref[target].astype(jnp.float32)
-            start = token_count + index * owned
-            refs[-1][start : start + owned] = both.astype(jnp.bfloat16)
-
-    rows = token_count + (2 if levels == RELAYED else 1) * owned
+def owed(keep_ref, took_ref, target):
+    both = keep_ref[target].astype(jnp.float32) + took_ref[target].astype(jnp.float32)
+    return both.astype(jnp.bfloat16)
+
+
+def combine(columns, pieces, capacity, level=None, part=0, terms=()):
+    token_count, wide = columns.shape[0], pieces[0].shape[1]
+
+    def kernel(columns_ref, *refs):
+        piece_refs, out_ref = refs[len(terms) : -1], refs[-1]
+        mixed = mixing(columns_ref[...], piece_refs, capacity).astype(jnp.bfloat16)
+        out_ref[:token_count] = mixed
+        if terms:
+            me_ref, keep_ref, took_ref = refs[:3]
+            step = 3 - me_ref[1] if level == 2 else 2 + me_ref[1]
+            rows = owed(keep_ref, took_ref, me_ref[3] ^ step)
+            out_ref[token_count:] = rows[:, part * wide : (part + 1) * wide]
+
+    rows = token_count + (terms[1].shape[1] if terms else 0)
     return pl.pallas_call(
         kernel,
-        out_shape=jax.ShapeDtypeStruct((rows, width), jnp.bfloat16),
-        in_specs=[SCALAR] + [VECTOR] * (3 + len(pieces)),
+        out_shape=jax.ShapeDtypeStruct((rows, wide), jnp.bfloat16),
+        in_specs=[VECTOR] + [SCALAR, VECTOR, VECTOR][: len(terms)] + [VECTOR] * len(pieces),
         out_specs=VECTOR,
         compiler_params=PARAMS,
         cost_estimate=pl.CostEstimate(
             flops=1_500_000_000, bytes_accessed=2_000_000, transcendentals=0
         ),
         name="combine",
-    )(me, columns, keep, took, *pieces)
-
-
-def merge(share, beside, across, token_count, owned):
-    end = token_count + owned
-
-    def kernel(share_ref, beside_ref, across_ref, out_ref):
-        total = share_ref[:end].astype(jnp.float32) + beside_ref[:end].astype(jnp.float32)
-        out_ref[:token_count] = total[:token_count].astype(jnp.bfloat16)
-        last = total[token_count:] + across_ref[end:].astype(jnp.float32)
-        out_ref[token_count:] = last.astype(jnp.bfloat16)
-
+    )(columns, *terms, *pieces)
+
+
+def owners(me, keep, took, levels):
+    def kernel(me_ref, keep_ref, took_ref, *out_refs):
+        for step, ref in enumerate(out_refs):
+            target = me_ref[3]
+            if step > 0:
+                if levels & (levels - 1) == 0:
+                    target = target ^ step
+                else:
+                    target = (target - step + levels) % levels
+            both = keep_ref[target].astype(jnp.float32) + took_ref[target].astype(jnp.float32)
+            ref[...] = both.astype(ref.dtype)
+
+    shapes = [
+        jax.ShapeDtypeStruct(keep.shape[1:], jnp.bfloat16 if step else jnp.float32)
+        for step in range(levels)
+    ]
     return pl.pallas_call(
         kernel,
-        out_shape=jax.ShapeDtypeStruct((end, share.shape[1]), jnp.bfloat16),
-        in_specs=[VECTOR] * 3,
-        out_specs=VECTOR,
+        out_shape=shapes,
+        in_specs=[SCALAR] + [VECTOR] * 2,
+        out_specs=[VECTOR] * levels,
         compiler_params=PARAMS,
         cost_estimate=pl.CostEstimate(
-            flops=500_000_000, bytes_accessed=2_000_000, transcendentals=0
+            flops=500_000_000, bytes_accessed=1_000_000, transcendentals=0
+        ),
+        name="owners",
+    )(me, keep, took)
+
+
+def merge(share, beside, count=1):
+    rows = share.shape[0]
+
+    def kernel(share_ref, beside_ref, *out_refs):
+        total = share_ref[...].astype(jnp.float32) + beside_ref[:rows].astype(jnp.float32)
+        total = total.astype(jnp.bfloat16)
+        part = rows // count
+        for index, ref in enumerate(out_refs):
+            ref[...] = total[index * part : (index + 1) * part]
+
+    shapes = piece_shapes(count, *share.shape)
+    return pl.pallas_call(
+        kernel,
+        out_shape=shapes,
+        in_specs=[VECTOR] * 2,
+        out_specs=[VECTOR] * count,
+        compiler_params=PARAMS,
+        cost_estimate=pl.CostEstimate(
+            flops=500_000_000, bytes_accessed=1_000_000, transcendentals=0
         ),
         name="merge",
-    )(share, beside, across)
-
-
-def finish(me, packed, pieces, capacity, expert_shares, mixer_shares, keep, took):
+    )(share, beside)
+
+
+def finish(me, packed, pieces, capacity, shares, keep, took, mixers):
     token_count, width = packed.shape
     width -= LANES
     owned = keep.shape[1]
-    shares = list({id(a): a for a in (*expert_shares, *(a for a, _ in mixer_shares))}.values())
-    places = {id(a): index for index, a in enumerate(shares)}
 
     def kernel(me_ref, columns_ref, keep_ref, took_ref, *refs):
         piece_refs = refs[: len(pieces)]
-        share_refs = refs[len(pieces) : -2]
+        share_refs = refs[len(pieces) : len(pieces) + len(shares)]
+        mixer_refs = refs[len(pieces) + len(shares) : -2]
         expert_ref, mixer_ref = refs[-2:]
         total = mixing(columns_ref[...], piece_refs, capacity)
-        for share in expert_shares:
-            total = total + share_refs[places[id(share)]][:token_count].astype(jnp.float32)
-        expert_ref[...] = total.astype(jnp.bfloat16)
         level = me_ref[3]
         mixer = keep_ref[level].astype(jnp.float32) + took_ref[level].astype(jnp.float32)
-        for share, slot in mixer_shares:
-            start = token_count + slot * owned
-            rows = share_refs[places[id(share)]][start : start + owned]
-            mixer = mixer + rows.astype(jnp.float32)
-        mixer_ref[...] = mixer.astype(jnp.bfloat16)
+        for ref in mixer_refs:
+            mixer = mixer + ref[...].astype(jnp.float32)
+        wide = share_refs[0].shape[1]
+        for left in range(0, width, wide):
+            part = total[:, left : left + wide]
+            terms = mixer[:, left : left + wide]
+            for ref, (place, _) in zip(share_refs, shares):
+                if place * wide == left:
+                    part = part + ref[:token_count].astype(jnp.float32)
+                    if ref.shape[0] > token_count:
+                        terms = terms + ref[token_count:].astype(jnp.float32)
+            expert_ref[:, left : left + wide] = part.astype(jnp.bfloat16)
+            mixer_ref[:, left : left + wide] = terms.astype(jnp.bfloat16)
 
     shapes = (
         jax.ShapeDtypeStruct((token_count, width), jnp.bfloat16),
         jax.ShapeDtypeStruct(keep.shape[1:], jnp.bfloat16),
     )
+    arrays = (keep, took, *pieces, *(share for _, share in shares))
+    ends = [
+        pl.BlockSpec((owned, width), lambda i, a=a: (a.shape[0] // owned - 1, 0)) for a in mixers
+    ]
     return pl.pallas_call(
         kernel,
         grid=(1,),
         out_shape=shapes,
         in_specs=[SCALAR, pl.BlockSpec((token_count, LANES), lambda i: (0, width // LANES))]
-        + [whole(a) for a in (keep, took, *pieces, *shares)],
+        + [whole(a) for a in arrays[: -len(shares)]]
+        + [VECTOR] * len(shares)
+        + ends,
         out_specs=[whole(a) for a in shapes],
         compiler_params=PARAMS,
         cost_estimate=pl.CostEstimate(
             flops=1_500_000_000, bytes_accessed=2_000_000, transcendentals=0
         ),
         name="finish",
-    )(me, packed, keep, took, *pieces, *shares)
+    )(me, packed, *arrays, *mixers)
 
 
 def body(
@@ -538,7 +595,7 @@
     own = (gate_weight[0].T, up_weight[0].T, down_weight[0])
     weights = [tuple(over_core(w, step) for w in own) for step in range(1, CORES)]
     own = tuple(pltpu.with_memory_space_constraint(w, pltpu.VMEM) for w in own)
-    weights = [own] + weights
+    weights = [own] + [hold(group) for group in weights]
     arrived = [over_ep(pieces)]
     if piece_count == 1:
         both = jnp.concatenate([key_rows, value_rows], axis=1)
@@ -568,36 +625,43 @@
         arrived.append(over_ep(picked))
 
     piece_rows = slot_count // piece_count
+    terms = (me, keep, took)
 
     def layer(level, **options):
         return expert_layer(arrived[level], piece_rows, weights, **options)
 
-    def share_of(level):
-        returned = over_ep(layer(level), back=True)
-        return combine(me, columns[level], returned, capacity, level, levels, keep, took)
-
+    def shares_of(level, parts, **options):
+        shares = []
+        for part, results in enumerate(layer(level, parts=parts)):
+            returned = over_ep(results, back=True)
+            shares.append(
+                combine(columns[level], returned, capacity, level, part, **options)
+            )
+        return shares
+
+    shares = []
     if levels == RELAYED:
-        beside = over_z(layer(1, joined=True)[0], [(0, 1), (1, 0), (2, 3), (3, 2)])
-        share = share_of(2)
-        inner = over_z(share, [(1, 2), (2, 1)])
-        distant = over_z(share, [(0, 2), (3, 1)])
-        share = share_of(3)
-        nearer = over_z(share, [(0, 1), (3, 2)])
-        share = merge(share, nearer, inner, token_count, keep.shape[1])
-        last = over_z(share, [(1, 3), (2, 0)])
-        results = layer(0, addend=beside)
-        expert_shares = [inner, distant, last]
-        mixer_shares = [(inner, 0), (distant, 0), (nearer, 1), (last, 0)]
+        results = layer(1, joined=True, terms=terms)[0][0]
+        beside = over_z(results, [(0, 1), (1, 0), (2, 3), (3, 2)])
+        mixers = [beside]
+        for level, pairs in ((2, [(1, 2), (2, 1)]), (3, [(1, 3), (2, 0)])):
+            for part, share in enumerate(shares_of(level, PARTS, terms=terms)):
+                nearer = over_z(share, [(0, 1), (3, 2)])
+                (share,) = merge(share, nearer)
+                shares.append((part, over_z(share, pairs)))
+        results = layer(0, joined=True)[0][0]
+        results = merge(results, beside, piece_count)
     else:
-        expert_shares = []
+        mixers = []
+        far_terms = owners(me, keep, took, levels)
         for level in range(1, levels):
             pairs = [(partner(i, level, levels), i) for i in range(levels)]
-            expert_shares.append(over_z(share_of(level), pairs))
-        results = layer(0)
-        mixer_shares = [(share, 0) for share in expert_shares]
+            shares.append((0, over_z(shares_of(level, 1)[0], pairs)))
+            mixers.append(over_z(far_terms[level], pairs))
+        results = layer(0)[0]
     returned = over_ep(results, back=True)
     expert_output, mixer_output = finish(
-        me, packed, returned, capacity, expert_shares, mixer_shares, keep, took
+        me, packed, returned, capacity, shares, keep, took, mixers
     )
     return (mixer_output, expert_output)
 

time: 180 us -> 169 us (0.939)
  waiting for transfers between devices: 102 us -> 82.4 us
  starting transfers between devices: 45.9 us -> 52.7 us
    ppermute x21 -> x27, waiting for transfers between devices: 43.7 us -> 31.4 us  [over_ep(): moved.append(lax.ppermute(pieces[step], 'ep', pairs))]
    ppermute x10 -> x14, waiting for transfers between devices: 57.9 us -> 51 us  [over_z(): return lax.ppermute(array, 'tp', pairs)]
    ppermute x10 -> x14, starting transfers between devices: 17.9 us -> 21.8 us  [over_z(): return lax.ppermute(array, 'tp', pairs)]
    ppermute x21 -> x27, starting transfers between devices: 27.9 us -> 30.8 us  [over_ep(): moved.append(lax.ppermute(pieces[step], 'ep', pairs))]
    pallas_call x7 -> x14, Pallas kernels: 19.2 us -> 19.3 us  [the longest x4 14.7 us: expert_layer(): pl.pallas_call(kernel, out_shape=shapes, in_specs=[VECTOR] * count + [SCA...]
  transfers between devices with their start and end apart: 35 -> 45, of which waited for: 17 -> 15; matrix products, arithmetic and copies ran while one was open for 0% -> 0% of each run, Pallas kernels for 15% -> 16%
where the time goes in v2:
time: 169 us; the launch traced here: 168 us
  waiting for transfers between devices  82.4 us (49%)
  starting transfers between devices  52.7 us (31%)
  Pallas kernels  31.7 us (19%)
    ppermute x14, waiting for transfers between devices, over_z(): return lax.ppermute(array, 'tp', pairs)  51 us
    ppermute x27, waiting for transfers between devices, over_ep(): moved.append(lax.ppermute(pieces[step], 'ep', pairs))  31.4 us
    ppermute x27, starting transfers between devices, over_ep(): moved.append(lax.ppermute(pieces[step], 'ep', pairs))  30.8 us
    ppermute x14, starting transfers between devices, over_z(): return lax.ppermute(array, 'tp', pairs)  21.8 us
    pallas_call x4, Pallas kernels, expert_layer(): pl.pallas_call(kernel, out_shape=shapes, in_specs=[VECTOR] * count + [SCA...  14.7 us
    pallas_call x1, Pallas kernels, attention(): pl.pallas_call(lambda *refs: attention_kernel(slots, *refs), out_shape=[j...  4.69 us
    pallas_call x4, Pallas kernels, combine(): pl.pallas_call(kernel, out_shape=jax.ShapeDtypeStruct((rows, wide), jnp.b...  3.6 us
  transfers between devices with their start and end apart: 45, of which 15 were waited for; matrix products, arithmetic and copies ran while one was open for 0% of the time, Pallas kernels for 16%

profile of v2, /device:TPU:0, one launch (start us, length us, event | category | flops | bytes accessed | tf_op | source)
XLA Modules:
  0.0 168.0 jit_solution(15729070282355419510)
XLA Ops:
  0.8 2.6 %prepare.1 = (bf16[128,2176]{1,0:T(8,128)(2,1)S(1)}, bf16[64,2048]{1,0:T(8,128)(2,1)S(1)}, bf16[96,2048]{1,0:T(8,128)(2,1)S(1)}, bf16[96,2048]{1,0:T(8,128)(2,1)S(1)}, bf16[96,2048]{1,0:T(8,128)(2,1)S(1)}) custom-call(s32[4]{0:T(128)S(1)} %pad_add_fusion.refs_0_.me_ref.refs_4_, bf16[128,2048]{1,0:T(8,128)(2,1)} %refs_1_.2, f32[1,2048]{1,0:T(1,128)} %bitcast.33, ...), custom_call_target="tpu_custom_call" | custom-call | flops 2000000000 | bytes 3000000 | tf_op jit(solution)/shard_map/prepare/pallas_call | solution.py:276
  3.4 3.0 %collective-permute-start = (bf16[96,2048]{1,0:T(8,128)(2,1)S(1)}, bf16[96,2048]{1,0:T(8,128)(2,1)S(1)}, u32[]{:S(2)}, u32[]{:S(2)}) collective-permute-start(bf16[96,2048]{1,0:T(8,128)(2,1)S(1)} %get-tuple-element.49), channel_id=1, source_target_pairs={{0,8},{8,0},{16,24},{24,16},{1,9},{9,1},{17,25},{25,17},{2,10},{10... | collective-permute-start | bytes 1179656 | tf_op jit(solution)/shard_map/ppermute | solution.py:40
  6.5 1.5 collective-permute-start.1
  8.0 1.6 collective-permute-start.7
  10.1 6.4 %collective-permute-done.refs_8_.refs_1_ = bf16[96,2048]{1,0:T(8,128)(2,1)S(1)} collective-permute-done((bf16[96,2048]{1,0:T(8,128)(2,1)S(1)}, bf16[96,2048]{1,0:T(8,128)(2,1)S(1)}, u32[]{:S(2)}, u32[]{:S(2)}) %collective-permute-start) | collective-permute-done | bytes 393248 | tf_op jit(solution)/shard_map/ppermute | solution.py:40
  16.4 9.0 %collective-permute-done.1.refs_9_.refs_2_ = bf16[96,2048]{1,0:T(8,128)(2,1)S(1)} collective-permute-done((bf16[96,2048]{1,0:T(8,128)(2,1)S(1)}, bf16[96,2048]{1,0:T(8,128)(2,1)S(1)}, u32[]{:S(2)}, u32[]{:S(2)}) %collective-permute-start.1) | collective-permute-done | bytes 393248 | tf_op jit(solution)/shard_map/ppermute | solution.py:40
  29.6 4.7 %attention.1 = (bf16[4,16,2048]{2,1,0:T(8,128)(2,1)S(1)}, bf16[4,16,2048]{2,1,0:T(8,128)(2,1)S(1)}) custom-call(s32[4]{0:T(128)S(1)} %pad_add_fusion.refs_0_.me_ref.refs_4_, f32[4]{0:T(128)S(1)} %copy-done.7, bf16[128,256]{1,0:T(8,128)(2,1)S(1)} %copy-done.6, f32[1,64]{1,0:T(1,128)S(1)} %bitcast.31, f32[1,64]{1,0:T(1,128)S(1)} %bitcast.32, ...), custom_call_target="tpu_custom_call" | custom-call | flops 6000000000 | bytes 3000000 | tf_op jit(solution)/shard_map/attention/pallas_call | solution.py:170
  34.3 23.4 %collective-permute-done.16.refs_0_ = bf16[128,2176]{1,0:T(8,128)(2,1)S(1)} collective-permute-done((bf16[128,2176]{1,0:T(8,128)(2,1)S(1)}, bf16[128,2176]{1,0:T(8,128)(2,1)S(1)}, u32[]{:S(2)}, u32[]{:S(2)}) %collective-permute-start.16) | collective-permute-done | bytes 557088 | tf_op jit(solution)/shard_map/ppermute | solution.py:46
  58.8 10.8 %collective-permute-done.31.refs_0_ = bf16[128,2176]{1,0:T(8,128)(2,1)S(1)} collective-permute-done((bf16[128,2176]{1,0:T(8,128)(2,1)S(1)}, bf16[128,2176]{1,0:T(8,128)(2,1)S(1)}, u32[]{:S(2)}, u32[]{:S(2)}) %collective-permute-start.31) | collective-permute-done | bytes 557088 | tf_op jit(solution)/shard_map/ppermute | solution.py:46
  69.6 1.5 collective-permute-start.18
  73.5 2.0 %collective-permute-start.8 = (bf16[64,2048]{1,0:T(8,128)(2,1)S(1)}, bf16[64,2048]{1,0:T(8,128)(2,1)S(1)}, u32[]{:S(2)}, u32[]{:S(2)}) collective-permute-start(bf16[64,2048]{1,0:T(8,128)(2,1)S(1)} %get-tuple-element.59), channel_id=1, source_target_pairs={{0,8},{8,0},{16,24},{24,16},{1,9},{9,1},{17,25},{25,17},{2,10},{10... | collective-permute-start | bytes 786440 | tf_op jit(solution)/shard_map/ppermute | solution.py:40
  75.9 1.6 collective-permute-start.9
  77.5 7.1 %collective-permute-done.18.refs_2_ = bf16[64,2048]{1,0:T(8,128)(2,1)S(1)} collective-permute-done((bf16[64,2048]{1,0:T(8,128)(2,1)S(1)}, bf16[64,2048]{1,0:T(8,128)(2,1)S(1)}, u32[]{:S(2)}, u32[]{:S(2)}) %collective-permute-start.18) | collective-permute-done | bytes 262176 | tf_op jit(solution)/shard_map/ppermute | solution.py:40
  85.0 1.7 %collective-permute-start.32 = (bf16[64,2048]{1,0:T(8,128)(2,1)S(1)}, bf16[64,2048]{1,0:T(8,128)(2,1)S(1)}, u32[]{:S(2)}, u32[]{:S(2)}) collective-permute-start(bf16[64,2048]{1,0:T(8,128)(2,1)S(1)} %get-tuple-element.81), channel_id=1, source_target_pairs={{0,8},{8,0},{16,24},{24,16},{1,9},{9,1},{17,25},{25,17},{2,10},{10... | collective-permute-start | bytes 786440 | tf_op jit(solution)/shard_map/ppermute | solution.py:40
  86.7 3.5 %expert_layer.6 = (bf16[64,1024]{1,0:T(8,128)(2,1)S(1)}, bf16[64,1024]{1,0:T(8,128)(2,1)S(1)}, bf16[64,1024]{1,0:T(8,128)(2,1)S(1)}, bf16[64,1024]{1,0:T(8,128)(...) custom-call(bf16[64,2048]{1,0:T(8,128)(2,1)S(1)} %get-tuple-element., ...), custom_call_target="tpu_custom_call" | custom-call | flops 2818572288 | bytes 11010048 | tf_op jit(solution)/shard_map/expert_layer/pallas_call | solution.py:386
  92.1 5.8 %collective-permute-done.9.refs_2_ = bf16[64,2048]{1,0:T(8,128)(2,1)S(1)} collective-permute-done((bf16[64,2048]{1,0:T(8,128)(2,1)S(1)}, bf16[64,2048]{1,0:T(8,128)(2,1)S(1)}, u32[]{:S(2)}, u32[]{:S(2)}) %collective-permute-start.9) | collective-permute-done | bytes 262176 | tf_op jit(solution)/shard_map/ppermute | solution.py:40
  98.0 2.0 %collective-permute-start.25 = (bf16[64,1024]{1,0:T(8,128)(2,1)S(1)}, bf16[64,1024]{1,0:T(8,128)(2,1)S(1)}, u32[]{:S(2)}, u32[]{:S(2)}) collective-permute-start(bf16[64,1024]{1,0:T(8,128)(2,1)S(1)} %get-tuple-element.76), channel_id=1, source_target_pairs={{8,0},{0,8},{24,16},{16,24},{9,1},{1,9},{25,17},{17,25},{10,2},{2,... | collective-permute-start | bytes 393224 | tf_op jit(solution)/shard_map/ppermute | solution.py:40
  100.0 4.1 %expert_layer.5 = bf16[272,2048]{1,0:T(8,128)(2,1)S(1)} custom-call(bf16[64,2048]{1,0:T(8,128)(2,1)S(1)} %get-tuple-element.58.refs_0_, bf16[64,2048]{1,0:T(8,128)(2,1)S(1)} %collective-permute-done.8.refs_1_, bf16[64,2048]{1,0:T(8,128)(2,1)S(1)} %collective-permute-done.9.refs_2_, bf16[64,2048]{1,0:T(8,128)(2,1)S(1)} %collective-permute-done.10.refs_3_, ...), custom_call_target="tpu_custom_call" | custom-call | flops 2818572288 | bytes 11010048 | tf_op jit(solution)/shard_map/expert_layer/pallas_call | solution.py:386
  104.7 2.5 %collective-permute-done.33.refs_2_ = bf16[64,2048]{1,0:T(8,128)(2,1)S(1)} collective-permute-done((bf16[64,2048]{1,0:T(8,128)(2,1)S(1)}, bf16[64,2048]{1,0:T(8,128)(2,1)S(1)}, u32[]{:S(2)}, u32[]{:S(2)}) %collective-permute-start.33) | collective-permute-done | bytes 262176 | tf_op jit(solution)/shard_map/ppermute | solution.py:40
  107.5 3.5 %expert_layer.7 = (bf16[64,1024]{1,0:T(8,128)(2,1)S(1)}, bf16[64,1024]{1,0:T(8,128)(2,1)S(1)}, bf16[64,1024]{1,0:T(8,128)(2,1)S(1)}, bf16[64,1024]{1,0:T(8,128)(...) custom-call(bf16[64,2048]{1,0:T(8,128)(2,1)S(1)} %get-tuple-element., ...), custom_call_target="tpu_custom_call" | custom-call | flops 2818572288 | bytes 11010048 | tf_op jit(solution)/shard_map/expert_layer/pallas_call | solution.py:386
  112.1 2.3 %collective-permute-start.22 = (bf16[64,1024]{1,0:T(8,128)(2,1)S(1)}, bf16[64,1024]{1,0:T(8,128)(2,1)S(1)}, u32[]{:S(2)}, u32[]{:S(2)}) collective-permute-start(bf16[64,1024]{1,0:T(8,128)(2,1)S(1)} %get-tuple-element.74), channel_id=1, source_target_pairs={{24,0},{16,8},{8,16},{0,24},{25,1},{17,9},{9,17},{1,25},{26,2},{18... | collective-permute-start | bytes 393224 | tf_op jit(solution)/shard_map/ppermute | solution.py:40
  115.5 2.0 %collective-permute-start.40 = (bf16[64,1024]{1,0:T(8,128)(2,1)S(1)}, bf16[64,1024]{1,0:T(8,128)(2,1)S(1)}, u32[]{:S(2)}, u32[]{:S(2)}) collective-permute-start(bf16[64,1024]{1,0:T(8,128)(2,1)S(1)} %get-tuple-element.89), channel_id=1, source_target_pairs={{8,0},{0,8},{24,16},{16,24},{9,1},{1,9},{25,17},{17,25},{10,2},{2,... | collective-permute-start | bytes 393224 | tf_op jit(solution)/shard_map/ppermute | solution.py:40
  118.9 2.2 %collective-permute-start.42 = (bf16[64,1024]{1,0:T(8,128)(2,1)S(1)}, bf16[64,1024]{1,0:T(8,128)(2,1)S(1)}, u32[]{:S(2)}, u32[]{:S(2)}) collective-permute-start(bf16[64,1024]{1,0:T(8,128)(2,1)S(1)} %get-tuple-element.91), channel_id=1, source_target_pairs={{24,0},{16,8},{8,16},{0,24},{25,1},{17,9},{9,17},{1,25},{26,2},{18... | collective-permute-start | bytes 393224 | tf_op jit(solution)/shard_map/ppermute | solution.py:40
  121.1 6.2 %collective-permute-start.28 = (bf16[144,1024]{1,0:T(8,128)(2,1)S(1)}, bf16[144,1024]{1,0:T(8,128)(2,1)S(1)}, u32[]{:S(2)}, u32[]{:S(2)}) collective-permute-start(bf16[144,1024]{1,0:T(8,128)(2,1)S(1)} %combine.5.share_ref), channel_id=1, source_target_pairs={{0,2},{1,3},{6,4},{7,5},{8,10},{9,11},{14,12},{15,13},{16,18},{17,... | collective-permute-start | bytes 884744 | tf_op jit(solution)/shard_map/ppermute | solution.py:46
  129.4 3.2 %collective-permute-start.23 = (bf16[144,1024]{1,0:T(8,128)(2,1)S(1)}, bf16[144,1024]{1,0:T(8,128)(2,1)S(1)}, u32[]{:S(2)}, u32[]{:S(2)}) collective-permute-start(bf16[144,1024]{1,0:T(8,128)(2,1)S(1)} %combine.4.share_ref), channel_id=1, source_target_pairs={{0,2},{1,3},{6,4},{7,5},{8,10},{9,11},{14,12},{15,13},{16,18},{17,... | collective-permute-start | bytes 884744 | tf_op jit(solution)/shard_map/ppermute | solution.py:46
  139.5 5.6 %collective-permute-done.23.beside_ref = bf16[144,1024]{1,0:T(8,128)(2,1)S(1)} collective-permute-done((bf16[144,1024]{1,0:T(8,128)(2,1)S(1)}, bf16[144,1024]{1,0:T(8,128)(2,1)S(1)}, u32[]{:S(2)}, u32[]{:S(2)}) %collective-permute-start.23) | collective-permute-done | bytes 294944 | tf_op jit(solution)/shard_map/ppermute | solution.py:46
  146.1 3.5 %expert_layer.4.share_ref = bf16[256,2048]{1,0:T(8,128)(2,1)S(1)} custom-call(bf16[64,2048]{1,0:T(8,128)(2,1)S(1)} %get-tuple-element.54.refs_0_, bf16[96,2048]{1,0:T(8,128)(2,1)S(1)} %collective-permute-done.refs_8_.refs_1_, bf16[96,2048]{1,0:T(8,128)(2,1)S(1)} %collective-permute-done.1.refs_9_.refs_2_, ...), custom_call_target="tpu_custom_call" | custom-call | flops 2818572288 | bytes 11010048 | tf_op jit(solution)/shard_map/expert_layer/pallas_call | solution.py:386
  152.1 1.8 %collective-permute-done.38.beside_ref = bf16[144,1024]{1,0:T(8,128)(2,1)S(1)} collective-permute-done((bf16[144,1024]{1,0:T(8,128)(2,1)S(1)}, bf16[144,1024]{1,0:T(8,128)(2,1)S(1)}, u32[]{:S(2)}, u32[]{:S(2)}) %collective-permute-start.38) | collective-permute-done | bytes 294944 | tf_op jit(solution)/shard_map/ppermute | solution.py:46
  156.6 2.6 %collective-permute-start.14 = (bf16[64,2048]{1,0:T(8,128)(2,1)S(1)}, bf16[64,2048]{1,0:T(8,128)(2,1)S(1)}, u32[]{:S(2)}, u32[]{:S(2)}) collective-permute-start(bf16[64,2048]{1,0:T(8,128)(2,1)S(1)} %get-tuple-element.65), channel_id=1, source_target_pairs={{24,0},{16,8},{8,16},{0,24},{25,1},{17,9},{9,17},{1,25},{26,2},{18... | collective-permute-start | bytes 786440 | tf_op jit(solution)/shard_map/ppermute | solution.py:40
  159.1 3.8 %collective-permute-done.44.refs_7_ = bf16[144,1024]{1,0:T(8,128)(2,1)S(1)} collective-permute-done((bf16[144,1024]{1,0:T(8,128)(2,1)S(1)}, bf16[144,1024]{1,0:T(8,128)(2,1)S(1)}, u32[]{:S(2)}, u32[]{:S(2)}) %collective-permute-start.44) | collective-permute-done | bytes 294944 | tf_op jit(solution)/shard_map/ppermute | solution.py:46
  163.0 3.2 %collective-permute-done.39.refs_6_ = bf16[144,1024]{1,0:T(8,128)(2,1)S(1)} collective-permute-done((bf16[144,1024]{1,0:T(8,128)(2,1)S(1)}, bf16[144,1024]{1,0:T(8,128)(2,1)S(1)}, u32[]{:S(2)}, u32[]{:S(2)}) %collective-permute-start.39) | collective-permute-done | bytes 294944 | tf_op jit(solution)/shard_map/ppermute | solution.py:46
  166.1 1.9 %finish.1 = (bf16[128,2048]{1,0:T(8,128)(2,1)}, bf16[16,2048]{1,0:T(8,128)(2,1)}) custom-call(s32[4]{0:T(128)S(1)} %pad_add_fusion.refs_0_.me_ref.refs_4_, bf16[128,2176]{1,0:T(8,128)(2,1)S(1)} %get-tuple-element.48.columns_ref, bf16[4,16,2048]{2,1,0:T(8,128)(2,1)S(1)} %get-tuple-element.52.refs_5_.refs_1_.keep_ref, ...), custom_call_target="tpu_custom_call" | custom-call | flops 1500000000 | bytes 2000000 | tf_op jit(solution)/shard_map/finish/pallas_call | solution.py:538
  (99 shorter events, 30.1 us)
Async XLA Ops:
  3.4 13.0 %collective-permute-start = (bf16[96,2048]{1,0:T(8,128)(2,1)S(1)}, bf16[96,2048]{1,0:T(8,128)(2,1)S(1)}, u32[]{:S(2)}, u32[]{:S(2)}) collective-permute-start(bf16[96,2048]{1,0:T(8,128)(2,1)S(1)} %get-tuple-element.49), channel_id=1, source_target_pairs={{0,8},{8,0},{16,24},{24,16},{1,9},{9,1},{17,25},{25,17},{2,10},{10... | collective-permute-start | bytes 1179656 | tf_op jit(solution)/shard_map/ppermute | solution.py:40
  6.5 19.0 %collective-permute-start.1 = (bf16[96,2048]{1,0:T(8,128)(2,1)S(1)}, bf16[96,2048]{1,0:T(8,128)(2,1)S(1)}, u32[]{:S(2)}, u32[]{:S(2)}) collective-permute-start(bf16[96,2048]{1,0:T(8,128)(2,1)S(1)} %get-tuple-element.50), channel_id=1, source_target_pairs={{0,16},{8,24},{16,0},{24,8},{1,17},{9,25},{17,1},{25,9},{2,18},{10... | collective-permute-start | bytes 1179656 | tf_op jit(solution)/shard_map/ppermute | solution.py:40
  8.0 63.1 %collective-permute-start.4 = (bf16[448,2048]{1,0:T(8,128)(2,1)S(1)}, bf16[448,2048]{1,0:T(8,128)(2,1)S(1)}, u32[]{:S(2)}, u32[]{:S(2)}) collective-permute-start(bf16[448,2048]{1,0:T(8,128)(2,1)S(1)} %bitcast.16), channel_id=1, source_target_pairs={{0,1},{1,0},{2,3},{3,2},{4,5},{5,4},{6,7},{7,6},{8,9},{9,8},{10,11... | collective-permute-start | bytes 5505032 | tf_op jit(solution)/shard_map/ppermute | solution.py:70
  8.0 18.2 %collective-permute-start.7 = (bf16[128,2176]{1,0:T(8,128)(2,1)S(1)}, bf16[128,2176]{1,0:T(8,128)(2,1)S(1)}, u32[]{:S(2)}, u32[]{:S(2)}) collective-permute-start(bf16[128,2176]{1,0:T(8,128)(2,1)S(1)} %get-tuple-element.48.columns_ref), channel_id=1, source_target_pairs={{0,2},{1,3},{2,0},{3,1},{4,6},{5,7},{6,4},{7,5},{8,10},{9,11},{10,... | collective-permute-start | bytes 1671176 | tf_op jit(solution)/shard_map/ppermute | solution.py:46
  9.6 15.9 %collective-permute-start.2 = (bf16[96,2048]{1,0:T(8,128)(2,1)S(1)}, bf16[96,2048]{1,0:T(8,128)(2,1)S(1)}, u32[]{:S(2)}, u32[]{:S(2)}) collective-permute-start(bf16[96,2048]{1,0:T(8,128)(2,1)S(1)} %get-tuple-element.51), channel_id=1, source_target_pairs={{0,24},{8,16},{16,8},{24,0},{1,25},{9,17},{17,9},{25,1},{2,26},{10... | collective-permute-start | bytes 1179656 | tf_op jit(solution)/shard_map/ppermute | solution.py:40
  16.4 56.9 %collective-permute-start.5 = (bf16[448,2048]{1,0:T(8,128)(2,1)S(1)}, bf16[448,2048]{1,0:T(8,128)(2,1)S(1)}, u32[]{:S(2)}, u32[]{:S(2)}) collective-permute-start(bf16[448,2048]{1,0:T(8,128)(2,1)S(1)} %bitcast.21), channel_id=1, source_target_pairs={{0,1},{1,0},{2,3},{3,2},{4,5},{5,4},{6,7},{7,6},{8,9},{9,8},{10,11... | collective-permute-start | bytes 5505032 | tf_op jit(solution)/shard_map/ppermute | solution.py:70
  25.5 48.0 %collective-permute-start.6 = (bf16[448,2048]{1,0:T(8,128)(2,1)S(1)}, bf16[448,2048]{1,0:T(8,128)(2,1)S(1)}, u32[]{:S(2)}, u32[]{:S(2)}) collective-permute-start(bf16[448,2048]{1,0:T(8,128)(2,1)S(1)} %bitcast.26), channel_id=1, source_target_pairs={{0,1},{1,0},{2,3},{3,2},{4,5},{5,4},{6,7},{7,6},{8,9},{9,8},{10,11... | collective-permute-start | bytes 5505032 | tf_op jit(solution)/shard_map/ppermute | solution.py:70
  26.9 30.8 %collective-permute-start.16 = (bf16[128,2176]{1,0:T(8,128)(2,1)S(1)}, bf16[128,2176]{1,0:T(8,128)(2,1)S(1)}, u32[]{:S(2)}, u32[]{:S(2)}) collective-permute-start(bf16[128,2176]{1,0:T(8,128)(2,1)S(1)} %collective-permute-done.15.refs_1_), channel_id=1, source_target_pairs={{2,0},{3,1},{4,6},{5,7},{10,8},{11,9},{12,14},{13,15},{18,16},{19,... | collective-permute-start | bytes 1671176 | tf_op jit(solution)/shard_map/ppermute | solution.py:46
  28.2 41.4 %collective-permute-start.31 = (bf16[128,2176]{1,0:T(8,128)(2,1)S(1)}, bf16[128,2176]{1,0:T(8,128)(2,1)S(1)}, u32[]{:S(2)}, u32[]{:S(2)}) collective-permute-start(bf16[128,2176]{1,0:T(8,128)(2,1)S(1)} %collective-permute-done.30.refs_1_), channel_id=1, source_target_pairs={{2,0},{3,1},{4,6},{5,7},{10,8},{11,9},{12,14},{13,15},{18,16},{19,... | collective-permute-start | bytes 1671176 | tf_op jit(solution)/shard_map/ppermute | solution.py:46
  58.7 17.2 %collective-permute-start.17 = (bf16[64,2048]{1,0:T(8,128)(2,1)S(1)}, bf16[64,2048]{1,0:T(8,128)(2,1)S(1)}, u32[]{:S(2)}, u32[]{:S(2)}) collective-permute-start(bf16[64,2048]{1,0:T(8,128)(2,1)S(1)} %get-tuple-element.68), channel_id=1, source_target_pairs={{0,8},{8,0},{16,24},{24,16},{1,9},{9,1},{17,25},{25,17},{2,10},{10... | collective-permute-start | bytes 786440 | tf_op jit(solution)/shard_map/ppermute | solution.py:40
  69.6 15.0 %collective-permute-start.18 = (bf16[64,2048]{1,0:T(8,128)(2,1)S(1)}, bf16[64,2048]{1,0:T(8,128)(2,1)S(1)}, u32[]{:S(2)}, u32[]{:S(2)}) collective-permute-start(bf16[64,2048]{1,0:T(8,128)(2,1)S(1)} %get-tuple-element.69), channel_id=1, source_target_pairs={{0,16},{8,24},{16,0},{24,8},{1,17},{9,25},{17,1},{25,9},{2,18},{10... | collective-permute-start | bytes 786440 | tf_op jit(solution)/shard_map/ppermute | solution.py:40
  71.1 13.9 %collective-permute-start.19 = (bf16[64,2048]{1,0:T(8,128)(2,1)S(1)}, bf16[64,2048]{1,0:T(8,128)(2,1)S(1)}, u32[]{:S(2)}, u32[]{:S(2)}) collective-permute-start(bf16[64,2048]{1,0:T(8,128)(2,1)S(1)} %get-tuple-element.70), channel_id=1, source_target_pairs={{0,24},{8,16},{16,8},{24,0},{1,25},{9,17},{17,9},{25,1},{2,26},{10... | collective-permute-start | bytes 786440 | tf_op jit(solution)/shard_map/ppermute | solution.py:40
  73.4 16.9 %collective-permute-start.3 = (bf16[4,16,2048]{2,1,0:T(8,128)(2,1)S(1)}, bf16[4,16,2048]{2,1,0:T(8,128)(2,1)S(1)}, u32[]{:S(2)}, u32[]{:S(2)}) collective-permute-start(bf16[4,16,2048]{2,1,0:T(8,128)(2,1)S(1)} %get-tuple-element.53), channel_id=1, source_target_pairs={{0,1},{1,0},{2,3},{3,2},{4,5},{5,4},{6,7},{7,6},{8,9},{9,8},{10,11... | collective-permute-start | bytes 786440 | tf_op jit(solution)/shard_map/ppermute | solution.py:70
  73.5 18.3 %collective-permute-start.8 = (bf16[64,2048]{1,0:T(8,128)(2,1)S(1)}, bf16[64,2048]{1,0:T(8,128)(2,1)S(1)}, u32[]{:S(2)}, u32[]{:S(2)}) collective-permute-start(bf16[64,2048]{1,0:T(8,128)(2,1)S(1)} %get-tuple-element.59), channel_id=1, source_target_pairs={{0,8},{8,0},{16,24},{24,16},{1,9},{9,1},{17,25},{25,17},{2,10},{10... | collective-permute-start | bytes 786440 | tf_op jit(solution)/shard_map/ppermute | solution.py:40
  75.9 22.0 %collective-permute-start.9 = (bf16[64,2048]{1,0:T(8,128)(2,1)S(1)}, bf16[64,2048]{1,0:T(8,128)(2,1)S(1)}, u32[]{:S(2)}, u32[]{:S(2)}) collective-permute-start(bf16[64,2048]{1,0:T(8,128)(2,1)S(1)} %get-tuple-element.60), channel_id=1, source_target_pairs={{0,16},{8,24},{16,0},{24,8},{1,17},{9,25},{17,1},{25,9},{2,18},{10... | collective-permute-start | bytes 786440 | tf_op jit(solution)/shard_map/ppermute | solution.py:40
  84.6 13.4 %collective-permute-start.10 = (bf16[64,2048]{1,0:T(8,128)(2,1)S(1)}, bf16[64,2048]{1,0:T(8,128)(2,1)S(1)}, u32[]{:S(2)}, u32[]{:S(2)}) collective-permute-start(bf16[64,2048]{1,0:T(8,128)(2,1)S(1)} %get-tuple-element.61), channel_id=1, source_target_pairs={{0,24},{8,16},{16,8},{24,0},{1,25},{9,17},{17,9},{25,1},{2,26},{10... | collective-permute-start | bytes 786440 | tf_op jit(solution)/shard_map/ppermute | solution.py:40
  85.0 19.0 %collective-permute-start.32 = (bf16[64,2048]{1,0:T(8,128)(2,1)S(1)}, bf16[64,2048]{1,0:T(8,128)(2,1)S(1)}, u32[]{:S(2)}, u32[]{:S(2)}) collective-permute-start(bf16[64,2048]{1,0:T(8,128)(2,1)S(1)} %get-tuple-element.81), channel_id=1, source_target_pairs={{0,8},{8,0},{16,24},{24,16},{1,9},{9,1},{17,25},{25,17},{2,10},{10... | collective-permute-start | bytes 786440 | tf_op jit(solution)/shard_map/ppermute | solution.py:40
  90.3 17.0 %collective-permute-start.33 = (bf16[64,2048]{1,0:T(8,128)(2,1)S(1)}, bf16[64,2048]{1,0:T(8,128)(2,1)S(1)}, u32[]{:S(2)}, u32[]{:S(2)}) collective-permute-start(bf16[64,2048]{1,0:T(8,128)(2,1)S(1)} %get-tuple-element.82), channel_id=1, source_target_pairs={{0,16},{8,24},{16,0},{24,8},{1,17},{9,25},{17,1},{25,9},{2,18},{10... | collective-permute-start | bytes 786440 | tf_op jit(solution)/shard_map/ppermute | solution.py:40
  91.7 15.8 %collective-permute-start.34 = (bf16[64,2048]{1,0:T(8,128)(2,1)S(1)}, bf16[64,2048]{1,0:T(8,128)(2,1)S(1)}, u32[]{:S(2)}, u32[]{:S(2)}) collective-permute-start(bf16[64,2048]{1,0:T(8,128)(2,1)S(1)} %get-tuple-element.83), channel_id=1, source_target_pairs={{0,24},{8,16},{16,8},{24,0},{1,25},{9,17},{17,9},{25,1},{2,26},{10... | collective-permute-start | bytes 786440 | tf_op jit(solution)/shard_map/ppermute | solution.py:40
  97.9 17.6 %collective-permute-start.20 = (bf16[64,1024]{1,0:T(8,128)(2,1)S(1)}, bf16[64,1024]{1,0:T(8,128)(2,1)S(1)}, u32[]{:S(2)}, u32[]{:S(2)}) collective-permute-start(bf16[64,1024]{1,0:T(8,128)(2,1)S(1)} %get-tuple-element.72), channel_id=1, source_target_pairs={{8,0},{0,8},{24,16},{16,24},{9,1},{1,9},{25,17},{17,25},{10,2},{2,... | collective-permute-start | bytes 393224 | tf_op jit(solution)/shard_map/ppermute | solution.py:40
  98.0 13.1 %collective-permute-start.25 = (bf16[64,1024]{1,0:T(8,128)(2,1)S(1)}, bf16[64,1024]{1,0:T(8,128)(2,1)S(1)}, u32[]{:S(2)}, u32[]{:S(2)}) collective-permute-start(bf16[64,1024]{1,0:T(8,128)(2,1)S(1)} %get-tuple-element.76), channel_id=1, source_target_pairs={{8,0},{0,8},{24,16},{16,24},{9,1},{1,9},{25,17},{17,25},{10,2},{2,... | collective-permute-start | bytes 393224 | tf_op jit(solution)/shard_map/ppermute | solution.py:40
  107.5 47.8 %collective-permute-start.11 = (bf16[272,2048]{1,0:T(8,128)(2,1)S(1)}, bf16[272,2048]{1,0:T(8,128)(2,1)S(1)}, u32[]{:S(2)}, u32[]{:S(2)}) collective-permute-start(bf16[272,2048]{1,0:T(8,128)(2,1)S(1)} %expert_layer.5), channel_id=1, source_target_pairs={{0,2},{1,3},{2,0},{3,1},{4,6},{5,7},{6,4},{7,5},{8,10},{9,11},{10,... | collective-permute-start | bytes 3342344 | tf_op jit(solution)/shard_map/ppermute | solution.py:46
  115.5 12.7 %collective-permute-start.40 = (bf16[64,1024]{1,0:T(8,128)(2,1)S(1)}, bf16[64,1024]{1,0:T(8,128)(2,1)S(1)}, u32[]{:S(2)}, u32[]{:S(2)}) collective-permute-start(bf16[64,1024]{1,0:T(8,128)(2,1)S(1)} %get-tuple-element.89), channel_id=1, source_target_pairs={{8,0},{0,8},{24,16},{16,24},{9,1},{1,9},{25,17},{17,25},{10,2},{2,... | collective-permute-start | bytes 393224 | tf_op jit(solution)/shard_map/ppermute | solution.py:40
  117.6 11.8 %collective-permute-start.41 = (bf16[64,1024]{1,0:T(8,128)(2,1)S(1)}, bf16[64,1024]{1,0:T(8,128)(2,1)S(1)}, u32[]{:S(2)}, u32[]{:S(2)}) collective-permute-start(bf16[64,1024]{1,0:T(8,128)(2,1)S(1)} %get-tuple-element.90), channel_id=1, source_target_pairs={{16,0},{24,8},{0,16},{8,24},{17,1},{25,9},{1,17},{9,25},{18,2},{26... | collective-permute-start | bytes 393224 | tf_op jit(solution)/shard_map/ppermute | solution.py:40
  121.1 17.7 %collective-permute-start.28 = (bf16[144,1024]{1,0:T(8,128)(2,1)S(1)}, bf16[144,1024]{1,0:T(8,128)(2,1)S(1)}, u32[]{:S(2)}, u32[]{:S(2)}) collective-permute-start(bf16[144,1024]{1,0:T(8,128)(2,1)S(1)} %combine.5.share_ref), channel_id=1, source_target_pairs={{0,2},{1,3},{6,4},{7,5},{8,10},{9,11},{14,12},{15,13},{16,18},{17,... | collective-permute-start | bytes 884744 | tf_op jit(solution)/shard_map/ppermute | solution.py:46
  129.4 15.7 %collective-permute-start.23 = (bf16[144,1024]{1,0:T(8,128)(2,1)S(1)}, bf16[144,1024]{1,0:T(8,128)(2,1)S(1)}, u32[]{:S(2)}, u32[]{:S(2)}) collective-permute-start(bf16[144,1024]{1,0:T(8,128)(2,1)S(1)} %combine.4.share_ref), channel_id=1, source_target_pairs={{0,2},{1,3},{6,4},{7,5},{8,10},{9,11},{14,12},{15,13},{16,18},{17,... | collective-permute-start | bytes 884744 | tf_op jit(solution)/shard_map/ppermute | solution.py:46
  133.6 17.2 %collective-permute-start.43 = (bf16[144,1024]{1,0:T(8,128)(2,1)S(1)}, bf16[144,1024]{1,0:T(8,128)(2,1)S(1)}, u32[]{:S(2)}, u32[]{:S(2)}) collective-permute-start(bf16[144,1024]{1,0:T(8,128)(2,1)S(1)} %combine.7.share_ref), channel_id=1, source_target_pairs={{0,2},{1,3},{6,4},{7,5},{8,10},{9,11},{14,12},{15,13},{16,18},{17,... | collective-permute-start | bytes 884744 | tf_op jit(solution)/shard_map/ppermute | solution.py:46
  136.1 17.8 %collective-permute-start.38 = (bf16[144,1024]{1,0:T(8,128)(2,1)S(1)}, bf16[144,1024]{1,0:T(8,128)(2,1)S(1)}, u32[]{:S(2)}, u32[]{:S(2)}) collective-permute-start(bf16[144,1024]{1,0:T(8,128)(2,1)S(1)} %combine.6.share_ref), channel_id=1, source_target_pairs={{0,2},{1,3},{6,4},{7,5},{8,10},{9,11},{14,12},{15,13},{16,18},{17,... | collective-permute-start | bytes 884744 | tf_op jit(solution)/shard_map/ppermute | solution.py:46
  138.8 17.7 %collective-permute-start.29 = (bf16[144,1024]{1,0:T(8,128)(2,1)S(1)}, bf16[144,1024]{1,0:T(8,128)(2,1)S(1)}, u32[]{:S(2)}, u32[]{:S(2)}) collective-permute-start(bf16[144,1024]{1,0:T(8,128)(2,1)S(1)} %merge.7), channel_id=1, source_target_pairs={{2,4},{3,5},{4,2},{5,3},{10,12},{11,13},{12,10},{13,11},{18,20},{1... | collective-permute-start | bytes 884744 | tf_op jit(solution)/shard_map/ppermute | solution.py:46
  145.2 11.4 %collective-permute-start.24 = (bf16[144,1024]{1,0:T(8,128)(2,1)S(1)}, bf16[144,1024]{1,0:T(8,128)(2,1)S(1)}, u32[]{:S(2)}, u32[]{:S(2)}) collective-permute-start(bf16[144,1024]{1,0:T(8,128)(2,1)S(1)} %merge.6), channel_id=1, source_target_pairs={{2,4},{3,5},{4,2},{5,3},{10,12},{11,13},{12,10},{13,11},{18,20},{1... | collective-permute-start | bytes 884744 | tf_op jit(solution)/shard_map/ppermute | solution.py:46
  150.8 12.2 %collective-permute-start.44 = (bf16[144,1024]{1,0:T(8,128)(2,1)S(1)}, bf16[144,1024]{1,0:T(8,128)(2,1)S(1)}, u32[]{:S(2)}, u32[]{:S(2)}) collective-permute-start(bf16[144,1024]{1,0:T(8,128)(2,1)S(1)} %merge.9), channel_id=1, source_target_pairs={{2,6},{3,7},{4,0},{5,1},{10,14},{11,15},{12,8},{13,9},{18,22},{19,... | collective-permute-start | bytes 884744 | tf_op jit(solution)/shard_map/ppermute | solution.py:46
  154.0 12.2 %collective-permute-start.39 = (bf16[144,1024]{1,0:T(8,128)(2,1)S(1)}, bf16[144,1024]{1,0:T(8,128)(2,1)S(1)}, u32[]{:S(2)}, u32[]{:S(2)}) collective-permute-start(bf16[144,1024]{1,0:T(8,128)(2,1)S(1)} %merge.8), channel_id=1, source_target_pairs={{2,6},{3,7},{4,0},{5,1},{10,14},{11,15},{12,8},{13,9},{18,22},{19,... | collective-permute-start | bytes 884744 | tf_op jit(solution)/shard_map/ppermute | solution.py:46
  (23 other events, 339.2 us)

commit v3 on v2

--- a/solution.py
+++ b/solution.py
@@ -202,7 +202,7 @@
 
 def prepare_kernel(expert_count, capacity, me_ref, *refs):
     inputs, outputs, scratch = refs[:6], refs[6:-6], refs[-6:]
-    packed_ref, *out_refs = outputs
+    packed_ref, mix_ref, *out_refs = outputs
     both_ref = scratch[4]
     tokens_ref, gain_ref, routes_ref, scores_ref = scratch[:4]
     half = both_ref.shape[1] // 2
@@ -247,8 +247,10 @@
     rows = jnp.concatenate(
         rows + [jnp.zeros((LANES - len(rows), token_count), jnp.float32)], axis=0
     )
-    packed_ref[:, width:] = rows.T.astype(jnp.bfloat16)
+    columns = rows.T.astype(jnp.bfloat16)
+    packed_ref[:, width:] = columns
     slot_count = expert_count * capacity
+    mix_ref[...] = weigh(columns, slot_count, capacity)
     spread(rows, normed, out_refs, slot_count, capacity)
     for ref in out_refs[1:]:
         fold = width // both_ref.shape[1]
@@ -268,12 +270,13 @@
     token_count, width = tokens.shape
     both = (keys.shape[0], keys.shape[1] + values.shape[1])
     shapes = [jax.ShapeDtypeStruct((token_count, width + LANES), jnp.bfloat16)]
+    shapes += [jax.ShapeDtypeStruct((token_count, expert_count * capacity), jnp.bfloat16)]
     shapes += piece_shapes(piece_count, expert_count * capacity, width)
     extra = both[0] * both[1] // width
-    shapes[2:] = [jax.ShapeDtypeStruct((capacity + extra, width), jnp.bfloat16)] * (piece_count - 1)
+    shapes[3:] = [jax.ShapeDtypeStruct((capacity + extra, width), jnp.bfloat16)] * (piece_count - 1)
     args = (tokens, gain[None], routes.T, scores.T, keys, values)
     args = tuple(pltpu.with_memory_space_constraint(a, pltpu.HBM) for a in args)
-    packed, *pieces = pl.pallas_call(
+    packed, mix, *pieces = pl.pallas_call(
         lambda *refs: prepare_kernel(expert_count, capacity, *refs),
         out_shape=shapes,
         in_specs=[SCALAR] + [REMAIN] * len(args),
@@ -286,7 +289,7 @@
         ),
         name="prepare",
     )(me, *args)
-    return packed, pieces
+    return packed, mix, pieces
 
 
 def select(me, candidates, piece_count, slot_count, capacity):
@@ -297,14 +300,14 @@
         packed = refs[0][...]
         if len(candidates) > 1:
             packed = jnp.where(me_ref[1] == 1, packed, refs[1][...])
-        columns_ref, *out_refs = refs[len(candidates) :]
-        columns_ref[...] = packed[:, width:]
+        mix_ref, *out_refs = refs[len(candidates) :]
+        mix_ref[...] = weigh(packed[:, width:], slot_count, capacity)
         rows = packed[:, width:].astype(jnp.float32).T
         spread(rows, packed[:, :width], out_refs, slot_count, capacity)
 
-    shapes = [jax.ShapeDtypeStruct((token_count, LANES), jnp.bfloat16)]
+    shapes = [jax.ShapeDtypeStruct((token_count, slot_count), jnp.bfloat16)]
     shapes += piece_shapes(piece_count, slot_count, width)
-    columns, *pieces = pl.pallas_call(
+    mix, *pieces = pl.pallas_call(
         kernel,
         out_shape=shapes,
         in_specs=[SCALAR] + [VECTOR] * len(candidates),
@@ -315,7 +318,7 @@
         ),
         name="select",
     )(me, *candidates)
-    return columns, pieces
+    return mix, pieces
 
 
 def hold(arrays):
@@ -402,8 +405,7 @@
     return [results[outputs * p : outputs * (p + 1)] for p in range(parts)]
 
 
-def mixing(columns, piece_refs, capacity):
-    slot_count = sum(ref.shape[0] for ref in piece_refs)
+def weigh(columns, slot_count, capacity):
     columns = columns.astype(jnp.float32)
     slots = lax.broadcasted_iota(jnp.int32, (1, slot_count), 1).astype(jnp.float32)
     mix = 0.0
@@ -411,8 +413,11 @@
         near = columns[:, TOP_K + k : TOP_K + k + 1]
         hit = near * capacity + columns[:, k : k + 1] == slots
         mix = mix + jnp.where(hit, columns[:, 2 * TOP_K + k : 2 * TOP_K + k + 1], 0.0)
-    rows = jnp.concatenate([ref[...] for ref in piece_refs], axis=0)
-    return dot(mix.astype(jnp.bfloat16), rows)
+    return mix.astype(jnp.bfloat16)
+
+
+def mixing(mix, piece_refs):
+    return dot(mix, jnp.concatenate([ref[...] for ref in piece_refs], axis=0))
 
 
 def owed(keep_ref, took_ref, target):
@@ -420,12 +425,12 @@
     return both.astype(jnp.bfloat16)
 
 
-def combine(columns, pieces, capacity, level=None, part=0, terms=()):
-    token_count, wide = columns.shape[0], pieces[0].shape[1]
-
-    def kernel(columns_ref, *refs):
+def combine(mix, pieces, level=None, part=0, terms=()):
+    token_count, wide = mix.shape[0], pieces[0].shape[1]
+
+    def kernel(mix_ref, *refs):
         piece_refs, out_ref = refs[len(terms) : -1], refs[-1]
-        mixed = mixing(columns_ref[...], piece_refs, capacity).astype(jnp.bfloat16)
+        mixed = mixing(mix_ref[...], piece_refs).astype(jnp.bfloat16)
         out_ref[:token_count] = mixed
         if terms:
             me_ref, keep_ref, took_ref = refs[:3]
@@ -444,7 +449,7 @@
             flops=1_500_000_000, bytes_accessed=2_000_000, transcendentals=0
         ),
         name="combine",
-    )(columns, *terms, *pieces)
+    )(mix, *terms, *pieces)
 
 
 def owners(me, keep, took, levels):
@@ -500,17 +505,17 @@
     )(share, beside)
 
 
-def finish(me, packed, pieces, capacity, shares, keep, took, mixers):
-    token_count, width = packed.shape
-    width -= LANES
+def finish(me, mix, pieces, shares, keep, took, mixers):
+    token_count = mix.shape[0]
+    width = keep.shape[2]
     owned = keep.shape[1]
 
-    def kernel(me_ref, columns_ref, keep_ref, took_ref, *refs):
+    def kernel(me_ref, mix_ref, keep_ref, took_ref, *refs):
         piece_refs = refs[: len(pieces)]
         share_refs = refs[len(pieces) : len(pieces) + len(shares)]
         mixer_refs = refs[len(pieces) + len(shares) : -2]
         expert_ref, mixer_ref = refs[-2:]
-        total = mixing(columns_ref[...], piece_refs, capacity)
+        total = mixing(mix_ref[...], piece_refs)
         level = me_ref[3]
         mixer = keep_ref[level].astype(jnp.float32) + took_ref[level].astype(jnp.float32)
         for ref in mixer_refs:
@@ -539,9 +544,9 @@
         kernel,
         grid=(1,),
         out_shape=shapes,
-        in_specs=[SCALAR, pl.BlockSpec((token_count, LANES), lambda i: (0, width // LANES))]
-        + [whole(a) for a in arrays[: -len(shares)]]
-        + [VECTOR] * len(shares)
+        in_specs=[SCALAR]
+        + [whole(a) for a in (mix, keep, took)]
+        + [VECTOR] * (len(pieces) + len(shares))
         + ends,
         out_specs=[whole(a) for a in shapes],
         compiler_params=PARAMS,
@@ -549,7 +554,7 @@
             flops=1_500_000_000, bytes_accessed=2_000_000, transcendentals=0
         ),
         name="finish",
-    )(me, packed, *arrays, *mixers)
+    )(me, mix, *arrays, *mixers)
 
 
 def body(
@@ -579,7 +584,7 @@
     outer = (level_index == 0) | (level_index == levels - 1)
     core_index = lax.axis_index("tp") % CORES
     me = jnp.stack([lax.axis_index("ep"), outer, core_index, level_index]).astype(jnp.int32)
-    packed, pieces = prepare(
+    packed, mix, pieces = prepare(
         me,
         routed_tokens,
         expert_gain,
@@ -616,12 +621,12 @@
     )
     took = over_core(give, 1)
 
-    columns = [None]
+    mixes = [mix]
     for level in range(1, levels):
-        column, picked = select(
+        mix, picked = select(
             me, blocks[level - 1], piece_count, slot_count, capacity
         )
-        columns.append(column)
+        mixes.append(mix)
         arrived.append(over_ep(picked))
 
     piece_rows = slot_count // piece_count
@@ -635,7 +640,7 @@
         for part, results in enumerate(layer(level, parts=parts)):
             returned = over_ep(results, back=True)
             shares.append(
-                combine(columns[level], returned, capacity, level, part, **options)
+                combine(mixes[level], returned, level, part, **options)
             )
         return shares
 
@@ -661,7 +666,7 @@
         results = layer(0)[0]
     returned = over_ep(results, back=True)
     expert_output, mixer_output = finish(
-        me, packed, returned, capacity, shares, keep, took, mixers
+        me, mixes[0], returned, shares, keep, took, mixers
     )
     return (mixer_output, expert_output)
 

time: 169 us -> 168 us (level)
  transfers between devices with their start and end apart: 45 -> 45, of which waited for: 15 -> 16; matrix products, arithmetic and copies ran while one was open for 0% -> 0% of each run, Pallas kernels for 16% -> 16%
where the time goes in v3:
time: 168 us
  waiting for transfers between devices  82.3 us (49%)
  starting transfers between devices  52.8 us (31%)
  Pallas kernels  31.5 us (19%)
    ppermute x14, waiting for transfers between devices, over_z(): return lax.ppermute(array, 'tp', pairs)  51.2 us
    ppermute x27, waiting for transfers between devices, over_ep(): moved.append(lax.ppermute(pieces[step], 'ep', pairs))  31.1 us
    ppermute x27, starting transfers between devices, over_ep(): moved.append(lax.ppermute(pieces[step], 'ep', pairs))  30.8 us
    ppermute x14, starting transfers between devices, over_z(): return lax.ppermute(array, 'tp', pairs)  22 us
    pallas_call x4, Pallas kernels, expert_layer(): pl.pallas_call(kernel, out_shape=shapes, in_specs=[VECTOR] * count + [SCA...  14.7 us
    pallas_call x1, Pallas kernels, attention(): pl.pallas_call(lambda *refs: attention_kernel(slots, *refs), out_shape=[j...  4.7 us
    pallas_call x3, Pallas kernels, select(): pl.pallas_call(kernel, out_shape=shapes, in_specs=[SCALAR] + [VECTOR] * l...  3.66 us
  transfers between devices with their start and end apart: 45, of which 16 were waited for; matrix products, arithmetic and copies ran while one was open for 0% of the time, Pallas kernels for 16%

profile of v3, /device:TPU:0, one launch (start us, length us, event | category | flops | bytes accessed | tf_op | source)
XLA Modules:
  0.0 167.9 jit_solution(7619164349257630899)
XLA Ops:
  0.8 2.6 %prepare.1 = (bf16[128,2176]{1,0:T(8,128)(2,1)S(1)}, bf16[128,256]{1,0:T(8,128)(2,1)S(1)}, bf16[64,2048]{1,0:T(8,128)(2,1)S(1)}, bf16[96,2048]{1,0:T(8,128)(2,1)...) custom-call(s32[4]{0:T(128)S(1)} %pad_add_fusion.refs_0_.me_ref.refs_4_, bf16[128,2048]{1,0:T(8,128)(2,1)} %refs_1_.2, ...), custom_call_target="tpu_custom_call" | custom-call | flops 2000000000 | bytes 3000000 | tf_op jit(solution)/shard_map/prepare/pallas_call | solution.py:279
  3.4 3.0 %collective-permute-start = (bf16[96,2048]{1,0:T(8,128)(2,1)S(1)}, bf16[96,2048]{1,0:T(8,128)(2,1)S(1)}, u32[]{:S(2)}, u32[]{:S(2)}) collective-permute-start(bf16[96,2048]{1,0:T(8,128)(2,1)S(1)} %get-tuple-element.50), channel_id=1, source_target_pairs={{0,8},{8,0},{16,24},{24,16},{1,9},{9,1},{17,25},{25,17},{2,10},{10... | collective-permute-start | bytes 1179656 | tf_op jit(solution)/shard_map/ppermute | solution.py:40
  8.0 1.6 collective-permute-start.7
  10.0 6.4 %collective-permute-done.refs_8_.refs_1_ = bf16[96,2048]{1,0:T(8,128)(2,1)S(1)} collective-permute-done((bf16[96,2048]{1,0:T(8,128)(2,1)S(1)}, bf16[96,2048]{1,0:T(8,128)(2,1)S(1)}, u32[]{:S(2)}, u32[]{:S(2)}) %collective-permute-start) | collective-permute-done | bytes 393248 | tf_op jit(solution)/shard_map/ppermute | solution.py:40
  16.4 9.0 %collective-permute-done.1.refs_9_.refs_2_ = bf16[96,2048]{1,0:T(8,128)(2,1)S(1)} collective-permute-done((bf16[96,2048]{1,0:T(8,128)(2,1)S(1)}, bf16[96,2048]{1,0:T(8,128)(2,1)S(1)}, u32[]{:S(2)}, u32[]{:S(2)}) %collective-permute-start.1) | collective-permute-done | bytes 393248 | tf_op jit(solution)/shard_map/ppermute | solution.py:40
  29.6 4.7 %attention.1 = (bf16[4,16,2048]{2,1,0:T(8,128)(2,1)S(1)}, bf16[4,16,2048]{2,1,0:T(8,128)(2,1)S(1)}) custom-call(s32[4]{0:T(128)S(1)} %pad_add_fusion.refs_0_.me_ref.refs_4_, f32[4]{0:T(128)S(1)} %copy-done.7, bf16[128,256]{1,0:T(8,128)(2,1)S(1)} %copy-done.6, f32[1,64]{1,0:T(1,128)S(1)} %bitcast.31, f32[1,64]{1,0:T(1,128)S(1)} %bitcast.32, ...), custom_call_target="tpu_custom_call" | custom-call | flops 6000000000 | bytes 3000000 | tf_op jit(solution)/shard_map/attention/pallas_call | solution.py:170
  34.3 23.4 %collective-permute-done.16.refs_0_ = bf16[128,2176]{1,0:T(8,128)(2,1)S(1)} collective-permute-done((bf16[128,2176]{1,0:T(8,128)(2,1)S(1)}, bf16[128,2176]{1,0:T(8,128)(2,1)S(1)}, u32[]{:S(2)}, u32[]{:S(2)}) %collective-permute-start.16) | collective-permute-done | bytes 557088 | tf_op jit(solution)/shard_map/ppermute | solution.py:46
  58.8 10.8 %collective-permute-done.31.refs_0_ = bf16[128,2176]{1,0:T(8,128)(2,1)S(1)} collective-permute-done((bf16[128,2176]{1,0:T(8,128)(2,1)S(1)}, bf16[128,2176]{1,0:T(8,128)(2,1)S(1)}, u32[]{:S(2)}, u32[]{:S(2)}) %collective-permute-start.31) | collective-permute-done | bytes 557088 | tf_op jit(solution)/shard_map/ppermute | solution.py:46
  71.1 1.6 select.9
  73.9 2.0 %collective-permute-start.8 = (bf16[64,2048]{1,0:T(8,128)(2,1)S(1)}, bf16[64,2048]{1,0:T(8,128)(2,1)S(1)}, u32[]{:S(2)}, u32[]{:S(2)}) collective-permute-start(bf16[64,2048]{1,0:T(8,128)(2,1)S(1)} %get-tuple-element.61), channel_id=1, source_target_pairs={{0,8},{8,0},{16,24},{24,16},{1,9},{9,1},{17,25},{25,17},{2,10},{10... | collective-permute-start | bytes 786440 | tf_op jit(solution)/shard_map/ppermute | solution.py:40
  76.3 1.6 collective-permute-start.9
  77.9 6.7 %collective-permute-done.18.refs_2_ = bf16[64,2048]{1,0:T(8,128)(2,1)S(1)} collective-permute-done((bf16[64,2048]{1,0:T(8,128)(2,1)S(1)}, bf16[64,2048]{1,0:T(8,128)(2,1)S(1)}, u32[]{:S(2)}, u32[]{:S(2)}) %collective-permute-start.18) | collective-permute-done | bytes 262176 | tf_op jit(solution)/shard_map/ppermute | solution.py:40
  85.0 1.7 %collective-permute-start.32 = (bf16[64,2048]{1,0:T(8,128)(2,1)S(1)}, bf16[64,2048]{1,0:T(8,128)(2,1)S(1)}, u32[]{:S(2)}, u32[]{:S(2)}) collective-permute-start(bf16[64,2048]{1,0:T(8,128)(2,1)S(1)} %get-tuple-element.83), channel_id=1, source_target_pairs={{0,8},{8,0},{16,24},{24,16},{1,9},{9,1},{17,25},{25,17},{2,10},{10... | collective-permute-start | bytes 786440 | tf_op jit(solution)/shard_map/ppermute | solution.py:40
  86.7 3.5 %expert_layer.6 = (bf16[64,1024]{1,0:T(8,128)(2,1)S(1)}, bf16[64,1024]{1,0:T(8,128)(2,1)S(1)}, bf16[64,1024]{1,0:T(8,128)(2,1)S(1)}, bf16[64,1024]{1,0:T(8,128)(...) custom-call(bf16[64,2048]{1,0:T(8,128)(2,1)S(1)} %get-tuple-element., ...), custom_call_target="tpu_custom_call" | custom-call | flops 2818572288 | bytes 11010048 | tf_op jit(solution)/shard_map/expert_layer/pallas_call | solution.py:389
  92.1 5.8 %collective-permute-done.9.refs_2_ = bf16[64,2048]{1,0:T(8,128)(2,1)S(1)} collective-permute-done((bf16[64,2048]{1,0:T(8,128)(2,1)S(1)}, bf16[64,2048]{1,0:T(8,128)(2,1)S(1)}, u32[]{:S(2)}, u32[]{:S(2)}) %collective-permute-start.9) | collective-permute-done | bytes 262176 | tf_op jit(solution)/shard_map/ppermute | solution.py:40
  97.9 2.0 %collective-permute-start.25 = (bf16[64,1024]{1,0:T(8,128)(2,1)S(1)}, bf16[64,1024]{1,0:T(8,128)(2,1)S(1)}, u32[]{:S(2)}, u32[]{:S(2)}) collective-permute-start(bf16[64,1024]{1,0:T(8,128)(2,1)S(1)} %get-tuple-element.78), channel_id=1, source_target_pairs={{8,0},{0,8},{24,16},{16,24},{9,1},{1,9},{25,17},{17,25},{10,2},{2,... | collective-permute-start | bytes 393224 | tf_op jit(solution)/shard_map/ppermute | solution.py:40
  99.9 4.1 %expert_layer.5 = bf16[272,2048]{1,0:T(8,128)(2,1)S(1)} custom-call(bf16[64,2048]{1,0:T(8,128)(2,1)S(1)} %get-tuple-element.60.refs_0_, bf16[64,2048]{1,0:T(8,128)(2,1)S(1)} %collective-permute-done.8.refs_1_, bf16[64,2048]{1,0:T(8,128)(2,1)S(1)} %collective-permute-done.9.refs_2_, bf16[64,2048]{1,0:T(8,128)(2,1)S(1)} %collective-permute-done.10.refs_3_, ...), custom_call_target="tpu_custom_call" | custom-call | flops 2818572288 | bytes 11010048 | tf_op jit(solution)/shard_map/expert_layer/pallas_call | solution.py:389
  104.7 2.5 %collective-permute-done.33.refs_2_ = bf16[64,2048]{1,0:T(8,128)(2,1)S(1)} collective-permute-done((bf16[64,2048]{1,0:T(8,128)(2,1)S(1)}, bf16[64,2048]{1,0:T(8,128)(2,1)S(1)}, u32[]{:S(2)}, u32[]{:S(2)}) %collective-permute-start.33) | collective-permute-done | bytes 262176 | tf_op jit(solution)/shard_map/ppermute | solution.py:40
  107.5 3.5 %expert_layer.7 = (bf16[64,1024]{1,0:T(8,128)(2,1)S(1)}, bf16[64,1024]{1,0:T(8,128)(2,1)S(1)}, bf16[64,1024]{1,0:T(8,128)(2,1)S(1)}, bf16[64,1024]{1,0:T(8,128)(...) custom-call(bf16[64,2048]{1,0:T(8,128)(2,1)S(1)} %get-tuple-element., ...), custom_call_target="tpu_custom_call" | custom-call | flops 2818572288 | bytes 11010048 | tf_op jit(solution)/shard_map/expert_layer/pallas_call | solution.py:389
  112.1 2.3 %collective-permute-start.22 = (bf16[64,1024]{1,0:T(8,128)(2,1)S(1)}, bf16[64,1024]{1,0:T(8,128)(2,1)S(1)}, u32[]{:S(2)}, u32[]{:S(2)}) collective-permute-start(bf16[64,1024]{1,0:T(8,128)(2,1)S(1)} %get-tuple-element.76), channel_id=1, source_target_pairs={{24,0},{16,8},{8,16},{0,24},{25,1},{17,9},{9,17},{1,25},{26,2},{18... | collective-permute-start | bytes 393224 | tf_op jit(solution)/shard_map/ppermute | solution.py:40
  115.4 2.0 %collective-permute-start.40 = (bf16[64,1024]{1,0:T(8,128)(2,1)S(1)}, bf16[64,1024]{1,0:T(8,128)(2,1)S(1)}, u32[]{:S(2)}, u32[]{:S(2)}) collective-permute-start(bf16[64,1024]{1,0:T(8,128)(2,1)S(1)} %get-tuple-element.91), channel_id=1, source_target_pairs={{8,0},{0,8},{24,16},{16,24},{9,1},{1,9},{25,17},{17,25},{10,2},{2,... | collective-permute-start | bytes 393224 | tf_op jit(solution)/shard_map/ppermute | solution.py:40
  118.9 2.2 %collective-permute-start.42 = (bf16[64,1024]{1,0:T(8,128)(2,1)S(1)}, bf16[64,1024]{1,0:T(8,128)(2,1)S(1)}, u32[]{:S(2)}, u32[]{:S(2)}) collective-permute-start(bf16[64,1024]{1,0:T(8,128)(2,1)S(1)} %get-tuple-element.93), channel_id=1, source_target_pairs={{24,0},{16,8},{8,16},{0,24},{25,1},{17,9},{9,17},{1,25},{26,2},{18... | collective-permute-start | bytes 393224 | tf_op jit(solution)/shard_map/ppermute | solution.py:40
  121.1 6.3 %collective-permute-start.28 = (bf16[144,1024]{1,0:T(8,128)(2,1)S(1)}, bf16[144,1024]{1,0:T(8,128)(2,1)S(1)}, u32[]{:S(2)}, u32[]{:S(2)}) collective-permute-start(bf16[144,1024]{1,0:T(8,128)(2,1)S(1)} %combine.5.share_ref), channel_id=1, source_target_pairs={{0,2},{1,3},{6,4},{7,5},{8,10},{9,11},{14,12},{15,13},{16,18},{17,... | collective-permute-start | bytes 884744 | tf_op jit(solution)/shard_map/ppermute | solution.py:46
  129.3 3.4 %collective-permute-start.23 = (bf16[144,1024]{1,0:T(8,128)(2,1)S(1)}, bf16[144,1024]{1,0:T(8,128)(2,1)S(1)}, u32[]{:S(2)}, u32[]{:S(2)}) collective-permute-start(bf16[144,1024]{1,0:T(8,128)(2,1)S(1)} %combine.4.share_ref), channel_id=1, source_target_pairs={{0,2},{1,3},{6,4},{7,5},{8,10},{9,11},{14,12},{15,13},{16,18},{17,... | collective-permute-start | bytes 884744 | tf_op jit(solution)/shard_map/ppermute | solution.py:46
  137.2 1.6 collective-permute-done.28.beside_ref
  139.5 5.6 %collective-permute-done.23.beside_ref = bf16[144,1024]{1,0:T(8,128)(2,1)S(1)} collective-permute-done((bf16[144,1024]{1,0:T(8,128)(2,1)S(1)}, bf16[144,1024]{1,0:T(8,128)(2,1)S(1)}, u32[]{:S(2)}, u32[]{:S(2)}) %collective-permute-start.23) | collective-permute-done | bytes 294944 | tf_op jit(solution)/shard_map/ppermute | solution.py:46
  146.1 3.5 %expert_layer.4.share_ref = bf16[256,2048]{1,0:T(8,128)(2,1)S(1)} custom-call(bf16[64,2048]{1,0:T(8,128)(2,1)S(1)} %get-tuple-element.55.refs_0_, bf16[96,2048]{1,0:T(8,128)(2,1)S(1)} %collective-permute-done.refs_8_.refs_1_, bf16[96,2048]{1,0:T(8,128)(2,1)S(1)} %collective-permute-done.1.refs_9_.refs_2_, ...), custom_call_target="tpu_custom_call" | custom-call | flops 2818572288 | bytes 11010048 | tf_op jit(solution)/shard_map/expert_layer/pallas_call | solution.py:389
  152.1 1.8 %collective-permute-done.38.beside_ref = bf16[144,1024]{1,0:T(8,128)(2,1)S(1)} collective-permute-done((bf16[144,1024]{1,0:T(8,128)(2,1)S(1)}, bf16[144,1024]{1,0:T(8,128)(2,1)S(1)}, u32[]{:S(2)}, u32[]{:S(2)}) %collective-permute-start.38) | collective-permute-done | bytes 294944 | tf_op jit(solution)/shard_map/ppermute | solution.py:46
  156.6 2.6 %collective-permute-start.14 = (bf16[64,2048]{1,0:T(8,128)(2,1)S(1)}, bf16[64,2048]{1,0:T(8,128)(2,1)S(1)}, u32[]{:S(2)}, u32[]{:S(2)}) collective-permute-start(bf16[64,2048]{1,0:T(8,128)(2,1)S(1)} %get-tuple-element.67), channel_id=1, source_target_pairs={{24,0},{16,8},{8,16},{0,24},{25,1},{17,9},{9,17},{1,25},{26,2},{18... | collective-permute-start | bytes 786440 | tf_op jit(solution)/shard_map/ppermute | solution.py:40
  159.1 3.8 %collective-permute-done.44.refs_7_ = bf16[144,1024]{1,0:T(8,128)(2,1)S(1)} collective-permute-done((bf16[144,1024]{1,0:T(8,128)(2,1)S(1)}, bf16[144,1024]{1,0:T(8,128)(2,1)S(1)}, u32[]{:S(2)}, u32[]{:S(2)}) %collective-permute-start.44) | collective-permute-done | bytes 294944 | tf_op jit(solution)/shard_map/ppermute | solution.py:46
  163.0 3.2 %collective-permute-done.39.refs_6_ = bf16[144,1024]{1,0:T(8,128)(2,1)S(1)} collective-permute-done((bf16[144,1024]{1,0:T(8,128)(2,1)S(1)}, bf16[144,1024]{1,0:T(8,128)(2,1)S(1)}, u32[]{:S(2)}, u32[]{:S(2)}) %collective-permute-start.39) | collective-permute-done | bytes 294944 | tf_op jit(solution)/shard_map/ppermute | solution.py:46
  166.1 1.7 %finish.1 = (bf16[128,2048]{1,0:T(8,128)(2,1)}, bf16[16,2048]{1,0:T(8,128)(2,1)}) custom-call(s32[4]{0:T(128)S(1)} %pad_add_fusion.refs_0_.me_ref.refs_4_, bf16[128,256]{1,0:T(8,128)(2,1)S(1)} %get-tuple-element.49.mix_ref, bf16[4,16,2048]{2,1,0:T(8,128)(2,1)S(1)} %get-tuple-element.53.refs_5_.refs_1_.keep_ref, ...), custom_call_target="tpu_custom_call" | custom-call | flops 1500000000 | bytes 2000000 | tf_op jit(solution)/shard_map/finish/pallas_call | solution.py:543
  (99 shorter events, 30.3 us)
Async XLA Ops:
  3.4 13.0 %collective-permute-start = (bf16[96,2048]{1,0:T(8,128)(2,1)S(1)}, bf16[96,2048]{1,0:T(8,128)(2,1)S(1)}, u32[]{:S(2)}, u32[]{:S(2)}) collective-permute-start(bf16[96,2048]{1,0:T(8,128)(2,1)S(1)} %get-tuple-element.50), channel_id=1, source_target_pairs={{0,8},{8,0},{16,24},{24,16},{1,9},{9,1},{17,25},{25,17},{2,10},{10... | collective-permute-start | bytes 1179656 | tf_op jit(solution)/shard_map/ppermute | solution.py:40
  6.5 19.0 %collective-permute-start.1 = (bf16[96,2048]{1,0:T(8,128)(2,1)S(1)}, bf16[96,2048]{1,0:T(8,128)(2,1)S(1)}, u32[]{:S(2)}, u32[]{:S(2)}) collective-permute-start(bf16[96,2048]{1,0:T(8,128)(2,1)S(1)} %get-tuple-element.51), channel_id=1, source_target_pairs={{0,16},{8,24},{16,0},{24,8},{1,17},{9,25},{17,1},{25,9},{2,18},{10... | collective-permute-start | bytes 1179656 | tf_op jit(solution)/shard_map/ppermute | solution.py:40
  8.0 63.1 %collective-permute-start.4 = (bf16[448,2048]{1,0:T(8,128)(2,1)S(1)}, bf16[448,2048]{1,0:T(8,128)(2,1)S(1)}, u32[]{:S(2)}, u32[]{:S(2)}) collective-permute-start(bf16[448,2048]{1,0:T(8,128)(2,1)S(1)} %bitcast.16), channel_id=1, source_target_pairs={{0,1},{1,0},{2,3},{3,2},{4,5},{5,4},{6,7},{7,6},{8,9},{9,8},{10,11... | collective-permute-start | bytes 5505032 | tf_op jit(solution)/shard_map/ppermute | solution.py:70
  8.0 18.2 %collective-permute-start.7 = (bf16[128,2176]{1,0:T(8,128)(2,1)S(1)}, bf16[128,2176]{1,0:T(8,128)(2,1)S(1)}, u32[]{:S(2)}, u32[]{:S(2)}) collective-permute-start(bf16[128,2176]{1,0:T(8,128)(2,1)S(1)} %get-tuple-element.59), channel_id=1, source_target_pairs={{0,2},{1,3},{2,0},{3,1},{4,6},{5,7},{6,4},{7,5},{8,10},{9,11},{10,... | collective-permute-start | bytes 1671176 | tf_op jit(solution)/shard_map/ppermute | solution.py:46
  9.6 15.9 %collective-permute-start.2 = (bf16[96,2048]{1,0:T(8,128)(2,1)S(1)}, bf16[96,2048]{1,0:T(8,128)(2,1)S(1)}, u32[]{:S(2)}, u32[]{:S(2)}) collective-permute-start(bf16[96,2048]{1,0:T(8,128)(2,1)S(1)} %get-tuple-element.52), channel_id=1, source_target_pairs={{0,24},{8,16},{16,8},{24,0},{1,25},{9,17},{17,9},{25,1},{2,26},{10... | collective-permute-start | bytes 1179656 | tf_op jit(solution)/shard_map/ppermute | solution.py:40
  16.4 57.3 %collective-permute-start.5 = (bf16[448,2048]{1,0:T(8,128)(2,1)S(1)}, bf16[448,2048]{1,0:T(8,128)(2,1)S(1)}, u32[]{:S(2)}, u32[]{:S(2)}) collective-permute-start(bf16[448,2048]{1,0:T(8,128)(2,1)S(1)} %bitcast.21), channel_id=1, source_target_pairs={{0,1},{1,0},{2,3},{3,2},{4,5},{5,4},{6,7},{7,6},{8,9},{9,8},{10,11... | collective-permute-start | bytes 5505032 | tf_op jit(solution)/shard_map/ppermute | solution.py:70
  25.5 48.4 %collective-permute-start.6 = (bf16[448,2048]{1,0:T(8,128)(2,1)S(1)}, bf16[448,2048]{1,0:T(8,128)(2,1)S(1)}, u32[]{:S(2)}, u32[]{:S(2)}) collective-permute-start(bf16[448,2048]{1,0:T(8,128)(2,1)S(1)} %bitcast.26), channel_id=1, source_target_pairs={{0,1},{1,0},{2,3},{3,2},{4,5},{5,4},{6,7},{7,6},{8,9},{9,8},{10,11... | collective-permute-start | bytes 5505032 | tf_op jit(solution)/shard_map/ppermute | solution.py:70
  26.9 30.8 %collective-permute-start.16 = (bf16[128,2176]{1,0:T(8,128)(2,1)S(1)}, bf16[128,2176]{1,0:T(8,128)(2,1)S(1)}, u32[]{:S(2)}, u32[]{:S(2)}) collective-permute-start(bf16[128,2176]{1,0:T(8,128)(2,1)S(1)} %collective-permute-done.15.refs_1_), channel_id=1, source_target_pairs={{2,0},{3,1},{4,6},{5,7},{10,8},{11,9},{12,14},{13,15},{18,16},{19,... | collective-permute-start | bytes 1671176 | tf_op jit(solution)/shard_map/ppermute | solution.py:46
  28.2 41.4 %collective-permute-start.31 = (bf16[128,2176]{1,0:T(8,128)(2,1)S(1)}, bf16[128,2176]{1,0:T(8,128)(2,1)S(1)}, u32[]{:S(2)}, u32[]{:S(2)}) collective-permute-start(bf16[128,2176]{1,0:T(8,128)(2,1)S(1)} %collective-permute-done.30.refs_1_), channel_id=1, source_target_pairs={{2,0},{3,1},{4,6},{5,7},{10,8},{11,9},{12,14},{13,15},{18,16},{19,... | collective-permute-start | bytes 1671176 | tf_op jit(solution)/shard_map/ppermute | solution.py:46
  58.7 17.6 %collective-permute-start.17 = (bf16[64,2048]{1,0:T(8,128)(2,1)S(1)}, bf16[64,2048]{1,0:T(8,128)(2,1)S(1)}, u32[]{:S(2)}, u32[]{:S(2)}) collective-permute-start(bf16[64,2048]{1,0:T(8,128)(2,1)S(1)} %get-tuple-element.70), channel_id=1, source_target_pairs={{0,8},{8,0},{16,24},{24,16},{1,9},{9,1},{17,25},{25,17},{2,10},{10... | collective-permute-start | bytes 786440 | tf_op jit(solution)/shard_map/ppermute | solution.py:40
  69.6 15.0 %collective-permute-start.18 = (bf16[64,2048]{1,0:T(8,128)(2,1)S(1)}, bf16[64,2048]{1,0:T(8,128)(2,1)S(1)}, u32[]{:S(2)}, u32[]{:S(2)}) collective-permute-start(bf16[64,2048]{1,0:T(8,128)(2,1)S(1)} %get-tuple-element.71), channel_id=1, source_target_pairs={{0,16},{8,24},{16,0},{24,8},{1,17},{9,25},{17,1},{25,9},{2,18},{10... | collective-permute-start | bytes 786440 | tf_op jit(solution)/shard_map/ppermute | solution.py:40
  71.1 13.9 %collective-permute-start.19 = (bf16[64,2048]{1,0:T(8,128)(2,1)S(1)}, bf16[64,2048]{1,0:T(8,128)(2,1)S(1)}, u32[]{:S(2)}, u32[]{:S(2)}) collective-permute-start(bf16[64,2048]{1,0:T(8,128)(2,1)S(1)} %get-tuple-element.72), channel_id=1, source_target_pairs={{0,24},{8,16},{16,8},{24,0},{1,25},{9,17},{17,9},{25,1},{2,26},{10... | collective-permute-start | bytes 786440 | tf_op jit(solution)/shard_map/ppermute | solution.py:40
  73.8 16.5 %collective-permute-start.3 = (bf16[4,16,2048]{2,1,0:T(8,128)(2,1)S(1)}, bf16[4,16,2048]{2,1,0:T(8,128)(2,1)S(1)}, u32[]{:S(2)}, u32[]{:S(2)}) collective-permute-start(bf16[4,16,2048]{2,1,0:T(8,128)(2,1)S(1)} %get-tuple-element.54), channel_id=1, source_target_pairs={{0,1},{1,0},{2,3},{3,2},{4,5},{5,4},{6,7},{7,6},{8,9},{9,8},{10,11... | collective-permute-start | bytes 786440 | tf_op jit(solution)/shard_map/ppermute | solution.py:70
  73.9 17.9 %collective-permute-start.8 = (bf16[64,2048]{1,0:T(8,128)(2,1)S(1)}, bf16[64,2048]{1,0:T(8,128)(2,1)S(1)}, u32[]{:S(2)}, u32[]{:S(2)}) collective-permute-start(bf16[64,2048]{1,0:T(8,128)(2,1)S(1)} %get-tuple-element.61), channel_id=1, source_target_pairs={{0,8},{8,0},{16,24},{24,16},{1,9},{9,1},{17,25},{25,17},{2,10},{10... | collective-permute-start | bytes 786440 | tf_op jit(solution)/shard_map/ppermute | solution.py:40
  76.3 21.6 %collective-permute-start.9 = (bf16[64,2048]{1,0:T(8,128)(2,1)S(1)}, bf16[64,2048]{1,0:T(8,128)(2,1)S(1)}, u32[]{:S(2)}, u32[]{:S(2)}) collective-permute-start(bf16[64,2048]{1,0:T(8,128)(2,1)S(1)} %get-tuple-element.62), channel_id=1, source_target_pairs={{0,16},{8,24},{16,0},{24,8},{1,17},{9,25},{17,1},{25,9},{2,18},{10... | collective-permute-start | bytes 786440 | tf_op jit(solution)/shard_map/ppermute | solution.py:40
  84.6 13.3 %collective-permute-start.10 = (bf16[64,2048]{1,0:T(8,128)(2,1)S(1)}, bf16[64,2048]{1,0:T(8,128)(2,1)S(1)}, u32[]{:S(2)}, u32[]{:S(2)}) collective-permute-start(bf16[64,2048]{1,0:T(8,128)(2,1)S(1)} %get-tuple-element.63), channel_id=1, source_target_pairs={{0,24},{8,16},{16,8},{24,0},{1,25},{9,17},{17,9},{25,1},{2,26},{10... | collective-permute-start | bytes 786440 | tf_op jit(solution)/shard_map/ppermute | solution.py:40
  85.0 19.0 %collective-permute-start.32 = (bf16[64,2048]{1,0:T(8,128)(2,1)S(1)}, bf16[64,2048]{1,0:T(8,128)(2,1)S(1)}, u32[]{:S(2)}, u32[]{:S(2)}) collective-permute-start(bf16[64,2048]{1,0:T(8,128)(2,1)S(1)} %get-tuple-element.83), channel_id=1, source_target_pairs={{0,8},{8,0},{16,24},{24,16},{1,9},{9,1},{17,25},{25,17},{2,10},{10... | collective-permute-start | bytes 786440 | tf_op jit(solution)/shard_map/ppermute | solution.py:40
  90.3 17.0 %collective-permute-start.33 = (bf16[64,2048]{1,0:T(8,128)(2,1)S(1)}, bf16[64,2048]{1,0:T(8,128)(2,1)S(1)}, u32[]{:S(2)}, u32[]{:S(2)}) collective-permute-start(bf16[64,2048]{1,0:T(8,128)(2,1)S(1)} %get-tuple-element.84), channel_id=1, source_target_pairs={{0,16},{8,24},{16,0},{24,8},{1,17},{9,25},{17,1},{25,9},{2,18},{10... | collective-permute-start | bytes 786440 | tf_op jit(solution)/shard_map/ppermute | solution.py:40
  91.7 15.8 %collective-permute-start.34 = (bf16[64,2048]{1,0:T(8,128)(2,1)S(1)}, bf16[64,2048]{1,0:T(8,128)(2,1)S(1)}, u32[]{:S(2)}, u32[]{:S(2)}) collective-permute-start(bf16[64,2048]{1,0:T(8,128)(2,1)S(1)} %get-tuple-element.85), channel_id=1, source_target_pairs={{0,24},{8,16},{16,8},{24,0},{1,25},{9,17},{17,9},{25,1},{2,26},{10... | collective-permute-start | bytes 786440 | tf_op jit(solution)/shard_map/ppermute | solution.py:40
  97.9 17.5 %collective-permute-start.20 = (bf16[64,1024]{1,0:T(8,128)(2,1)S(1)}, bf16[64,1024]{1,0:T(8,128)(2,1)S(1)}, u32[]{:S(2)}, u32[]{:S(2)}) collective-permute-start(bf16[64,1024]{1,0:T(8,128)(2,1)S(1)} %get-tuple-element.74), channel_id=1, source_target_pairs={{8,0},{0,8},{24,16},{16,24},{9,1},{1,9},{25,17},{17,25},{10,2},{2,... | collective-permute-start | bytes 393224 | tf_op jit(solution)/shard_map/ppermute | solution.py:40
  97.9 13.1 %collective-permute-start.25 = (bf16[64,1024]{1,0:T(8,128)(2,1)S(1)}, bf16[64,1024]{1,0:T(8,128)(2,1)S(1)}, u32[]{:S(2)}, u32[]{:S(2)}) collective-permute-start(bf16[64,1024]{1,0:T(8,128)(2,1)S(1)} %get-tuple-element.78), channel_id=1, source_target_pairs={{8,0},{0,8},{24,16},{16,24},{9,1},{1,9},{25,17},{17,25},{10,2},{2,... | collective-permute-start | bytes 393224 | tf_op jit(solution)/shard_map/ppermute | solution.py:40
  107.5 47.8 %collective-permute-start.11 = (bf16[272,2048]{1,0:T(8,128)(2,1)S(1)}, bf16[272,2048]{1,0:T(8,128)(2,1)S(1)}, u32[]{:S(2)}, u32[]{:S(2)}) collective-permute-start(bf16[272,2048]{1,0:T(8,128)(2,1)S(1)} %expert_layer.5), channel_id=1, source_target_pairs={{0,2},{1,3},{2,0},{3,1},{4,6},{5,7},{6,4},{7,5},{8,10},{9,11},{10,... | collective-permute-start | bytes 3342344 | tf_op jit(solution)/shard_map/ppermute | solution.py:46
  115.4 12.7 %collective-permute-start.40 = (bf16[64,1024]{1,0:T(8,128)(2,1)S(1)}, bf16[64,1024]{1,0:T(8,128)(2,1)S(1)}, u32[]{:S(2)}, u32[]{:S(2)}) collective-permute-start(bf16[64,1024]{1,0:T(8,128)(2,1)S(1)} %get-tuple-element.91), channel_id=1, source_target_pairs={{8,0},{0,8},{24,16},{16,24},{9,1},{1,9},{25,17},{17,25},{10,2},{2,... | collective-permute-start | bytes 393224 | tf_op jit(solution)/shard_map/ppermute | solution.py:40
  117.4 11.8 %collective-permute-start.41 = (bf16[64,1024]{1,0:T(8,128)(2,1)S(1)}, bf16[64,1024]{1,0:T(8,128)(2,1)S(1)}, u32[]{:S(2)}, u32[]{:S(2)}) collective-permute-start(bf16[64,1024]{1,0:T(8,128)(2,1)S(1)} %get-tuple-element.92), channel_id=1, source_target_pairs={{16,0},{24,8},{0,16},{8,24},{17,1},{25,9},{1,17},{9,25},{18,2},{26... | collective-permute-start | bytes 393224 | tf_op jit(solution)/shard_map/ppermute | solution.py:40
  121.1 17.7 %collective-permute-start.28 = (bf16[144,1024]{1,0:T(8,128)(2,1)S(1)}, bf16[144,1024]{1,0:T(8,128)(2,1)S(1)}, u32[]{:S(2)}, u32[]{:S(2)}) collective-permute-start(bf16[144,1024]{1,0:T(8,128)(2,1)S(1)} %combine.5.share_ref), channel_id=1, source_target_pairs={{0,2},{1,3},{6,4},{7,5},{8,10},{9,11},{14,12},{15,13},{16,18},{17,... | collective-permute-start | bytes 884744 | tf_op jit(solution)/shard_map/ppermute | solution.py:46
  129.3 15.8 %collective-permute-start.23 = (bf16[144,1024]{1,0:T(8,128)(2,1)S(1)}, bf16[144,1024]{1,0:T(8,128)(2,1)S(1)}, u32[]{:S(2)}, u32[]{:S(2)}) collective-permute-start(bf16[144,1024]{1,0:T(8,128)(2,1)S(1)} %combine.4.share_ref), channel_id=1, source_target_pairs={{0,2},{1,3},{6,4},{7,5},{8,10},{9,11},{14,12},{15,13},{16,18},{17,... | collective-permute-start | bytes 884744 | tf_op jit(solution)/shard_map/ppermute | solution.py:46
  133.4 17.3 %collective-permute-start.43 = (bf16[144,1024]{1,0:T(8,128)(2,1)S(1)}, bf16[144,1024]{1,0:T(8,128)(2,1)S(1)}, u32[]{:S(2)}, u32[]{:S(2)}) collective-permute-start(bf16[144,1024]{1,0:T(8,128)(2,1)S(1)} %combine.7.share_ref), channel_id=1, source_target_pairs={{0,2},{1,3},{6,4},{7,5},{8,10},{9,11},{14,12},{15,13},{16,18},{17,... | collective-permute-start | bytes 884744 | tf_op jit(solution)/shard_map/ppermute | solution.py:46
  135.9 18.0 %collective-permute-start.38 = (bf16[144,1024]{1,0:T(8,128)(2,1)S(1)}, bf16[144,1024]{1,0:T(8,128)(2,1)S(1)}, u32[]{:S(2)}, u32[]{:S(2)}) collective-permute-start(bf16[144,1024]{1,0:T(8,128)(2,1)S(1)} %combine.6.share_ref), channel_id=1, source_target_pairs={{0,2},{1,3},{6,4},{7,5},{8,10},{9,11},{14,12},{15,13},{16,18},{17,... | collective-permute-start | bytes 884744 | tf_op jit(solution)/shard_map/ppermute | solution.py:46
  138.8 17.7 %collective-permute-start.29 = (bf16[144,1024]{1,0:T(8,128)(2,1)S(1)}, bf16[144,1024]{1,0:T(8,128)(2,1)S(1)}, u32[]{:S(2)}, u32[]{:S(2)}) collective-permute-start(bf16[144,1024]{1,0:T(8,128)(2,1)S(1)} %merge.7), channel_id=1, source_target_pairs={{2,4},{3,5},{4,2},{5,3},{10,12},{11,13},{12,10},{13,11},{18,20},{1... | collective-permute-start | bytes 884744 | tf_op jit(solution)/shard_map/ppermute | solution.py:46
  145.2 11.4 %collective-permute-start.24 = (bf16[144,1024]{1,0:T(8,128)(2,1)S(1)}, bf16[144,1024]{1,0:T(8,128)(2,1)S(1)}, u32[]{:S(2)}, u32[]{:S(2)}) collective-permute-start(bf16[144,1024]{1,0:T(8,128)(2,1)S(1)} %merge.6), channel_id=1, source_target_pairs={{2,4},{3,5},{4,2},{5,3},{10,12},{11,13},{12,10},{13,11},{18,20},{1... | collective-permute-start | bytes 884744 | tf_op jit(solution)/shard_map/ppermute | solution.py:46
  150.8 12.2 %collective-permute-start.44 = (bf16[144,1024]{1,0:T(8,128)(2,1)S(1)}, bf16[144,1024]{1,0:T(8,128)(2,1)S(1)}, u32[]{:S(2)}, u32[]{:S(2)}) collective-permute-start(bf16[144,1024]{1,0:T(8,128)(2,1)S(1)} %merge.9), channel_id=1, source_target_pairs={{2,6},{3,7},{4,0},{5,1},{10,14},{11,15},{12,8},{13,9},{18,22},{19,... | collective-permute-start | bytes 884744 | tf_op jit(solution)/shard_map/ppermute | solution.py:46
  154.0 12.2 %collective-permute-start.39 = (bf16[144,1024]{1,0:T(8,128)(2,1)S(1)}, bf16[144,1024]{1,0:T(8,128)(2,1)S(1)}, u32[]{:S(2)}, u32[]{:S(2)}) collective-permute-start(bf16[144,1024]{1,0:T(8,128)(2,1)S(1)} %merge.8), channel_id=1, source_target_pairs={{2,6},{3,7},{4,0},{5,1},{10,14},{11,15},{12,8},{13,9},{18,22},{19,... | collective-permute-start | bytes 884744 | tf_op jit(solution)/shard_map/ppermute | solution.py:46
  (23 other events, 338.9 us)
